TPU v7x, 32 devices: a whole 2x2x4 slice. The times are simulated.
32 devices in a mesh: sp: 8 (over z, y), tp: 4 (over x, core).
Axes of the slice: x: 2, y: 2, z: 4, core: 2. Of those that a mesh axis runs over, the one named last changes fastest.
Arguments:
- stream_in: bfloat16 [2048, 4096], P(('sp', 'tp')), may hold values from -6 to 6
- q_first: bfloat16 [2048, 1024], P('sp', 'tp'), may hold values from -110 to 110
- q_second: bfloat16 [2048, 1024], P('sp', 'tp'), may hold values from -110 to 110
- k_first: bfloat16 [2048, 512], P('sp', 'tp'), may hold values from -7 to 7
- k_second: bfloat16 [2048, 512], P('sp', 'tp'), may hold values from -7 to 7
- values: bfloat16 [2048, 1024], P('sp', 'tp'), may hold values from -6 to 6
- head_lambda: float32 [8], P('tp'), may hold values from 0.3 to 0.8
- w_out: bfloat16 [2048, 4096], P('tp'), may hold values from -0.125 to 0.125
- norm_gain: float32 [4096], replicated, may hold values from 0.1 to 1.9
- routes: int32 [2048, 4], P(('sp', 'tp')), may hold values from 0 to 7, all different within a row; in each aligned block of 64 rows (0 to 63, 64 to 127, ...) at most 48 rows name the same one
- route_w: float32 [2048, 4], P(('sp', 'tp')), may hold values from 0.2 to 1
- w_gate: bfloat16 [8, 4096, 128], P('sp'), may hold values from -0.09375 to 0.09375
- w_up: bfloat16 [8, 4096, 128], P('sp'), may hold values from -0.09375 to 0.09375
- w_down: bfloat16 [8, 128, 4096], P('sp'), may hold values from -0.5 to 0.5
- s_gate: bfloat16 [4096, 512], P(None, 'tp'), may hold values from -0.09375 to 0.09375
- s_up: bfloat16 [4096, 512], P(None, 'tp'), may hold values from -0.09375 to 0.09375
- s_down: bfloat16 [512, 4096], P('tp'), may hold values from -0.25 to 0.25
Outputs:
- layer_out: bfloat16 [2048, 4096], P(('sp', 'tp'))
Inputs may be any that keep to these rules, and one draw needn't show every extreme that they name: `routes`: each row names 4 different experts. Within the rows of one device (aligned blocks of 64 rows) no expert is named more than 48 times, and in some blocks one expert is named exactly 48 times.
All inputs are finite; a program needn't handle non-finite values.
Results may differ from a plain program's by a relative error of at most 0.017.
Values may be sent and summed in bfloat16 or wider, within the bound.
No kernel may reach another device: no remote copies, remote signals or barrier semaphores. Data moves between devices by JAX's collectives and lax.ppermute only.
A program may use at most 128 MiB of HBM per device.

v0:
```python
import math

import jax
import jax.numpy as jnp
from jax import lax
from jax.sharding import PartitionSpec as P

HEAD = 128


FLOOR = -1e30


def absorb(state, first_q, second_q, first_k, second_k, value_rows, query_pos, key_pos):
    allowed = key_pos[None, :] <= query_pos[:, None]
    scale = first_q.shape[-1] ** (-0.5)
    result = []
    pairs = ((first_q, first_k), (second_q, second_k))
    for index in range(2):
        query_rows, key_rows = pairs[index]
        peak, total, accum = (state[3 * index], state[3 * index + 1], state[3 * index + 2])
        scores = (
            jnp.einsum("qagd,kad->agqk", query_rows, key_rows, preferred_element_type=jnp.float32)
            * scale
        )
        scores = jnp.where(allowed, scores, FLOOR)
        raised = jnp.maximum(peak, scores.max(-1))
        weights = jnp.where(allowed, jnp.exp(scores - raised[..., None]), 0.0)
        fade = jnp.exp(peak - raised)
        total = total * fade + weights.sum(-1)
        accum = accum * fade[..., None] + jnp.einsum(
            "agqk,kad->agqd",
            weights.astype(jnp.bfloat16),
            value_rows,
            preferred_element_type=jnp.float32,
        )
        result += [raised, total, accum]
    return tuple(result)


def empty_state(kv_local, group, count, value_dim):
    peaks = jnp.full((kv_local, group, count), FLOOR, jnp.float32)
    sums = jnp.zeros((kv_local, group, count), jnp.float32)
    accums = jnp.zeros((kv_local, group, count, value_dim), jnp.float32)
    return (peaks, sums, accums, peaks, sums, accums)


def fold_rows(state, first_q, second_q, query_pos, last_row, pieces, start):
    first_k, second_k, value_rows = pieces
    length = first_k.shape[0]
    kv_local = first_q.shape[1]
    value_dim = value_rows.shape[1] // kv_local
    span = math.gcd(length, 2048)

    def sweep(current):

        def visit(block, inner):
            begin = block * span
            key_one = lax.dynamic_slice_in_dim(first_k, begin, span, 0).reshape(
                span, kv_local, HEAD
            )
            key_two = lax.dynamic_slice_in_dim(second_k, begin, span, 0).reshape(
                span, kv_local, HEAD
            )
            value_part = lax.dynamic_slice_in_dim(value_rows, begin, span, 0).reshape(
                span, kv_local, value_dim
            )
            key_pos = begin + jnp.arange(span, dtype=jnp.int32)
            return absorb(
                inner, first_q, second_q, key_one, key_two, value_part, query_pos, key_pos
            )

        return lax.fori_loop(0, length // span, visit, current)

    def unchanged(current):
        return current

    return lax.cond(start <= last_row, sweep, unchanged, state)


def finish_heads(final, head_lambda):
    kv_local, group, count, value_dim = final[2].shape
    weight = head_lambda.reshape(kv_local, group, 1, 1)
    head_out = final[2] / final[1][..., None] - weight * final[5] / final[4][..., None]
    head_out = head_out * lax.rsqrt(jnp.mean(head_out * head_out, axis=-1, keepdims=True) + 1e-05)
    return (
        head_out.transpose(2, 0, 1, 3)
        .reshape(count, kv_local * group * value_dim)
        .astype(jnp.bfloat16)
    )


def shared_part(normed, s_gate, s_up, s_down):
    piece = lax.all_gather(normed, "tp", axis=0, tiled=True)
    gate_part = jnp.dot(piece, s_gate, preferred_element_type=jnp.float32)
    up_part = jnp.dot(piece, s_up, preferred_element_type=jnp.float32)
    hidden = (jax.nn.silu(gate_part) * up_part).astype(jnp.bfloat16)
    terms = jnp.dot(hidden, s_down, preferred_element_type=jnp.float32)
    return lax.psum_scatter(
        terms.astype(jnp.bfloat16), "tp", scatter_dimension=0, tiled=True
    ).astype(jnp.float32)


def routed_part(normed, routes, route_w, w_gate, w_up, w_down):
    rows, topk = routes.shape
    local_experts = w_gate.shape[0]
    experts = local_experts * lax.axis_size("sp")
    slots = max(2, 3 * rows * topk // (2 * experts))
    flat_ids = routes.reshape(-1)
    hits = (flat_ids[:, None] == jnp.arange(experts, dtype=jnp.int32)[None, :]).astype(jnp.int32)
    slot_of = jnp.sum(jnp.cumsum(hits, axis=0) * hits, axis=1) - 1
    target = flat_ids * slots + slot_of
    placing = jnp.any(
        jnp.arange(experts * slots, dtype=jnp.int32)[:, None, None]
        == target.reshape(rows, topk)[None, :, :],
        axis=-1,
    ).astype(jnp.bfloat16)
    outgoing = (
        jnp.dot(placing, normed, preferred_element_type=jnp.float32)
        .astype(jnp.bfloat16)
        .reshape(experts, slots, normed.shape[1])
    )
    arrived = lax.all_to_all(outgoing, "sp", split_axis=0, concat_axis=0, tiled=True)
    sources = arrived.shape[0] // local_experts
    grouped = arrived.reshape(sources, local_experts, arrived.shape[1], arrived.shape[2])
    gate_part = jnp.einsum("sjcd,jdf->sjcf", grouped, w_gate, preferred_element_type=jnp.float32)
    up_part = jnp.einsum("sjcd,jdf->sjcf", grouped, w_up, preferred_element_type=jnp.float32)
    hidden = (jax.nn.silu(gate_part) * up_part).astype(jnp.bfloat16)
    result = jnp.einsum(
        "sjcf,jfd->sjcd", hidden, w_down, preferred_element_type=jnp.float32
    ).astype(jnp.bfloat16)
    returned = lax.all_to_all(
        result.reshape(arrived.shape), "sp", split_axis=0, concat_axis=0, tiled=True
    )
    picked = (
        returned.reshape(experts * slots, normed.shape[1])[target]
        .reshape(rows, topk, normed.shape[1])
        .astype(jnp.float32)
    )
    return jnp.sum(picked * route_w[..., None], axis=1)


def local(
    stream_in,
    q_first,
    q_second,
    k_first,
    k_second,
    values,
    head_lambda,
    w_out,
    norm_gain,
    routes,
    route_w,
    w_gate,
    w_up,
    w_down,
    s_gate,
    s_up,
    s_down,
):
    seq_rows = q_first.shape[0]
    kv_local = k_first.shape[1] // HEAD
    heads_local = q_first.shape[1] // HEAD
    group = heads_local // kv_local
    value_dim = values.shape[1] // kv_local
    offset = lax.axis_index("sp") * seq_rows
    query_pos = offset + jnp.arange(seq_rows, dtype=jnp.int32)
    last_row = offset + seq_rows - 1
    first_q = q_first.reshape(seq_rows, kv_local, group, HEAD)
    second_q = q_second.reshape(seq_rows, kv_local, group, HEAD)
    start_state = empty_state(kv_local, group, seq_rows, value_dim)
    folded_state = fold_rows(
        start_state,
        first_q,
        second_q,
        query_pos,
        last_row,
        (
            lax.all_gather(k_first, "sp", axis=0, tiled=True),
            lax.all_gather(k_second, "sp", axis=0, tiled=True),
            lax.all_gather(values, "sp", axis=0, tiled=True),
        ),
        jnp.int32(0),
    )
    attn_rows = finish_heads(folded_state, head_lambda)
    attn = lax.psum_scatter(
        jnp.dot(attn_rows, w_out, preferred_element_type=jnp.float32).astype(jnp.bfloat16),
        "tp",
        scatter_dimension=0,
        tiled=True,
    ).astype(jnp.float32)
    resid = (stream_in.astype(jnp.float32) + attn).astype(jnp.bfloat16)
    stream = lax.optimization_barrier(resid).astype(jnp.float32)
    normed = (
        stream * lax.rsqrt(jnp.mean(stream * stream, axis=-1, keepdims=True) + 1e-06) * norm_gain
    ).astype(jnp.bfloat16)
    routed = routed_part(normed, routes, route_w, w_gate, w_up, w_down)
    shared = shared_part(normed, s_gate, s_up, s_down)
    return (stream + routed + shared).astype(jnp.bfloat16)


def solution(mesh):
    return jax.shard_map(
        local,
        mesh=mesh,
        in_specs=(
            P(("sp", "tp"), None),
            P("sp", "tp"),
            P("sp", "tp"),
            P("sp", "tp"),
            P("sp", "tp"),
            P("sp", "tp"),
            P("tp"),
            P("tp", None),
            P(),
            P(("sp", "tp"), None),
            P(("sp", "tp"), None),
            P("sp", None, None),
            P("sp", None, None),
            P("sp", None, None),
            P(None, "tp"),
            P(None, "tp"),
            P("tp", None),
        ),
        out_specs=P(("sp", "tp"), None),
        check_vma=False,
    )
```

profile of v0, /device:TPU:0, one launch (start us, length us, event | category | flops | bytes accessed | tf_op | source)
XLA Modules:
  0.0 313.2 jit_solution(3209219373579061836)
XLA Ops:
  6.5 0.7 all-gather.3.cloned.1.call-update
  7.3 0.0 reduce-scatter.3.cloned.1.call-start
  7.3 33.8 %all_gather.12 = bf16[2048,128]{1,0:T(8,128)(2,1)S(1)} all-gather(bf16[256,128]{1,0:T(8,128)(2,1)} %param.22), channel_id=1, replica_groups=mesh['sp'=8,'tp'=4] {'sp'}, dimensions={0}, use_global_device_ids=true | all-gather | bytes 589824 | tf_op jit(solution)/shard_map/all_gather | solution.py:180
  41.1 32.0 %all_gather.14 = bf16[2048,128]{1,0:T(8,128)(2,1)S(1)} all-gather(bf16[256,128]{1,0:T(8,128)(2,1)} %param.23), channel_id=1, replica_groups=mesh['sp'=8,'tp'=4] {'sp'}, dimensions={0}, use_global_device_ids=true | all-gather | bytes 589824 | tf_op jit(solution)/shard_map/all_gather | solution.py:181
  73.1 12.4 %conditional.1 = (f32[1,2,256]{2,1,0:T(2,128)S(1)}, f32[1,2,256]{2,1,0:T(2,128)S(1)}, f32[1,2,256,256]{2,3,1,0:T(8,128)S(1)}, f32[1,2,256,256]{2,3,1,0:T(8,128)}) conditional(s32[]{:T(128)} %convert_element_type.75, () %tuple.15, (s32[]{:T(128)}, s32[256]{0:T(256)S(1)}, bf16[256,256]{1,0:T(8,128)(2,1)}, bf16[2048,128]{1,0:T(8,128)(2,1)S(1)}, ...), branch_computations={%region_0.0_spmd, %region_1.6_spmd} | conditional | flops 1638665472 | bytes 60079224 | solution.py:78
  73.1 0.3 iota_compare_fusion
  73.5 1.6 fusion.30
  75.1 1.5 fusion.1
  76.6 0.4 copy-done.1
  77.0 2.1 fusion.5
  79.1 1.5 fusion.17
  80.6 1.0 copy.52
  81.6 3.6 %fusion.23 = f32[1,2,256,256]{3,2,1,0:T(8,128)S(1)} fusion(f32[2048,256,2]{1,0,2:T(8,128)} %copy-done.1, f32[2,256]{1,0:T(2,128)S(1)} %broadcast_maximum_fusion.1, pred[256,2048]{0,1:T(8,128)(4,1)S(1)} %iota_compare_fusion, bf16[2048,256]{1,0:T(8,128)(2,1)S(1)} %copy-done.13, f32[2,256]{1,0:T(2,128)S(1)} %get-tuple-element.98), kind=kOutput, calls=%fused_computation.21 | convolution fusion | flops 542244864 | bytes 6295552 | tf_op jit(solution)/shard_map/cond/branch_1_fun/while/body/eval_jaxpr/agqk,kad->agqd/dot_general | solution.py:31
  85.3 0.2 copy.50
  85.5 1.2 multiply_reduce_fusion.1
  86.8 4.9 %convolution_convert_fusion.3 = bf16[256,4096]{1,0:T(8,128)(2,1)} fusion(bf16[256,512]{0,1:T(8,128)(2,1)S(1)} %bitcast.154, bf16[512,4096]{1,0:T(8,128)(2,1)} %param.26), kind=kOutput, calls=%fused_computation.48 | convolution fusion | flops 1074790400 | bytes 6553600 | tf_op jit(solution)/shard_map/dot_general | solution.py:188
  91.7 0.1 copy.42
  91.8 0.1 eq.43
  91.9 0.1 eq.39
  92.0 0.6 reduce-window.6
  92.6 0.2 slice_reduce_fusion
  92.9 0.1 fusion.69
  93.0 0.1 sub.77
  93.1 0.1 copy.45
  93.2 0.1 fusion.56
  93.3 30.8 %reduce-scatter.3.cloned.1.call-done = bf16[64,4096]{1,0:T(8,128)(2,1)} async-done(((bf16[256,4096]{1,0:T(8,128)(2,1)}), bf16[64,4096]{1,0:T(8,128)(2,1)}) %reduce-scatter.3.cloned.1.call-update) | async-done | bytes 524304 | tf_op jit(solution)/shard_map/reduce_scatter | solution.py:187
  124.1 1.2 add_convert_fusion
  125.3 0.2 fusion.46
  125.5 0.6 copy-done.3
  126.1 0.2 fusion.48
  126.3 2.7 convolution_convert_fusion
  129.0 5.7 %all-to-all-start = ((bf16[8,48,4096]{2,1,0:T(8,128)(2,1)}), bf16[8,48,4096]{2,1,0:T(8,128)(2,1)}, u32[]{:S(2)}, u32[]{:S(2)}) async-start(bf16[8,48,4096]{2,1,0:T(8,128)(2,1)} %bitcast.153), calls=%async_computation.1 | async-start | bytes 6291456 | tf_op jit(solution)/shard_map/all_to_all | solution.py:123
  134.6 0.2 all-gather.5.cloned.1.call-start
  134.8 0.5 all-gather.5.cloned.1.call-update
  135.4 69.9 %all-to-all-done = bf16[8,48,4096]{2,1,0:T(8,128)(2,1)} async-done(((bf16[8,48,4096]{2,1,0:T(8,128)(2,1)}), bf16[8,48,4096]{2,1,0:T(8,128)(2,1)}, u32[]{:S(2)}, u32[]{:S(2)}) %all-to-all-start) | async-done | bytes 3145760 | tf_op jit(solution)/shard_map/all_to_all | solution.py:123
  205.3 2.9 convolution_bitcast_fusion.1
  208.1 7.3 %convolution_convert_fusion.1 = bf16[8,48,4096]{2,1,0:T(8,128)(2,1)} fusion(bf16[1,128,4096]{2,1,0:T(8,128)(2,1)S(1)} %copy-done, bf16[8,48,4096]{2,1,0:T(8,128)(2,1)} %all-to-all-done, bf16[1,4096,128]{2,1,0:T(8,128)(2,1)} %param.31, f32[8,1,48,128]{3,2,0,1:T(8,128)S(1)} %convolution_bitcast_fusion.1), kind=kOutput, calls=%fused_computation.46 | convolution fusion | flops 807174144 | bytes 8585216 | tf_op jit(solution)/shard_map/sjcf,jfd->sjcd/dot_general | solution.py:129
  215.4 4.4 %all-to-all-start.1 = ((bf16[8,48,4096]{2,1,0:T(8,128)(2,1)}), bf16[8,48,4096]{2,1,0:T(8,128)(2,1)}, u32[]{:S(2)}, u32[]{:S(2)}) async-start(bf16[8,48,4096]{2,1,0:T(8,128)(2,1)} %convolution_convert_fusion.1), calls=%async_computation.2 | async-start | bytes 6291456 | tf_op jit(solution)/shard_map/all_to_all | solution.py:132
  219.9 0.0 reduce-scatter.5.cloned.1.call-start
  219.9 2.7 fusion.74
  222.7 4.2 %convolution_convert_fusion.2 = bf16[256,4096]{1,0:T(8,128)(2,1)} fusion(bf16[128,4096]{1,0:T(8,128)(2,1)} %param.35, bf16[256,4096]{1,0:T(8,128)(2,1)S(1)} %copy-done.2, bf16[4096,128]{1,0:T(8,128)(2,1)} %param.34, f32[256,128]{1,0:T(8,128)S(1)} %fusion.74), kind=kOutput, calls=%fused_computation.47 | convolution fusion | flops 538116096 | bytes 6422528 | tf_op jit(solution)/shard_map/dot_general | solution.py:98
  226.9 0.1 mul.180
  227.0 0.1 copy.46
  227.1 62.9 %all-to-all-done.1 = bf16[8,48,4096]{2,1,0:T(8,128)(2,1)} async-done(((bf16[8,48,4096]{2,1,0:T(8,128)(2,1)}), bf16[8,48,4096]{2,1,0:T(8,128)(2,1)}, u32[]{:S(2)}, u32[]{:S(2)}) %all-to-all-start.1) | async-done | bytes 3145760 | tf_op jit(solution)/shard_map/all_to_all | solution.py:132
  290.0 6.2 %gather_fusion = bf16[256,4096]{1,0:T(8,128)(2,1)S(1)} fusion(bf16[384,4096]{1,0:T(8,128)(2,1)} %bitcast.35, s32[1024]{0:T(1024)S(1)} %pad_clamp_fusion), kind=kCustom, calls=%fused_computation | custom fusion | bytes 4195328 | tf_op jit(solution)/shard_map/gather | solution.py:136
  296.2 3.0 reshape.284
  299.3 5.3 %multiply_reduce_fusion = f32[64,4096]{1,0:T(8,128)S(1)} fusion(f32[64,4,4096]{2,1,0:T(4,128)} %reshape.284, f32[64,4]{1,0:T(8,128)S(1)} %copy.46), kind=kLoop, calls=%fused_computation.49 | loop fusion | flops 1835008 | bytes 5243904 | tf_op jit(solution)/shard_map/reduce_sum | solution.py:140
  304.7 2.0 fusion.50
  (47 shorter events, 0.3 us)
Async XLA Ops:
  6.5 201.6 %copy-start = (bf16[1,128,4096]{2,1,0:T(8,128)(2,1)S(1)}, bf16[1,128,4096]{2,1,0:T(8,128)(2,1)}, u32[]{:S(2)}) copy-start(bf16[1,128,4096]{2,1,0:T(8,128)(2,1)} %param.32) | copy-start | bytes 3145732
  6.5 66.5 %all-gather.3.cloned.1.call-start = ((), (), s32[]{:S(2)}) async-start(), calls=%async_computation.4 | async-start | bytes 1179648 | tf_op jit(solution)/shard_map/all_gather | solution.py:182
  7.3 116.8 %reduce-scatter.3.cloned.1.call-start = ((), (), s32[]{:S(2)}) async-start(), calls=%async_computation.5 | async-start | bytes 2621440 | tf_op jit(solution)/shard_map/reduce_scatter | solution.py:187
  73.1 12.4 %copy-start.12 = (f32[2]{0:T(128)S(1)}, f32[2]{0:T(128)}, u32[]{:S(2)}) copy-start(f32[2]{0:T(128)} %param.25) | copy-start | bytes 28
  73.1 2.0 copy-start.8
  75.1 1.9 copy-start.1
  77.0 2.1 copy-start.13
  86.8 4.9 %copy-start.10 = (s32[64,4]{0,1:T(4,128)S(1)}, s32[64,4]{0,1:T(4,128)}, u32[]{:S(2)}) copy-start(s32[64,4]{0,1:T(4,128)} %param.28) | copy-start | bytes 3076
  86.8 37.3 %copy-start.7 = (bf16[64,4096]{1,0:T(8,128)(2,1)S(1)}, bf16[64,4096]{1,0:T(8,128)(2,1)}, u32[]{:S(2)}) copy-start(bf16[64,4096]{1,0:T(8,128)(2,1)} %param.19) | copy-start | bytes 1572868
  86.8 39.3 %copy-start.9 = (f32[4096]{0:T(1024)S(1)}, f32[4096]{0:T(1024)}, u32[]{:S(2)}) copy-start(f32[4096]{0:T(1024)} %param.27) | copy-start | bytes 49156
  125.3 0.8 copy-start.3
  126.3 2.7 copy-start.5
  129.0 76.3 %copy-start.6 = (bf16[1,4096,128]{2,1,0:T(8,128)(2,1)S(1)}, bf16[1,4096,128]{2,1,0:T(8,128)(2,1)}, u32[]{:S(2)}) copy-start(bf16[1,4096,128]{2,1,0:T(8,128)(2,1)} %param.30) | copy-start | bytes 3145732
  129.0 76.3 %all-to-all-start = ((bf16[8,48,4096]{2,1,0:T(8,128)(2,1)}), bf16[8,48,4096]{2,1,0:T(8,128)(2,1)}, u32[]{:S(2)}, u32[]{:S(2)}) async-start(bf16[8,48,4096]{2,1,0:T(8,128)(2,1)} %bitcast.153), calls=%async_computation.1 | async-start | bytes 6291456 | tf_op jit(solution)/shard_map/all_to_all | solution.py:123
  134.6 85.3 %all-gather.5.cloned.1.call-start = ((), (), s32[]{:S(2)}) async-start(), calls=%async_computation.6 | async-start | bytes 2621440 | tf_op jit(solution)/shard_map/all_gather | solution.py:94
  215.4 74.6 %all-to-all-start.1 = ((bf16[8,48,4096]{2,1,0:T(8,128)(2,1)}), bf16[8,48,4096]{2,1,0:T(8,128)(2,1)}, u32[]{:S(2)}, u32[]{:S(2)}) async-start(bf16[8,48,4096]{2,1,0:T(8,128)(2,1)} %convolution_convert_fusion.1), calls=%async_computation.2 | async-start | bytes 6291456 | tf_op jit(solution)/shard_map/all_to_all | solution.py:132
  219.9 84.8 %reduce-scatter.5.cloned.1.call-start = ((), (), s32[]{:S(2)}) async-start(), calls=%async_computation.7 | async-start | bytes 2621440 | tf_op jit(solution)/shard_map/reduce_scatter | solution.py:99
  219.9 2.7 copy-start.2
  222.7 4.4 %copy-start.11 = (f32[64,4]{0,1:T(4,128)S(1)}, f32[64,4]{0,1:T(4,128)}, u32[]{:S(2)}) copy-start(f32[64,4]{0,1:T(4,128)} %param.29) | copy-start | bytes 3076
  299.3 5.4 %copy-start.4 = (bf16[64,4096]{1,0:T(8,128)(2,1)S(1)}, bf16[64,4096]{1,0:T(8,128)(2,1)}, u32[]{:S(2)}) copy-start(bf16[64,4096]{1,0:T(8,128)(2,1)} %copy-done.3) | copy-start | bytes 1572868
Sparse Core Ops, SparseCore 0:
  9.5 45.9 all-gather.2
  91.8 32.2 reduce-scatter.2
  137.0 23.0 all-gather.4
  227.0 31.4 reduce-scatter.4
where the time goes:
time: 314 us; the launch traced here: 313 us
  waiting for transfers between devices  165 us (53%)
  blocking collectives  65.8 us (21%)
  matrix products  32.8 us (10%)
  other arithmetic  13.5 us (4%)
  between operations  13.4 us (4%)
  local copies, waits for them, and re-layouts  12.3 us (4%)
  starting transfers between devices  10.4 us (3%)
    all_to_all x1, waiting for transfers between devices, routed_part(): lax.all_to_all(outgoing, 'sp', split_axis=0, concat_axis=0, tiled=True)  69.9 us
    all_to_all x1, waiting for transfers between devices, routed_part(): lax.all_to_all(result.reshape(arrived.shape), 'sp', split_axis=0, concat_...  62.9 us
    all_gather x1, blocking collectives, local(): lax.all_gather(k_first, 'sp', axis=0, tiled=True)  33.8 us
    all_gather x1, blocking collectives, local(): lax.all_gather(k_second, 'sp', axis=0, tiled=True)  32 us
    reduce_scatter x1, waiting for transfers between devices, local(): lax.psum_scatter(jnp.dot(attn_rows, w_out, preferred_element_type=jnp.flo...  30.8 us
    dot_general x1, matrix products, routed_part(): jnp.einsum('sjcf,jfd->sjcd', hidden, w_down, preferred_element_type=jnp.f...  7.26 us
  transfers between devices with their start and end apart: 6, of which 3 were waited for; matrix products, arithmetic and copies ran while one was open for 11% of the time, Pallas kernels for 0%

commit v1 on v0

--- a/solution.py
+++ b/solution.py
@@ -3,9 +3,12 @@
 import jax
 import jax.numpy as jnp
 from jax import lax
+from jax.experimental import pallas as pl
+from jax.experimental.pallas import tpu as pltpu
 from jax.sharding import PartitionSpec as P
 
 HEAD = 128
+TURNS = (0, 2, 1, 3)
 
 
 FLOOR = -1e30
@@ -140,7 +143,7 @@
     return jnp.sum(picked * route_w[..., None], axis=1)
 
 
-def local(
+def slow_local(
     stream_in,
     q_first,
     q_second,
@@ -200,6 +203,678 @@
     return (stream + routed + shared).astype(jnp.bfloat16)
 
 
+VMEM = pltpu.MemorySpace.VMEM
+MIB = 1024 * 1024
+SMEM = pltpu.MemorySpace.SMEM
+HBM = pltpu.MemorySpace.HBM
+
+
+def ring_order(count):
+    return list(range(0, count, 2)) + list(range(count - 1, 0, -2))
+
+
+def ring_pairs(count):
+    order = ring_order(count)
+    forward = [(order[i], order[(i + 1) % count]) for i in range(count)]
+    return forward, [(b, a) for a, b in forward]
+
+
+def ring_sources(count):
+    order = ring_order(count)
+    rows = [None] * count
+    for place, index in enumerate(order):
+        row = [index]
+        for step in range(1, count // 2):
+            row += [order[(place - step) % count], order[(place + step) % count]]
+        row.append(order[(place + count // 2) % count])
+        rows[index] = row
+    return rows
+
+
+def dot_nt(a, b):
+    return lax.dot_general(a, b, (((1,), (1,)), ((), ())), preferred_element_type=jnp.float32)
+
+
+def grouped(copies):
+    for copy in copies:
+        copy.start()
+    return copies
+
+
+def attn_kernel(spans, first, last, scale, own_rows, *refs):
+    refs = list(refs)
+    ids_ref = refs.pop(0)
+    if last:
+        lam_ref = refs.pop(0)
+    q_in = [refs.pop(0), refs.pop(0)]
+    kv_in = [refs.pop(0) for _ in spans]
+    if not first:
+        state_in = [refs.pop(0) for _ in range(3)]
+    if last:
+        w_ref, stream_ref = refs.pop(0), refs.pop(0)
+        own_ref, send_ref, m_ref, l_ref, acc_ref, mixed_ref, w, stream, w_sem = refs[:9]
+        del refs[:9]
+        load = pltpu.make_async_copy(w_ref, w, w_sem.at[0])
+        feed = pltpu.make_async_copy(stream_ref, stream, w_sem.at[1])
+    elif first:
+        q_refs = [refs.pop(0), refs.pop(0)]
+        m_ref, l_ref, acc_ref = refs.pop(0), refs.pop(0), refs.pop(0)
+    else:
+        m_ref, l_ref, acc_ref = refs.pop(0), refs.pop(0), refs.pop(0)
+    kv_scratch, sem = refs
+    rows = q_in[0].shape[0]
+    heads = q_in[0].shape[1] // HEAD
+    parts = rows // own_rows
+    me, mine = ids_ref[0], ids_ref[1]
+    outs = (m_ref, l_ref, acc_ref)
+    starts = [sum(b.shape[0] for b in kv_in[:at]) for at in range(len(spans))]
+    kv_refs = [
+        kv_scratch.at[pl.ds(start, ref.shape[0])] for start, ref in zip(starts, kv_in)
+    ]
+    copies = grouped(
+        [
+            pltpu.make_async_copy(source, into, sem.at[at])
+            for at, (source, into) in enumerate(zip(kv_in, kv_refs))
+        ]
+    )
+    if last:
+        load.start()
+        feed.start()
+    if first:
+        loads = grouped(
+            [
+                pltpu.make_async_copy(
+                    q_in[which].at[
+                        pl.ds(pl.multiple_of((mine ^ turn) * own_rows, own_rows), own_rows)
+                    ],
+                    q_refs[which].at[pl.ds(index * own_rows, own_rows)],
+                    sem.at[len(spans) + which * parts + index],
+                )
+                for which in range(2)
+                for index, turn in enumerate(TURNS)
+            ]
+        )
+        for copy in loads:
+            copy.wait()
+    else:
+        q_refs = q_in
+
+    def fold(kv_ref, diagonal, old_refs=outs):
+        keys = kv_ref.shape[0]
+        v = kv_ref[:, 2 * HEAD :]
+        old_m, old_l, old_acc = old_refs
+        if diagonal:
+            row_at = lax.broadcasted_iota(jnp.int32, (rows, keys), 0)
+            key_at = lax.broadcasted_iota(jnp.int32, (rows, keys), 1)
+            part = row_at // own_rows
+            place = jnp.zeros_like(part)
+            for index, turn in enumerate(TURNS):
+                place = jnp.where(part == index, mine ^ turn, place)
+            allowed = key_at <= place * own_rows + row_at % own_rows
+        for head in range(heads):
+            for which in range(2):
+                pair = 2 * head + which
+                q = q_refs[which][:, head * HEAD : (head + 1) * HEAD]
+                k = kv_ref[:, which * HEAD : (which + 1) * HEAD]
+                s = dot_nt(q, k)
+                if diagonal:
+                    s = jnp.where(allowed, s, FLOOR)
+                top = jnp.max(s, axis=1, keepdims=True)
+                if diagonal:
+                    raised = jnp.broadcast_to(top, (rows, 128))
+                else:
+                    old = old_m[pair]
+                    raised = jnp.maximum(old, top)
+                wide = jnp.concatenate([raised] * (keys // 128), axis=1)
+                p = jnp.exp((s - wide) * scale)
+                part_sum = p[:, :128]
+                for at in range(128, keys, 128):
+                    part_sum = part_sum + p[:, at : at + 128]
+                prod = jnp.dot(p.astype(jnp.bfloat16), v, preferred_element_type=jnp.float32)
+                m_ref[pair] = raised
+                if diagonal:
+                    l_ref[pair] = part_sum
+                    acc_ref[pair] = prod
+                else:
+                    fade = jnp.exp((old - raised) * scale)
+                    l_ref[pair] = old_l[pair] * fade + part_sum
+                    fades = jnp.concatenate([fade] * (prod.shape[1] // 128), axis=1)
+                    acc_ref[pair] = old_acc[pair] * fades + prod
+
+    for index, (place, pieces) in enumerate(spans):
+        copies[index].wait()
+        if pieces == 2:
+            copies[index + 1].wait()
+            kv_ref = kv_scratch.at[
+                pl.ds(starts[index], kv_in[index].shape[0] + kv_in[index + 1].shape[0])
+            ]
+        elif pieces == 0:
+            continue
+        else:
+            kv_ref = kv_refs[index]
+        if first and index == 0:
+            fold(kv_ref, True)
+            continue
+        earlier = ids_ref[2 + place] < me
+        carry = not first and index == 0
+
+        @pl.when(earlier)
+        def _(kv_ref=kv_ref, carry=carry):
+            fold(kv_ref, False, state_in if carry else outs)
+
+        if carry:
+
+            @pl.when(jnp.logical_not(earlier))
+            def _():
+                for into, source in zip(outs, state_in):
+                    into[...] = source[...]
+
+        if pieces == 2:
+            break
+
+    if last:
+        for head in range(heads):
+            terms = []
+            for which in range(2):
+                pair = 2 * head + which
+                total = jnp.sum(l_ref[pair], axis=1, keepdims=True)
+                terms.append(acc_ref[pair] / total)
+            mixed = terms[0] - lam_ref[head] * terms[1]
+            square = jnp.mean(mixed * mixed, axis=1, keepdims=True)
+            mixed = mixed * lax.rsqrt(square + 1e-05)
+            width = mixed.shape[1]
+            mixed_ref[:, head * width : (head + 1) * width] = mixed.astype(jnp.bfloat16)
+        load.wait()
+        feed.wait()
+        half = rows // 2
+        step = math.gcd(w.shape[1], 512)
+
+        def body(at, _):
+            cols = pl.ds(pl.multiple_of(at * step, step), step)
+            out = jnp.dot(mixed_ref[...], w[:, cols], preferred_element_type=jnp.float32)
+            own_ref[:own_rows, cols] = out[:own_rows] + stream[:, cols].astype(jnp.float32)
+            own_ref[own_rows:, cols] = out[own_rows:half]
+            send_ref[:, cols] = out[half:].astype(jnp.bfloat16)
+            return 0
+
+        lax.fori_loop(0, w.shape[1] // step, body, 0)
+
+
+def specs(space, count):
+    return [pl.BlockSpec(memory_space=space)] * count
+
+
+def attn_call(ids, q_first, q_second, blocks, spans, state, own_rows, lam=None, w_out=None, stream_in=None):
+    rows = q_first.shape[0]
+    heads = q_first.shape[1] // HEAD
+    value_dim = blocks[0].shape[1] - 2 * HEAD
+    first, last = state is None, w_out is not None
+    states = [
+        pltpu.VMEM((2 * heads, rows, 128), jnp.float32),
+        pltpu.VMEM((2 * heads, rows, 128), jnp.float32),
+        pltpu.VMEM((2 * heads, rows, value_dim), jnp.float32),
+    ]
+    operands = [ids] + ([lam] if last else []) + [q_first, q_second, *blocks]
+    in_specs = specs(SMEM, 2 if last else 1)
+    in_specs += specs(HBM if first else VMEM, 2) + specs(HBM, len(blocks))
+    if not first:
+        operands += list(state)
+        in_specs += specs(VMEM, 3)
+    scratch = []
+    if last:
+        operands += [w_out, stream_in]
+        in_specs += specs(HBM, 2)
+        width = w_out.shape[1]
+        out_shape = [
+            pltpu.VMEM((rows // 2, width), jnp.float32),
+            jax.ShapeDtypeStruct((rows // 2, width), jnp.bfloat16),
+        ]
+        scratch = [
+            *states,
+            pltpu.VMEM((rows, heads * value_dim), jnp.bfloat16),
+            pltpu.VMEM(w_out.shape, jnp.bfloat16),
+            pltpu.VMEM(stream_in.shape, jnp.bfloat16),
+            pltpu.SemaphoreType.DMA((2,)),
+        ]
+    else:
+        out_shape = list(states)
+        if first:
+            out_shape = [pltpu.VMEM(q_first.shape, q_first.dtype)] * 2 + out_shape
+    keys = sum(b.shape[0] for b in blocks)
+    scratch += [
+        pltpu.VMEM((keys, blocks[0].shape[1]), jnp.bfloat16),
+        pltpu.SemaphoreType.DMA((len(blocks) + 2 * rows // own_rows,)),
+    ]
+    body = lambda *refs: attn_kernel(spans, first, last, HEAD**-0.5, own_rows, *refs)
+    return pl.pallas_call(
+        body,
+        out_shape=out_shape,
+        in_specs=in_specs,
+        out_specs=specs(VMEM, len(out_shape)),
+        scratch_shapes=scratch,
+        cost_estimate=pl.CostEstimate(
+            flops=8 * heads * rows * keys * (HEAD + value_dim),
+            bytes_accessed=4 * 1024 * 1024,
+            transcendentals=2 * heads * rows * keys,
+        ),
+        compiler_params=pltpu.CompilerParams(vmem_limit_bytes=(22 if last else 12) * MIB),
+    )(*operands)
+
+
+def pack_kernel(one_ref, two_ref, three_ref, out_ref, sem):
+    wide = one_ref.shape[1]
+    cuts = ((0, wide), (wide, wide), (2 * wide, three_ref.shape[1]))
+    copies = grouped(
+        [
+            pltpu.make_async_copy(ref, out_ref.at[:, pl.ds(start, size)], sem.at[at])
+            for at, (ref, (start, size)) in enumerate(zip((one_ref, two_ref, three_ref), cuts))
+        ]
+    )
+    for copy in copies:
+        copy.wait()
+
+
+def pack_call(one, two, three):
+    width = one.shape[1] + two.shape[1] + three.shape[1]
+    return pl.pallas_call(
+        pack_kernel,
+        out_shape=jax.ShapeDtypeStruct((one.shape[0], width), one.dtype),
+        in_specs=specs(HBM, 3),
+        out_specs=pl.BlockSpec(memory_space=VMEM),
+        scratch_shapes=[pltpu.SemaphoreType.DMA((3,))],
+        name="pack",
+    )(one, two, three)
+
+
+def slices_kernel(unit, ids_ref, gate_ref, up_ref, down_ref, gate_out, rest_out, gate, up, turned, sem):
+    start = pl.multiple_of(ids_ref[1] * unit, unit)
+    loads = grouped(
+        [
+            pltpu.make_async_copy(gate_ref, gate, sem.at[0]),
+            pltpu.make_async_copy(up_ref, up, sem.at[1]),
+            pltpu.make_async_copy(
+                down_ref.at[pl.ds(start, unit)], rest_out.at[pl.ds(unit, unit)], sem.at[2]
+            ),
+        ]
+    )
+    loads[0].wait()
+    turned[...] = gate[...].T
+    gate_out[...] = turned[pl.ds(start, unit)]
+    loads[1].wait()
+    turned[...] = up[...].T
+    rest_out[:unit] = turned[pl.ds(start, unit)]
+    loads[2].wait()
+
+
+def slices_call(ids, gate, up, down, unit):
+    width = gate.shape[0]
+    return pl.pallas_call(
+        lambda *refs: slices_kernel(unit, *refs),
+        out_shape=[
+            jax.ShapeDtypeStruct((unit, width), gate.dtype),
+            jax.ShapeDtypeStruct((2 * unit, width), gate.dtype),
+        ],
+        in_specs=specs(SMEM, 1) + specs(HBM, 3),
+        out_specs=specs(VMEM, 2),
+        scratch_shapes=[
+            pltpu.VMEM(gate.shape, gate.dtype),
+            pltpu.VMEM(up.shape, gate.dtype),
+            pltpu.VMEM((gate.shape[1], width), gate.dtype),
+            pltpu.SemaphoreType.DMA((3,)),
+        ],
+        name="slices",
+    )(ids, gate, up, down)
+
+
+def silu(v):
+    return v / (1.0 + jnp.exp(-v))
+
+
+def stack_kernel(unit, gates_count, rests_count, *refs):
+    refs = list(refs)
+    gates = [refs.pop(0) for _ in range(gates_count)]
+    rests = [refs.pop(0) for _ in range(rests_count)]
+    sg_ref, su_ref, sd_ref, gate_out, up_out, down_out, sg_out, su_out, sem = refs
+    moves = [(sg_ref, sg_out), (su_ref, su_out)]
+    at = 0
+    for ref in gates:
+        moves.append((ref, gate_out.at[pl.ds(at, ref.shape[0])]))
+        at += ref.shape[0]
+    for index, ref in enumerate(rests):
+        moves.append((ref.at[pl.ds(0, unit)], up_out.at[pl.ds(index * unit, unit)]))
+        moves.append((ref.at[pl.ds(unit, unit)], down_out.at[pl.ds(index * unit, unit)]))
+    moves.append((sd_ref, down_out.at[pl.ds(rests_count * unit, sd_ref.shape[0])]))
+    copies = grouped(
+        [pltpu.make_async_copy(a, b, sem.at[k]) for k, (a, b) in enumerate(moves)]
+    )
+    for copy in copies:
+        copy.wait()
+
+
+def stack_call(gates, rests, s_gate, s_up, s_down):
+    unit = rests[0].shape[0] // 2
+    width = rests[0].shape[1]
+    operands = [*gates, *rests, s_gate, s_up, s_down]
+    total = sum(g.shape[0] for g in gates)
+    most = len(rests) * unit
+    return pl.pallas_call(
+        lambda *refs: stack_kernel(unit, len(gates), len(rests), *refs),
+        out_shape=[
+            pltpu.VMEM((total, width), jnp.bfloat16),
+            pltpu.VMEM((most, width), jnp.bfloat16),
+            pltpu.VMEM((most + s_down.shape[0], width), jnp.bfloat16),
+            pltpu.VMEM(s_gate.shape, jnp.bfloat16),
+            pltpu.VMEM(s_up.shape, jnp.bfloat16),
+        ],
+        in_specs=specs(HBM, len(operands)),
+        out_specs=specs(VMEM, 5),
+        scratch_shapes=[pltpu.SemaphoreType.DMA((len(gates) + 2 * len(rests) + 3,))],
+        cost_estimate=pl.CostEstimate(flops=10**9, bytes_accessed=16 * MIB, transcendentals=0),
+        compiler_params=pltpu.CompilerParams(vmem_limit_bytes=2 * MIB),
+        name="stack",
+    )(*operands)
+
+
+def spread(ids_ref, combine, first, count, unit):
+    expert = lax.broadcasted_iota(jnp.int32, combine.shape, 1)
+    columns = []
+    for block in range(first, first + count):
+        picked = jnp.where(expert == ids_ref[2 + block], combine, 0.0)
+        column = jnp.sum(picked, axis=1, keepdims=True)
+        columns.append(jnp.broadcast_to(column, (combine.shape[0], unit)))
+    return jnp.concatenate(columns, axis=1)
+
+
+def most_kernel(count, unit, ids_ref, one_ref, two_ref, near_ref, far_ref, *refs):
+    refs = list(refs)
+    late = [refs.pop(0) for _ in range(count)]
+    gate_ref, up_ref, down_ref, sg_ref, su_ref, out_ref, x_ref, late_ref, hidden_ref, sem = refs
+    half = one_ref.shape[0]
+    moves = [(one_ref, x_ref.at[pl.ds(0, half)]), (two_ref, x_ref.at[pl.ds(half, half)])]
+    moves += [
+        (ref, late_ref.at[pl.ds(2 * unit * index, 2 * unit)]) for index, ref in enumerate(late)
+    ]
+    copies = grouped(
+        [pltpu.make_async_copy(a, b, sem.at[k]) for k, (a, b) in enumerate(moves)]
+    )
+    copies[0].wait()
+    copies[1].wait()
+    x = x_ref[...]
+    begun = up_ref.shape[0]
+    used = begun + count * unit
+    gate = dot_nt(x, gate_ref[:used])
+    for copy in copies[2:]:
+        copy.wait()
+    ups = [late_ref[2 * unit * index : 2 * unit * index + unit] for index in range(count)]
+    up = dot_nt(x, jnp.concatenate([up_ref[...]] + ups, axis=0))
+    combine = jnp.concatenate([near_ref[...], far_ref[...]], axis=0)
+    scale = spread(ids_ref, combine, 0, used // unit, unit)
+    hidden = (silu(gate) * up * scale).astype(jnp.bfloat16)
+    gate = jnp.dot(x, sg_ref[...], preferred_element_type=jnp.float32)
+    up = jnp.dot(x, su_ref[...], preferred_element_type=jnp.float32)
+    shared = (silu(gate) * up).astype(jnp.bfloat16)
+    hidden_ref[:, :begun] = hidden[:, :begun]
+    hidden_ref[:, begun : begun + shared.shape[1]] = shared
+    hidden_ref[:, begun + shared.shape[1] :] = hidden[:, begun:]
+    width = out_ref.shape[1]
+    step = math.gcd(width, 512)
+
+    def body(at, _):
+        cols = pl.ds(pl.multiple_of(at * step, step), step)
+        downs = [
+            late_ref[2 * unit * index + unit : 2 * unit * (index + 1), cols]
+            for index in range(count)
+        ]
+        down = jnp.concatenate([down_ref[:, cols]] + downs, axis=0)
+        out_ref[:, cols] = jnp.dot(hidden_ref[...], down, preferred_element_type=jnp.float32)
+        return 0
+
+    lax.fori_loop(0, width // step, body, 0)
+
+
+def most_call(ids, own, other, combine, late, stacked):
+    unit = late[0].shape[0] // 2
+    half, width = own.shape
+    hidden = stacked[2].shape[0] + len(late) * unit
+    operands = [ids, own, other, *combine, *late, *stacked]
+    return pl.pallas_call(
+        lambda *refs: most_kernel(len(late), unit, *refs),
+        out_shape=pltpu.VMEM((2 * half, width), jnp.float32),
+        in_specs=specs(SMEM, 1)
+        + specs(HBM, 2)
+        + specs(VMEM, 2)
+        + specs(HBM, len(late))
+        + specs(VMEM, 5),
+        out_specs=pl.BlockSpec(memory_space=VMEM),
+        scratch_shapes=[
+            pltpu.VMEM((2 * half, width), jnp.bfloat16),
+            pltpu.VMEM((2 * unit * len(late), width), jnp.bfloat16),
+            pltpu.VMEM((2 * half, hidden), jnp.bfloat16),
+            pltpu.SemaphoreType.DMA((2 + len(late),)),
+        ],
+        cost_estimate=pl.CostEstimate(
+            flops=2 * 2 * half * width * 3 * hidden,
+            bytes_accessed=16 * MIB,
+            transcendentals=2 * half * hidden,
+        ),
+        compiler_params=pltpu.CompilerParams(vmem_limit_bytes=14 * MIB),
+        name="experts_most",
+    )(*operands)
+
+
+def rest_kernel(unit, ids_ref, one_ref, two_ref, near_ref, far_ref, gate_ref, up_ref, down_ref, most_ref, own_ref, send_ref, x_ref, both_ref, d_ref, sem):
+    half = one_ref.shape[0]
+    copies = grouped(
+        [
+            pltpu.make_async_copy(one_ref, x_ref.at[pl.ds(0, half)], sem.at[0]),
+            pltpu.make_async_copy(two_ref, x_ref.at[pl.ds(half, half)], sem.at[1]),
+            pltpu.make_async_copy(up_ref, both_ref.at[pl.ds(unit, unit)], sem.at[2]),
+            pltpu.make_async_copy(down_ref, d_ref, sem.at[3]),
+        ]
+    )
+    used = gate_ref.shape[0] - unit
+    both_ref[:unit] = gate_ref[used:]
+    for copy in copies[:3]:
+        copy.wait()
+    both = dot_nt(x_ref[...], both_ref[...])
+    gate, up = both[:, :unit], both[:, unit:]
+    combine = jnp.concatenate([near_ref[...], far_ref[...]], axis=0)
+    scale = spread(ids_ref, combine, used // unit, 1, unit)
+    hidden = (silu(gate) * up * scale).astype(jnp.bfloat16)
+    copies[3].wait()
+    width = most_ref.shape[1]
+    step = math.gcd(width, 512)
+
+    def body(at, _):
+        cols = pl.ds(pl.multiple_of(at * step, step), step)
+        out = most_ref[:, cols] + jnp.dot(
+            hidden, d_ref[:, cols], preferred_element_type=jnp.float32
+        )
+        own_ref[:, cols] = out[:half]
+        send_ref[:, cols] = out[half:].astype(jnp.bfloat16)
+        return 0
+
+    lax.fori_loop(0, width // step, body, 0)
+
+
+def rest_call(ids, own, other, combine, gate, up, down, most):
+    unit = up.shape[0]
+    half, width = own.shape
+    return pl.pallas_call(
+        lambda *refs: rest_kernel(unit, *refs),
+        out_shape=[
+            pltpu.VMEM((half, width), jnp.float32),
+            jax.ShapeDtypeStruct((half, width), jnp.bfloat16),
+        ],
+        in_specs=specs(SMEM, 1)
+        + specs(HBM, 2)
+        + specs(VMEM, 3)
+        + specs(HBM, 2)
+        + specs(VMEM, 1),
+        out_specs=specs(VMEM, 2),
+        scratch_shapes=[
+            pltpu.VMEM((2 * half, width), jnp.bfloat16),
+            pltpu.VMEM((2 * unit, width), jnp.bfloat16),
+            pltpu.VMEM((unit, width), jnp.bfloat16),
+            pltpu.SemaphoreType.DMA((4,)),
+        ],
+        cost_estimate=pl.CostEstimate(
+            flops=2 * 2 * half * width * 3 * unit,
+            bytes_accessed=10 * MIB,
+            transcendentals=2 * half * unit,
+        ),
+        compiler_params=pltpu.CompilerParams(vmem_limit_bytes=10 * MIB),
+        name="experts_rest",
+    )(ids, own, other, *combine, gate, up, down, most)
+
+
+def norm_rows(resid, gain):
+    stream = resid.astype(jnp.float32)
+    return (
+        stream * lax.rsqrt(jnp.mean(stream * stream, axis=-1, keepdims=True) + 1e-06) * gain
+    ).astype(jnp.bfloat16)
+
+
+def ring_step(ahead, back, pairs):
+    ahead = lax.ppermute(ahead, "sp", pairs[0])
+    back = lax.ppermute(back, "sp", pairs[1])
+    return ahead, back
+
+
+def ring_gather(block, count):
+    pairs = ring_pairs(count)
+    out = [block]
+    ahead = back = block
+    for _ in range(1, count // 2):
+        ahead, back = ring_step(ahead, back, pairs)
+        out += [ahead, back]
+    half = block.shape[0] // 2
+    low, high = ring_step(ahead[:half], back[half:], pairs)
+    return out, low, high
+
+
+def swap(rows, pairs):
+    return lax.ppermute(rows, "tp", pairs)
+
+
+def fast_local(
+    stream_in,
+    q_first,
+    q_second,
+    k_first,
+    k_second,
+    values,
+    head_lambda,
+    w_out,
+    norm_gain,
+    routes,
+    route_w,
+    w_gate,
+    w_up,
+    w_down,
+    s_gate,
+    s_up,
+    s_down,
+):
+    count = lax.axis_size("sp")
+    members = lax.axis_size("tp")
+    me = lax.axis_index("sp")
+    mine = lax.axis_index("tp")
+    seq_rows = q_first.shape[0]
+    own_rows = seq_rows // members
+    experts = w_gate.shape[0] * count
+    unit = w_gate.shape[2] // members
+    cores = [(t, t ^ 1) for t in range(members)]
+    sides = [(t, t ^ 2) for t in range(members)]
+
+    sources = jnp.asarray(ring_sources(count), jnp.int32)[me]
+    ids = jnp.concatenate([jnp.stack([me, mine]).astype(jnp.int32), sources])
+    kv = pack_call(k_first, k_second, values)
+    blocks, low, high = ring_gather(kv, count)
+    gate, rest = slices_call(ids, w_gate[0], w_up[0], w_down[0], unit)
+    gates, gate_low, gate_high = ring_gather(gate, count)
+    rests, rest_up, rest_down = ring_gather(rest, count)
+
+    queries = (q_first, q_second)
+    state = None
+    for step in range(1, count // 2):
+        begin, end = (0 if step == 1 else 2 * step - 1), 2 * step + 1
+        spans = tuple((place, 1) for place in range(begin, end))
+        result = attn_call(ids, *queries, blocks[begin:end], spans, state, own_rows)
+        if step == 1:
+            queries = result[:2]
+        state = result[-3:]
+    own, send = attn_call(
+        ids,
+        *queries,
+        [low, high],
+        ((count - 1, 2), (count - 1, 0)),
+        state,
+        own_rows,
+        head_lambda,
+        w_out,
+        stream_in,
+    )
+
+    combine = jnp.sum(
+        jnp.where(
+            routes[:, :, None] == jnp.arange(experts, dtype=jnp.int32)[None, None, :],
+            route_w[:, :, None],
+            0.0,
+        ),
+        axis=1,
+    )
+    across = swap(combine, sides)
+    paired = jnp.concatenate([combine, across])
+    combine = (paired, swap(paired, cores))
+
+    met = swap(send, cores)
+    pair = (own + met.astype(jnp.float32)).astype(jnp.bfloat16)
+    met = swap(pair, sides)
+    stacked = stack_call([*gates, gate_low, gate_high], rests[:5], s_gate, s_up, s_down)
+    resid = (
+        pair.astype(jnp.float32)
+        + jnp.concatenate([met[own_rows:], met[:own_rows]]).astype(jnp.float32)
+    ).astype(jnp.bfloat16)
+    resid = lax.optimization_barrier(resid)
+    normed = norm_rows(resid, norm_gain)
+    other = swap(normed, cores)
+    most = most_call(ids, normed, other, combine, rests[5:], stacked)
+    own, send = rest_call(
+        ids, normed, other, combine, stacked[0], rest_up, rest_down, most
+    )
+    met = swap(send, cores)
+    terms = own + met.astype(jnp.float32)
+    met = swap(terms[own_rows:].astype(jnp.bfloat16), sides)
+    return (
+        resid[:own_rows].astype(jnp.float32) + terms[:own_rows] + met.astype(jnp.float32)
+    ).astype(jnp.bfloat16)
+
+
+def weights_travel(count, members, seq_rows, k_first, values, w_gate):
+    unit = w_gate.shape[2] // members
+    gathered = 3 * count * unit * w_gate.shape[1] * 2
+    return (
+        members == 4
+        and count >= 4
+        and count % 2 == 0
+        and w_gate.shape[0] == 1
+        and k_first.shape[1] == HEAD
+        and values.shape[1] % 128 == 0
+        and w_gate.shape[2] % (32 * members) == 0
+        and seq_rows % (32 * members) == 0
+        and count == 8
+        and gathered <= 16 * 1024 * 1024
+    )
+
+
+def local(*args):
+    count, members = lax.axis_size("sp"), lax.axis_size("tp")
+    if weights_travel(count, members, args[1].shape[0], args[3], args[5], args[11]):
+        return fast_local(*args)
+    return slow_local(*args)
+
+
 def solution(mesh):
     return jax.shard_map(
         local,

time: 314 us -> 154 us (0.49)
  waiting for transfers between devices: 165 us -> 75.8 us
  blocking collectives: 65.8 us -> 0 us
  matrix products: 32.8 us -> 0 us
  Pallas kernels: 0 us -> 24.6 us
  starting transfers between devices: 10.4 us -> 30.2 us
  between operations: 13.4 us -> 0.39 us
  other arithmetic: 13.5 us -> 2.48 us
  local copies, waits for them, and re-layouts: 12.3 us -> 20.1 us
    all_to_all x2 -> x0, waiting for transfers between devices: 133 us -> none  [the longest x1 69.9 us: routed_part(): lax.all_to_all(outgoing, 'sp', split_axis=0, concat_axis=0, tiled=True)]
    ppermute x0 -> x31, waiting for transfers between devices: none -> 75.8 us  [the longest x12 49.2 us: ring_step(): ahead = lax.ppermute(ahead, 'sp', pairs[0])]
    all_gather x2 -> x0, blocking collectives: 65.8 us -> none  [the longest x1 33.8 us: local(): lax.all_gather(k_first, 'sp', axis=0, tiled=True)]
    dot_general x10 -> x0, matrix products: 32.8 us -> none  [the longest x1 7.26 us: routed_part(): jnp.einsum('sjcf,jfd->sjcd', hidden, w_down, preferred_element_type=jnp.f...]
    reduce_scatter x2 -> x0, waiting for transfers between devices: 30.8 us -> none  [the longest x1 30.8 us: local(): lax.psum_scatter(jnp.dot(attn_rows, w_out, preferred_element_type=jnp.flo...]
    ppermute x0 -> x31, starting transfers between devices: none -> 30.2 us  [the longest x12 20.3 us: ring_step(): ahead = lax.ppermute(ahead, 'sp', pairs[0])]
    pallas_call x0 -> x9, Pallas kernels: none -> 24.6 us  [the longest x4 7.6 us: attn_call(): pl.pallas_call(body, out_shape=out_shape, in_specs=in_specs, out_specs=sp...]
    unnamed x24 -> x66, local copies, waits for them, and re-layouts: 0.81 us -> 17.8 us
  transfers between devices with their start and end apart: 6 -> 31, of which waited for: 3 -> 18; matrix products, arithmetic and copies ran while one was open for 11% -> 2% of each run, Pallas kernels for 0% -> 10%
where the time goes in v1:
time: 154 us
  waiting for transfers between devices  75.8 us (49%)
  starting transfers between devices  30.2 us (20%)
  Pallas kernels  24.6 us (16%)
  local copies, waits for them, and re-layouts  20.1 us (13%)
  other arithmetic  2.48 us (2%)
    ppermute x12, waiting for transfers between devices, ring_step(): ahead = lax.ppermute(ahead, 'sp', pairs[0])  49.2 us
    ppermute x7, waiting for transfers between devices, swap(): return lax.ppermute(rows, 'tp', pairs)  22.2 us
    ppermute x12, starting transfers between devices, ring_step(): ahead = lax.ppermute(ahead, 'sp', pairs[0])  20.3 us
    unnamed x66, local copies, waits for them, and re-layouts  17.8 us
    pallas_call x4, Pallas kernels, attn_call(): pl.pallas_call(body, out_shape=out_shape, in_specs=in_specs, out_specs=sp...  7.6 us
    pallas_call x1, Pallas kernels, most_call(): pl.pallas_call(lambda *refs: most_kernel(len(late), unit, *refs), out_sha...  6.83 us
    ppermute x12, starting transfers between devices, ring_step(): back = lax.ppermute(back, 'sp', pairs[1])  5.82 us
    ppermute x12, waiting for transfers between devices, ring_step(): back = lax.ppermute(back, 'sp', pairs[1])  4.36 us
  transfers between devices with their start and end apart: 31, of which 18 were waited for; matrix products, arithmetic and copies ran while one was open for 2% of the time, Pallas kernels for 10%

profile of v1, /device:TPU:0, one launch (start us, length us, event | category | flops | bytes accessed | tf_op | source)
XLA Modules:
  0.0 153.6 jit_solution(4963402740373697108)
XLA Ops:
  0.0 1.7 %pack.1.refs_3_ = bf16[256,512]{1,0:T(8,128)(2,1)} custom-call(bf16[256,128]{1,0:T(8,128)(2,1)} %one_ref.1, bf16[256,128]{1,0:T(8,128)(2,1)} %two_ref.1, bf16[256,256]{1,0:T(8,128)(2,1)} %three_ref.1), custom_call_target="tpu_custom_call" | custom-call | tf_op jit(solution)/shard_map/pack/pallas_call | solution.py:479
  1.7 3.1 %collective-permute-start = (bf16[256,512]{1,0:T(8,128)(2,1)}, bf16[256,512]{1,0:T(8,128)(2,1)S(1)}, u32[]{:S(2)}, u32[]{:S(2)}) collective-permute-start(bf16[256,512]{1,0:T(8,128)(2,1)} %pack.1.refs_3_), channel_id=1, source_target_pairs={{0,8},{8,16},{16,24},{24,28},{28,20},{20,12},{12,4},{4,0},{1,9},{9... | collective-permute-start | bytes 786440 | tf_op jit(solution)/shard_map/ppermute | solution.py:739
  4.8 6.5 %collective-permute-done.refs_4_ = bf16[256,512]{1,0:T(8,128)(2,1)S(1)} collective-permute-done((bf16[256,512]{1,0:T(8,128)(2,1)}, bf16[256,512]{1,0:T(8,128)(2,1)S(1)}, u32[]{:S(2)}, u32[]{:S(2)}) %collective-permute-start) | collective-permute-done | bytes 262176 | tf_op jit(solution)/shard_map/ppermute | solution.py:739
  11.3 1.8 %collective-permute-start.2 = (bf16[256,512]{1,0:T(8,128)(2,1)S(1)}, bf16[256,512]{1,0:T(8,128)(2,1)S(1)}, u32[]{:S(2)}, u32[]{:S(2)}) collective-permute-start(bf16[256,512]{1,0:T(8,128)(2,1)S(1)} %collective-permute-done.refs_4_), channel_id=1, source_target_pairs={{0,8},{8,16},{16,24},{24,28},{28,20},{20,12},{12,4},{4,0},{1,9},{9... | collective-permute-start | bytes 786440 | tf_op jit(solution)/shard_map/ppermute | solution.py:739
  13.3 5.4 %collective-permute-done.2.refs_3_ = bf16[256,512]{1,0:T(8,128)(2,1)S(1)} collective-permute-done((bf16[256,512]{1,0:T(8,128)(2,1)S(1)}, bf16[256,512]{1,0:T(8,128)(2,1)S(1)}, u32[]{:S(2)}, u32[]{:S(2)}) %collective-permute-start.2) | collective-permute-done | bytes 262176 | tf_op jit(solution)/shard_map/ppermute | solution.py:739
  18.7 1.5 collective-permute-start.3
  21.5 0.9 copy-done.22
  24.3 1.7 %shard_map.172 = (bf16[256,256]{1,0:T(8,128)(2,1)S(1)}, bf16[256,256]{1,0:T(8,128)(2,1)S(1)}, f32[4,256,128]{2,1,0:T(8,128)S(1)}, f32[4,256,128]{2,1,0:T(8,128)S(1)}, f32[4,256,256]{2,1,0:T(8,128)S(1)}) custom-call(s32[10]{0:T(128)S(1)} %pad_add_fusion.refs_0_, bf16[256,256]{1,0:T(8,128)(2,1)S(1)} %copy-done.26, bf16[256,256]{1,0:T(8,128)(2,1)S(1)} %copy-done.27, ...), custom_call_target="tpu_custom_call" | custom-call | flops 1207959552 | bytes 4194304 | tf_op jit(solution)/shard_map/pallas_call | solution.py:449
  26.0 2.3 %collective-permute-start.4 = (bf16[128,512]{1,0:T(8,128)(2,1)S(1)}, bf16[128,512]{1,0:T(8,128)(2,1)S(1)}, u32[]{:S(2)}, u32[]{:S(2)}) collective-permute-start(bf16[128,512]{1,0:T(8,128)(2,1)S(1)} %slice.45), channel_id=1, source_target_pairs={{0,8},{8,16},{16,24},{24,28},{28,20},{20,12},{12,4},{4,0},{1,9},{9... | collective-permute-start | bytes 393224 | tf_op jit(solution)/shard_map/ppermute | solution.py:739
  30.1 1.1 collective-permute-done.4.refs_4_
  31.2 2.1 %collective-permute-done.7.refs_5_ = bf16[128,512]{1,0:T(8,128)(2,1)S(1)} collective-permute-done((bf16[128,512]{1,0:T(8,128)(2,1)S(1)}, bf16[128,512]{1,0:T(8,128)(2,1)S(1)}, u32[]{:S(2)}, u32[]{:S(2)}) %collective-permute-start.7) | collective-permute-done | bytes 131104 | tf_op jit(solution)/shard_map/ppermute | solution.py:740
  33.4 4.3 %shard_map.175 = (f32[128,4096]{1,0:T(8,128)S(1)}, bf16[128,4096]{1,0:T(8,128)(2,1)S(1)}) custom-call(s32[10]{0:T(128)S(1)} %pad_add_fusion.refs_0_, f32[2]{0:T(128)S(1)} %copy-done.25, bf16[256,256]{1,0:T(8,128)(2,1)S(1)} %get-tuple-element.27.refs_1_.refs_2_, bf16[256,256]{1,0:T(8,128)(2,1)S(1)} %get-tuple-element.28.refs_2_.refs_3_, ...), custom_call_target="tpu_custom_call" | custom-call | flops 402653184 | bytes 4194304 | tf_op jit(solution)/shard_map/pallas_call | solution.py:449
  37.7 2.6 %collective-permute-done.8 = bf16[128,4096]{1,0:T(8,128)(2,1)S(1)} collective-permute-done((bf16[128,4096]{1,0:T(8,128)(2,1)S(1)}, bf16[128,4096]{1,0:T(8,128)(2,1)S(1)}, u32[]{:S(2)}, u32[]{:S(2)}) %collective-permute-start.8) | collective-permute-done | bytes 1048608 | tf_op jit(solution)/shard_map/ppermute | solution.py:757
  40.6 1.6 %collective-permute-start.9 = (bf16[128,4096]{1,0:T(8,128)(2,1)S(1)}, bf16[128,4096]{1,0:T(8,128)(2,1)S(1)}, u32[]{:S(2)}, u32[]{:S(2)}) collective-permute-start(bf16[128,4096]{1,0:T(8,128)(2,1)S(1)} %add_convert_fusion.1), channel_id=1, source_target_pairs={{0,2},{1,3},{2,0},{3,1},{4,6},{5,7},{6,4},{7,5},{8,10},{9,11},{10,... | collective-permute-start | bytes 3145736 | tf_op jit(solution)/shard_map/ppermute | solution.py:757
  42.2 3.5 %slices.1 = (bf16[32,4096]{1,0:T(8,128)(2,1)}, bf16[64,4096]{1,0:T(8,128)(2,1)}) custom-call(s32[10]{0:T(128)} %copy-done.23, bf16[4096,128]{1,0:T(8,128)(2,1)} %bitcast.7, bf16[4096,128]{1,0:T(8,128)(2,1)} %bitcast.8, bf16[128,4096]{1,0:T(8,128)(2,1)} %bitcast.9), custom_call_target="tpu_custom_call" | custom-call | tf_op jit(solution)/shard_map/slices/pallas_call | solution.py:511
  45.7 1.6 %collective-permute-start.21 = (bf16[64,4096]{1,0:T(8,128)(2,1)}, bf16[64,4096]{1,0:T(8,128)(2,1)S(1)}, u32[]{:S(2)}, u32[]{:S(2)}) collective-permute-start(bf16[64,4096]{1,0:T(8,128)(2,1)} %get-tuple-element.41.refs_9_), channel_id=1, source_target_pairs={{0,8},{8,16},{16,24},{24,28},{28,20},{20,12},{12,4},{4,0},{1,9},{9... | collective-permute-start | bytes 1572872 | tf_op jit(solution)/shard_map/ppermute | solution.py:739
  47.8 11.9 %collective-permute-done.21.refs_10_ = bf16[64,4096]{1,0:T(8,128)(2,1)S(1)} collective-permute-done((bf16[64,4096]{1,0:T(8,128)(2,1)}, bf16[64,4096]{1,0:T(8,128)(2,1)S(1)}, u32[]{:S(2)}, u32[]{:S(2)}) %collective-permute-start.21) | collective-permute-done | bytes 524320 | tf_op jit(solution)/shard_map/ppermute | solution.py:739
  59.6 1.6 %collective-permute-start.23 = (bf16[64,4096]{1,0:T(8,128)(2,1)S(1)}, bf16[64,4096]{1,0:T(8,128)(2,1)}, u32[]{:S(2)}, u32[]{:S(2)}) collective-permute-start(bf16[64,4096]{1,0:T(8,128)(2,1)S(1)} %collective-permute-done.21.refs_10_), channel_id=1, source_target_pairs={{0,8},{8,16},{16,24},{24,28},{28,20},{20,12},{12,4},{4,0},{1,9},{9... | collective-permute-start | bytes 1572872 | tf_op jit(solution)/shard_map/ppermute | solution.py:739
  61.7 4.2 %collective-permute-done.9 = bf16[128,4096]{1,0:T(8,128)(2,1)S(1)} collective-permute-done((bf16[128,4096]{1,0:T(8,128)(2,1)S(1)}, bf16[128,4096]{1,0:T(8,128)(2,1)S(1)}, u32[]{:S(2)}, u32[]{:S(2)}) %collective-permute-start.9) | collective-permute-done | bytes 1048608 | tf_op jit(solution)/shard_map/ppermute | solution.py:757
  67.4 1.6 %collective-permute-start.13 = (bf16[32,4096]{1,0:T(8,128)(2,1)S(1)}, bf16[32,4096]{1,0:T(8,128)(2,1)S(1)}, u32[]{:S(2)}, u32[]{:S(2)}) collective-permute-start(bf16[32,4096]{1,0:T(8,128)(2,1)S(1)} %copy-done.12), channel_id=1, source_target_pairs={{0,8},{8,16},{16,24},{24,28},{28,20},{20,12},{12,4},{4,0},{1,9},{9... | collective-permute-start | bytes 786440 | tf_op jit(solution)/shard_map/ppermute | solution.py:739
  69.5 8.6 %collective-permute-done.13.refs_1_ = bf16[32,4096]{1,0:T(8,128)(2,1)S(1)} collective-permute-done((bf16[32,4096]{1,0:T(8,128)(2,1)S(1)}, bf16[32,4096]{1,0:T(8,128)(2,1)S(1)}, u32[]{:S(2)}, u32[]{:S(2)}) %collective-permute-start.13) | collective-permute-done | bytes 262176 | tf_op jit(solution)/shard_map/ppermute | solution.py:739
  78.1 1.6 %collective-permute-start.15 = (bf16[32,4096]{1,0:T(8,128)(2,1)S(1)}, bf16[32,4096]{1,0:T(8,128)(2,1)S(1)}, u32[]{:S(2)}, u32[]{:S(2)}) collective-permute-start(bf16[32,4096]{1,0:T(8,128)(2,1)S(1)} %collective-permute-done.13.refs_1_), channel_id=1, source_target_pairs={{0,8},{8,16},{16,24},{24,28},{28,20},{20,12},{12,4},{4,0},{1,9},{9... | collective-permute-start | bytes 786440 | tf_op jit(solution)/shard_map/ppermute | solution.py:739
  81.0 2.0 %collective-permute-start.25 = (bf16[64,4096]{1,0:T(8,128)(2,1)}, bf16[64,4096]{1,0:T(8,128)(2,1)S(1)}, u32[]{:S(2)}, u32[]{:S(2)}) collective-permute-start(bf16[64,4096]{1,0:T(8,128)(2,1)} %collective-permute-done.23.refs_12_), channel_id=1, source_target_pairs={{0,8},{8,16},{16,24},{24,28},{28,20},{20,12},{12,4},{4,0},{1,9},{9... | collective-permute-start | bytes 1572872 | tf_op jit(solution)/shard_map/ppermute | solution.py:739
  83.0 4.1 %collective-permute-done.15.refs_3_ = bf16[32,4096]{1,0:T(8,128)(2,1)S(1)} collective-permute-done((bf16[32,4096]{1,0:T(8,128)(2,1)S(1)}, bf16[32,4096]{1,0:T(8,128)(2,1)S(1)}, u32[]{:S(2)}, u32[]{:S(2)}) %collective-permute-start.15) | collective-permute-done | bytes 262176 | tf_op jit(solution)/shard_map/ppermute | solution.py:739
  87.1 1.6 %collective-permute-start.17 = (bf16[32,4096]{1,0:T(8,128)(2,1)S(1)}, bf16[32,4096]{1,0:T(8,128)(2,1)S(1)}, u32[]{:S(2)}, u32[]{:S(2)}) collective-permute-start(bf16[32,4096]{1,0:T(8,128)(2,1)S(1)} %collective-permute-done.15.refs_3_), channel_id=1, source_target_pairs={{0,8},{8,16},{16,24},{24,28},{28,20},{20,12},{12,4},{4,0},{1,9},{9... | collective-permute-start | bytes 786440 | tf_op jit(solution)/shard_map/ppermute | solution.py:739
  90.8 10.9 %collective-permute-done.17.refs_5_ = bf16[32,4096]{1,0:T(8,128)(2,1)S(1)} collective-permute-done((bf16[32,4096]{1,0:T(8,128)(2,1)S(1)}, bf16[32,4096]{1,0:T(8,128)(2,1)S(1)}, u32[]{:S(2)}, u32[]{:S(2)}) %collective-permute-start.17) | collective-permute-done | bytes 262176 | tf_op jit(solution)/shard_map/ppermute | solution.py:739
  103.8 1.5 collective-permute-start.19
  105.9 1.9 %collective-permute-start.20 = (bf16[16,4096]{1,0:T(8,128)(2,1)}, bf16[16,4096]{1,0:T(8,128)(2,1)}, u32[]{:S(2)}, u32[]{:S(2)}) collective-permute-start(bf16[16,4096]{1,0:T(8,128)(2,1)} %slice.51), channel_id=1, source_target_pairs={{8,0},{16,8},{24,16},{28,24},{20,28},{12,20},{4,12},{0,4},{9,1},{1... | collective-permute-start | bytes 393224 | tf_op jit(solution)/shard_map/ppermute | solution.py:740
  109.1 1.6 %collective-permute-start.28 = (bf16[32,4096]{1,0:T(8,128)(2,1)S(1)}, bf16[32,4096]{1,0:T(8,128)(2,1)S(1)}, u32[]{:S(2)}, u32[]{:S(2)}) collective-permute-start(bf16[32,4096]{1,0:T(8,128)(2,1)S(1)} %slice.53), channel_id=1, source_target_pairs={{8,0},{16,8},{24,16},{28,24},{20,28},{12,20},{4,12},{0,4},{9,1},{1... | collective-permute-start | bytes 786440 | tf_op jit(solution)/shard_map/ppermute | solution.py:740
  111.2 1.2 copy-done.1
  112.4 1.2 copy-done.2
  113.7 1.2 copy-done.3
  114.9 0.9 copy-done.5
  115.8 1.0 copy-done.7
  116.9 1.0 copy-done.9
  117.9 1.0 copy-done.11
  119.0 0.9 copy-done.13
  119.9 0.9 copy-done.15
  120.9 0.9 copy-done.17
  121.8 0.9 copy-done.19
  122.8 0.9 copy-done.21
  123.7 1.8 %stack.9 = (bf16[256,4096]{1,0:T(8,128)(2,1)S(1)}, bf16[160,4096]{1,0:T(8,128)(2,1)S(1)}, bf16[288,4096]{1,0:T(8,128)(2,1)S(1)}, bf16[4096,128]{1,0:T(8,128)(2,1)S(1)}, bf16[4096,128]{1,0:T(8,128)(2,1)S(1)}) custom-call(bf16[32,4096]{1,0:T(8,128)(2,1)S(1)} %copy-done.13, bf16[32,4096]{1,0:T(8,128)(2,1)S(1)} %copy-done.15, bf16[32,4096]{1,0:T(8,128)(2,1)S(1)} %copy-done.17, ...), custom_call_target="tpu_custom_call" | custom-call | flops 1000000000 | bytes 16777216 | tf_op jit(solution)/shard_map/stack/pallas_call | solution.py:560
  125.6 6.8 %experts_most.1.refs_8_ = f32[256,4096]{1,0:T(8,128)S(1)} custom-call(s32[10]{0:T(128)S(1)} %copy-done.24, bf16[128,4096]{1,0:T(8,128)(2,1)S(1)} %fusion.2.refs_1_, bf16[128,4096]{1,0:T(8,128)(2,1)S(1)} %collective-permute-done.10.refs_2_, f32[128,8]{1,0:T(8,128)S(1)} %copy.28.refs_3_, f32[128,8]{1,0:T(8,128)S(1)} %collective-permute-done.12.refs_4_, ...), custom_call_target="tpu_custom_call" | custom-call | flops 2214592512 | bytes 16777216 | tf_op jit(solution)/shard_map/experts_most/pallas_call | solution.py:640
  132.4 3.2 %experts_rest.1 = (f32[128,4096]{1,0:T(8,128)S(1)}, bf16[128,4096]{1,0:T(8,128)(2,1)S(1)}) custom-call(s32[10]{0:T(128)S(1)} %copy-done.24, bf16[128,4096]{1,0:T(8,128)(2,1)S(1)} %fusion.2.refs_1_, bf16[128,4096]{1,0:T(8,128)(2,1)S(1)} %collective-permute-done.10.refs_2_, f32[128,8]{1,0:T(8,128)S(1)} %copy.28.refs_3_, ...), custom_call_target="tpu_custom_call" | custom-call | flops 201326592 | bytes 10485760 | tf_op jit(solution)/shard_map/experts_rest/pallas_call | solution.py:703
  135.7 2.6 %collective-permute-done.29 = bf16[128,4096]{1,0:T(8,128)(2,1)S(1)} collective-permute-done((bf16[128,4096]{1,0:T(8,128)(2,1)S(1)}, bf16[128,4096]{1,0:T(8,128)(2,1)S(1)}, u32[]{:S(2)}, u32[]{:S(2)}) %collective-permute-start.29) | collective-permute-done | bytes 1048608 | tf_op jit(solution)/shard_map/ppermute | solution.py:757
  138.6 1.4 collective-permute-start.30
  139.9 12.7 %collective-permute-done.30 = bf16[64,4096]{1,0:T(8,128)(2,1)S(1)} collective-permute-done((bf16[64,4096]{1,0:T(8,128)(2,1)S(1)}, bf16[64,4096]{1,0:T(8,128)(2,1)S(1)}, u32[]{:S(2)}, u32[]{:S(2)}) %collective-permute-start.30) | collective-permute-done | bytes 524320 | tf_op jit(solution)/shard_map/ppermute | solution.py:757
  152.6 1.0 fusion.4
  (109 shorter events, 16.6 us)
Async XLA Ops:
  1.7 9.6 %collective-permute-start = (bf16[256,512]{1,0:T(8,128)(2,1)}, bf16[256,512]{1,0:T(8,128)(2,1)S(1)}, u32[]{:S(2)}, u32[]{:S(2)}) collective-permute-start(bf16[256,512]{1,0:T(8,128)(2,1)} %pack.1.refs_3_), channel_id=1, source_target_pairs={{0,8},{8,16},{16,24},{24,28},{28,20},{20,12},{12,4},{4,0},{1,9},{9... | collective-permute-start | bytes 786440 | tf_op jit(solution)/shard_map/ppermute | solution.py:739
  4.8 8.3 %collective-permute-start.1 = (bf16[256,512]{1,0:T(8,128)(2,1)}, bf16[256,512]{1,0:T(8,128)(2,1)S(1)}, u32[]{:S(2)}, u32[]{:S(2)}) collective-permute-start(bf16[256,512]{1,0:T(8,128)(2,1)} %pack.1.refs_3_), channel_id=1, source_target_pairs={{8,0},{16,8},{24,16},{28,24},{20,28},{12,20},{4,12},{0,4},{9,1},{1... | collective-permute-start | bytes 786440 | tf_op jit(solution)/shard_map/ppermute | solution.py:740
  11.3 7.5 %collective-permute-start.2 = (bf16[256,512]{1,0:T(8,128)(2,1)S(1)}, bf16[256,512]{1,0:T(8,128)(2,1)S(1)}, u32[]{:S(2)}, u32[]{:S(2)}) collective-permute-start(bf16[256,512]{1,0:T(8,128)(2,1)S(1)} %collective-permute-done.refs_4_), channel_id=1, source_target_pairs={{0,8},{8,16},{16,24},{24,28},{28,20},{20,12},{12,4},{4,0},{1,9},{9... | collective-permute-start | bytes 786440 | tf_op jit(solution)/shard_map/ppermute | solution.py:739
  13.1 7.2 %collective-permute-start.5 = (bf16[256,512]{1,0:T(8,128)(2,1)S(1)}, bf16[256,512]{1,0:T(8,128)(2,1)S(1)}, u32[]{:S(2)}, u32[]{:S(2)}) collective-permute-start(bf16[256,512]{1,0:T(8,128)(2,1)S(1)} %collective-permute-done.1.refs_5_), channel_id=1, source_target_pairs={{8,0},{16,8},{24,16},{28,24},{20,28},{12,20},{4,12},{0,4},{9,1},{1... | collective-permute-start | bytes 786440 | tf_op jit(solution)/shard_map/ppermute | solution.py:740
  18.7 7.3 %collective-permute-start.3 = (bf16[256,512]{1,0:T(8,128)(2,1)S(1)}, bf16[256,512]{1,0:T(8,128)(2,1)S(1)}, u32[]{:S(2)}, u32[]{:S(2)}) collective-permute-start(bf16[256,512]{1,0:T(8,128)(2,1)S(1)} %collective-permute-done.2.refs_3_), channel_id=1, source_target_pairs={{0,8},{8,16},{16,24},{24,28},{28,20},{20,12},{12,4},{4,0},{1,9},{9... | collective-permute-start | bytes 786440 | tf_op jit(solution)/shard_map/ppermute | solution.py:739
  20.3 8.0 %collective-permute-start.6 = (bf16[256,512]{1,0:T(8,128)(2,1)S(1)}, bf16[256,512]{1,0:T(8,128)(2,1)S(1)}, u32[]{:S(2)}, u32[]{:S(2)}) collective-permute-start(bf16[256,512]{1,0:T(8,128)(2,1)S(1)} %collective-permute-done.5.refs_4_), channel_id=1, source_target_pairs={{8,0},{16,8},{24,16},{28,24},{20,28},{12,20},{4,12},{0,4},{9,1},{1... | collective-permute-start | bytes 786440 | tf_op jit(solution)/shard_map/ppermute | solution.py:740
  24.3 9.0 %copy-start.23 = (s32[10]{0:T(128)}, s32[10]{0:T(128)S(1)}, u32[]{:S(2)}) copy-start(s32[10]{0:T(128)S(1)} %pad_add_fusion.refs_0_) | copy-start | bytes 124
  26.0 5.2 %collective-permute-start.4 = (bf16[128,512]{1,0:T(8,128)(2,1)S(1)}, bf16[128,512]{1,0:T(8,128)(2,1)S(1)}, u32[]{:S(2)}, u32[]{:S(2)}) collective-permute-start(bf16[128,512]{1,0:T(8,128)(2,1)S(1)} %slice.45), channel_id=1, source_target_pairs={{0,8},{8,16},{16,24},{24,28},{28,20},{20,12},{12,4},{4,0},{1,9},{9... | collective-permute-start | bytes 393224 | tf_op jit(solution)/shard_map/ppermute | solution.py:739
  28.3 5.0 %collective-permute-start.7 = (bf16[128,512]{1,0:T(8,128)(2,1)S(1)}, bf16[128,512]{1,0:T(8,128)(2,1)S(1)}, u32[]{:S(2)}, u32[]{:S(2)}) collective-permute-start(bf16[128,512]{1,0:T(8,128)(2,1)S(1)} %slice.46), channel_id=1, source_target_pairs={{8,0},{16,8},{24,16},{28,24},{20,28},{12,20},{4,12},{0,4},{9,1},{1... | collective-permute-start | bytes 393224 | tf_op jit(solution)/shard_map/ppermute | solution.py:740
  28.4 5.0 %copy-start = (bf16[512,4096]{1,0:T(8,128)(2,1)S(1)}, bf16[512,4096]{1,0:T(8,128)(2,1)}, u32[]{:S(2)}) copy-start(bf16[512,4096]{1,0:T(8,128)(2,1)} %refs_9_.1) | copy-start | bytes 12582916
  29.2 4.1 %copy-start.6 = (bf16[64,4096]{1,0:T(8,128)(2,1)S(1)}, bf16[64,4096]{1,0:T(8,128)(2,1)}, u32[]{:S(2)}) copy-start(bf16[64,4096]{1,0:T(8,128)(2,1)} %refs_10_.1) | copy-start | bytes 1572868
  29.2 4.1 %copy-start.25 = (f32[2]{0:T(128)S(1)}, f32[2]{0:T(128)}, u32[]{:S(2)}) copy-start(f32[2]{0:T(128)} %refs_1_.3) | copy-start | bytes 28
  37.6 2.7 %collective-permute-start.8 = (bf16[128,4096]{1,0:T(8,128)(2,1)S(1)}, bf16[128,4096]{1,0:T(8,128)(2,1)S(1)}, u32[]{:S(2)}, u32[]{:S(2)}) collective-permute-start(bf16[128,4096]{1,0:T(8,128)(2,1)S(1)} %get-tuple-element.39), channel_id=1, source_target_pairs={{0,1},{1,0},{2,3},{3,2},{4,5},{5,4},{6,7},{7,6},{8,9},{9,8},{10,11... | collective-permute-start | bytes 3145736 | tf_op jit(solution)/shard_map/ppermute | solution.py:757
  40.6 25.3 %collective-permute-start.9 = (bf16[128,4096]{1,0:T(8,128)(2,1)S(1)}, bf16[128,4096]{1,0:T(8,128)(2,1)S(1)}, u32[]{:S(2)}, u32[]{:S(2)}) collective-permute-start(bf16[128,4096]{1,0:T(8,128)(2,1)S(1)} %add_convert_fusion.1), channel_id=1, source_target_pairs={{0,2},{1,3},{2,0},{3,1},{4,6},{5,7},{6,4},{7,5},{8,10},{9,11},{10,... | collective-permute-start | bytes 3145736 | tf_op jit(solution)/shard_map/ppermute | solution.py:757
  45.7 13.9 %collective-permute-start.21 = (bf16[64,4096]{1,0:T(8,128)(2,1)}, bf16[64,4096]{1,0:T(8,128)(2,1)S(1)}, u32[]{:S(2)}, u32[]{:S(2)}) collective-permute-start(bf16[64,4096]{1,0:T(8,128)(2,1)} %get-tuple-element.41.refs_9_), channel_id=1, source_target_pairs={{0,8},{8,16},{16,24},{24,28},{28,20},{20,12},{12,4},{4,0},{1,9},{9... | collective-permute-start | bytes 1572872 | tf_op jit(solution)/shard_map/ppermute | solution.py:739
  47.3 14.3 %collective-permute-start.22 = (bf16[64,4096]{1,0:T(8,128)(2,1)}, bf16[64,4096]{1,0:T(8,128)(2,1)S(1)}, u32[]{:S(2)}, u32[]{:S(2)}) collective-permute-start(bf16[64,4096]{1,0:T(8,128)(2,1)} %get-tuple-element.41.refs_9_), channel_id=1, source_target_pairs={{8,0},{16,8},{24,16},{28,24},{20,28},{12,20},{4,12},{0,4},{9,1},{1... | collective-permute-start | bytes 1572872 | tf_op jit(solution)/shard_map/ppermute | solution.py:740
  59.6 6.6 %copy-start.8 = (bf16[64,4096]{1,0:T(8,128)(2,1)}, bf16[64,4096]{1,0:T(8,128)(2,1)S(1)}, u32[]{:S(2)}) copy-start(bf16[64,4096]{1,0:T(8,128)(2,1)S(1)} %collective-permute-done.21.refs_10_) | copy-start | bytes 1572868
  59.6 21.4 %collective-permute-start.23 = (bf16[64,4096]{1,0:T(8,128)(2,1)S(1)}, bf16[64,4096]{1,0:T(8,128)(2,1)}, u32[]{:S(2)}, u32[]{:S(2)}) collective-permute-start(bf16[64,4096]{1,0:T(8,128)(2,1)S(1)} %collective-permute-done.21.refs_10_), channel_id=1, source_target_pairs={{0,8},{8,16},{16,24},{24,28},{28,20},{20,12},{12,4},{4,0},{1,9},{9... | collective-permute-start | bytes 1572872 | tf_op jit(solution)/shard_map/ppermute | solution.py:739
  61.6 4.7 %copy-start.10 = (bf16[64,4096]{1,0:T(8,128)(2,1)}, bf16[64,4096]{1,0:T(8,128)(2,1)S(1)}, u32[]{:S(2)}) copy-start(bf16[64,4096]{1,0:T(8,128)(2,1)S(1)} %collective-permute-done.22.refs_11_) | copy-start | bytes 1572868
  61.6 21.4 %collective-permute-start.24 = (bf16[64,4096]{1,0:T(8,128)(2,1)S(1)}, bf16[64,4096]{1,0:T(8,128)(2,1)}, u32[]{:S(2)}, u32[]{:S(2)}) collective-permute-start(bf16[64,4096]{1,0:T(8,128)(2,1)S(1)} %collective-permute-done.22.refs_11_), channel_id=1, source_target_pairs={{8,0},{16,8},{24,16},{28,24},{20,28},{12,20},{4,12},{0,4},{9,1},{1... | collective-permute-start | bytes 1572872 | tf_op jit(solution)/shard_map/ppermute | solution.py:740
  66.3 41.5 %copy-start.28 = (bf16[128,4096]{1,0:T(8,128)(2,1)}, bf16[128,4096]{1,0:T(8,128)(2,1)S(1)}, u32[]{:S(2)}) copy-start(bf16[128,4096]{1,0:T(8,128)(2,1)S(1)} %add_convert_fusion) | copy-start | bytes 3145732
  66.3 1.1 copy-start.12
  66.3 24.4 %copy-start.31 = (f32[64,4]{0,1:T(4,128)S(1)}, f32[64,4]{0,1:T(4,128)}, u32[]{:S(2)}) copy-start(f32[64,4]{0,1:T(4,128)} %param.28) | copy-start | bytes 3076
  66.3 24.4 %copy-start.32 = (s32[64,4]{0,1:T(4,128)S(1)}, s32[64,4]{0,1:T(4,128)}, u32[]{:S(2)}) copy-start(s32[64,4]{0,1:T(4,128)} %param.27) | copy-start | bytes 3076
  67.1 58.5 %collective-permute-start.10 = (bf16[128,4096]{1,0:T(8,128)(2,1)S(1)}, bf16[128,4096]{1,0:T(8,128)(2,1)S(1)}, u32[]{:S(2)}, u32[]{:S(2)}) collective-permute-start(bf16[128,4096]{1,0:T(8,128)(2,1)S(1)} %fusion.2.refs_1_), channel_id=1, source_target_pairs={{0,1},{1,0},{2,3},{3,2},{4,5},{5,4},{6,7},{7,6},{8,9},{9,8},{10,11... | collective-permute-start | bytes 3145736 | tf_op jit(solution)/shard_map/ppermute | solution.py:757
  67.4 10.6 %collective-permute-start.13 = (bf16[32,4096]{1,0:T(8,128)(2,1)S(1)}, bf16[32,4096]{1,0:T(8,128)(2,1)S(1)}, u32[]{:S(2)}, u32[]{:S(2)}) collective-permute-start(bf16[32,4096]{1,0:T(8,128)(2,1)S(1)} %copy-done.12), channel_id=1, source_target_pairs={{0,8},{8,16},{16,24},{24,28},{28,20},{20,12},{12,4},{4,0},{1,9},{9... | collective-permute-start | bytes 786440 | tf_op jit(solution)/shard_map/ppermute | solution.py:739
  69.0 11.3 %collective-permute-start.14 = (bf16[32,4096]{1,0:T(8,128)(2,1)S(1)}, bf16[32,4096]{1,0:T(8,128)(2,1)S(1)}, u32[]{:S(2)}, u32[]{:S(2)}) collective-permute-start(bf16[32,4096]{1,0:T(8,128)(2,1)S(1)} %copy-done.12), channel_id=1, source_target_pairs={{8,0},{16,8},{24,16},{28,24},{20,28},{12,20},{4,12},{0,4},{9,1},{1... | collective-permute-start | bytes 786440 | tf_op jit(solution)/shard_map/ppermute | solution.py:740
  78.1 29.7 %copy-start.14 = (bf16[32,4096]{1,0:T(8,128)(2,1)}, bf16[32,4096]{1,0:T(8,128)(2,1)S(1)}, u32[]{:S(2)}) copy-start(bf16[32,4096]{1,0:T(8,128)(2,1)S(1)} %collective-permute-done.13.refs_1_) | copy-start | bytes 786436
  78.1 9.1 %collective-permute-start.15 = (bf16[32,4096]{1,0:T(8,128)(2,1)S(1)}, bf16[32,4096]{1,0:T(8,128)(2,1)S(1)}, u32[]{:S(2)}, u32[]{:S(2)}) collective-permute-start(bf16[32,4096]{1,0:T(8,128)(2,1)S(1)} %collective-permute-done.13.refs_1_), channel_id=1, source_target_pairs={{0,8},{8,16},{16,24},{24,28},{28,20},{20,12},{12,4},{4,0},{1,9},{9... | collective-permute-start | bytes 786440 | tf_op jit(solution)/shard_map/ppermute | solution.py:739
  80.3 9.2 %collective-permute-start.16 = (bf16[32,4096]{1,0:T(8,128)(2,1)S(1)}, bf16[32,4096]{1,0:T(8,128)(2,1)S(1)}, u32[]{:S(2)}, u32[]{:S(2)}) collective-permute-start(bf16[32,4096]{1,0:T(8,128)(2,1)S(1)} %collective-permute-done.14.refs_2_), channel_id=1, source_target_pairs={{8,0},{16,8},{24,16},{28,24},{20,28},{12,20},{4,12},{0,4},{9,1},{1... | collective-permute-start | bytes 786440 | tf_op jit(solution)/shard_map/ppermute | solution.py:740
  81.0 27.0 %collective-permute-start.25 = (bf16[64,4096]{1,0:T(8,128)(2,1)}, bf16[64,4096]{1,0:T(8,128)(2,1)S(1)}, u32[]{:S(2)}, u32[]{:S(2)}) collective-permute-start(bf16[64,4096]{1,0:T(8,128)(2,1)} %collective-permute-done.23.refs_12_), channel_id=1, source_target_pairs={{0,8},{8,16},{16,24},{24,28},{28,20},{20,12},{12,4},{4,0},{1,9},{9... | collective-permute-start | bytes 1572872 | tf_op jit(solution)/shard_map/ppermute | solution.py:739
  83.0 25.1 %collective-permute-start.27 = (bf16[64,4096]{1,0:T(8,128)(2,1)}, bf16[64,4096]{1,0:T(8,128)(2,1)S(1)}, u32[]{:S(2)}, u32[]{:S(2)}) collective-permute-start(bf16[64,4096]{1,0:T(8,128)(2,1)} %collective-permute-done.24.refs_13_), channel_id=1, source_target_pairs={{8,0},{16,8},{24,16},{28,24},{20,28},{12,20},{4,12},{0,4},{9,1},{1... | collective-permute-start | bytes 1572872 | tf_op jit(solution)/shard_map/ppermute | solution.py:740
  87.1 14.5 %collective-permute-start.17 = (bf16[32,4096]{1,0:T(8,128)(2,1)S(1)}, bf16[32,4096]{1,0:T(8,128)(2,1)S(1)}, u32[]{:S(2)}, u32[]{:S(2)}) collective-permute-start(bf16[32,4096]{1,0:T(8,128)(2,1)S(1)} %collective-permute-done.15.refs_3_), channel_id=1, source_target_pairs={{0,8},{8,16},{16,24},{24,28},{28,20},{20,12},{12,4},{4,0},{1,9},{9... | collective-permute-start | bytes 786440 | tf_op jit(solution)/shard_map/ppermute | solution.py:739
  89.5 14.3 %collective-permute-start.18 = (bf16[32,4096]{1,0:T(8,128)(2,1)S(1)}, bf16[32,4096]{1,0:T(8,128)(2,1)S(1)}, u32[]{:S(2)}, u32[]{:S(2)}) collective-permute-start(bf16[32,4096]{1,0:T(8,128)(2,1)S(1)} %collective-permute-done.16.refs_4_), channel_id=1, source_target_pairs={{8,0},{16,8},{24,16},{28,24},{20,28},{12,20},{4,12},{0,4},{9,1},{1... | collective-permute-start | bytes 786440 | tf_op jit(solution)/shard_map/ppermute | solution.py:740
  101.6 4.3 %collective-permute-start.11 = (f32[64,8]{0,1:T(8,128)S(1)}, f32[64,8]{0,1:T(8,128)S(1)}, u32[]{:S(2)}, u32[]{:S(2)}) collective-permute-start(f32[64,8]{0,1:T(8,128)S(1)} %select_reduce_fusion), channel_id=1, source_target_pairs={{0,2},{1,3},{2,0},{3,1},{4,6},{5,7},{6,4},{7,5},{8,10},{9,11},{10,... | collective-permute-start | bytes 6152 | tf_op jit(solution)/shard_map/ppermute | solution.py:757
  103.8 4.0 %copy-start.4 = (bf16[32,4096]{1,0:T(8,128)(2,1)}, bf16[32,4096]{1,0:T(8,128)(2,1)S(1)}, u32[]{:S(2)}) copy-start(bf16[32,4096]{1,0:T(8,128)(2,1)S(1)} %collective-permute-done.18.refs_6_) | copy-start | bytes 786436
  103.8 5.3 %collective-permute-start.19 = (bf16[16,4096]{1,0:T(8,128)(2,1)}, bf16[16,4096]{1,0:T(8,128)(2,1)}, u32[]{:S(2)}, u32[]{:S(2)}) collective-permute-start(bf16[16,4096]{1,0:T(8,128)(2,1)} %slice.50), channel_id=1, source_target_pairs={{0,8},{8,16},{16,24},{24,28},{28,20},{20,12},{12,4},{4,0},{1,9},{9... | collective-permute-start | bytes 393224 | tf_op jit(solution)/shard_map/ppermute | solution.py:739
  105.9 5.3 %collective-permute-start.20 = (bf16[16,4096]{1,0:T(8,128)(2,1)}, bf16[16,4096]{1,0:T(8,128)(2,1)}, u32[]{:S(2)}, u32[]{:S(2)}) collective-permute-start(bf16[16,4096]{1,0:T(8,128)(2,1)} %slice.51), channel_id=1, source_target_pairs={{8,0},{16,8},{24,16},{28,24},{20,28},{12,20},{4,12},{0,4},{9,1},{1... | collective-permute-start | bytes 393224 | tf_op jit(solution)/shard_map/ppermute | solution.py:740
  108.0 17.5 %collective-permute-start.12 = (f32[128,8]{1,0:T(8,128)S(1)}, f32[128,8]{1,0:T(8,128)S(1)}, u32[]{:S(2)}, u32[]{:S(2)}) collective-permute-start(f32[128,8]{1,0:T(8,128)S(1)} %copy.28.refs_3_), channel_id=1, source_target_pairs={{0,1},{1,0},{2,3},{3,2},{4,5},{5,4},{6,7},{7,6},{8,9},{9,8},{10,11... | collective-permute-start | bytes 12296 | tf_op jit(solution)/shard_map/ppermute | solution.py:757
  108.1 24.3 %collective-permute-start.26 = (bf16[32,4096]{1,0:T(8,128)(2,1)S(1)}, bf16[32,4096]{1,0:T(8,128)(2,1)S(1)}, u32[]{:S(2)}, u32[]{:S(2)}) collective-permute-start(bf16[32,4096]{1,0:T(8,128)(2,1)S(1)} %slice.52), channel_id=1, source_target_pairs={{0,8},{8,16},{16,24},{24,28},{28,20},{20,12},{12,4},{4,0},{1,9},{9... | collective-permute-start | bytes 786440 | tf_op jit(solution)/shard_map/ppermute | solution.py:739
  108.3 17.2 %copy-start.24 = (s32[10]{0:T(128)S(1)}, s32[10]{0:T(128)}, u32[]{:S(2)}) copy-start(s32[10]{0:T(128)} %copy-done.23) | copy-start | bytes 124
  109.1 23.3 %collective-permute-start.28 = (bf16[32,4096]{1,0:T(8,128)(2,1)S(1)}, bf16[32,4096]{1,0:T(8,128)(2,1)S(1)}, u32[]{:S(2)}, u32[]{:S(2)}) collective-permute-start(bf16[32,4096]{1,0:T(8,128)(2,1)S(1)} %slice.53), channel_id=1, source_target_pairs={{8,0},{16,8},{24,16},{28,24},{20,28},{12,20},{4,12},{0,4},{9,1},{1... | collective-permute-start | bytes 786440 | tf_op jit(solution)/shard_map/ppermute | solution.py:740
  111.2 1.2 copy-start.1
  112.4 1.2 copy-start.2
  113.7 1.2 copy-start.3
  135.6 2.7 %collective-permute-start.29 = (bf16[128,4096]{1,0:T(8,128)(2,1)S(1)}, bf16[128,4096]{1,0:T(8,128)(2,1)S(1)}, u32[]{:S(2)}, u32[]{:S(2)}) collective-permute-start(bf16[128,4096]{1,0:T(8,128)(2,1)S(1)} %get-tuple-element.48), channel_id=1, source_target_pairs={{0,1},{1,0},{2,3},{3,2},{4,5},{5,4},{6,7},{7,6},{8,9},{9,8},{10,11... | collective-permute-start | bytes 3145736 | tf_op jit(solution)/shard_map/ppermute | solution.py:757
  138.3 14.3 %copy-start.29 = (bf16[128,4096]{1,0:T(8,128)(2,1)S(1)}, bf16[128,4096]{1,0:T(8,128)(2,1)}, u32[]{:S(2)}) copy-start(bf16[128,4096]{1,0:T(8,128)(2,1)} %copy-done.28) | copy-start | bytes 3145732
  138.6 14.0 %collective-permute-start.30 = (bf16[64,4096]{1,0:T(8,128)(2,1)S(1)}, bf16[64,4096]{1,0:T(8,128)(2,1)S(1)}, u32[]{:S(2)}, u32[]{:S(2)}) collective-permute-start(bf16[64,4096]{1,0:T(8,128)(2,1)S(1)} %slice.63), channel_id=1, source_target_pairs={{0,2},{1,3},{2,0},{3,1},{4,6},{5,7},{6,4},{7,5},{8,10},{9,11},{10,... | collective-permute-start | bytes 1572872 | tf_op jit(solution)/shard_map/ppermute | solution.py:757
  (16 other events, 14.4 us)

commit v2 on v1

--- a/solution.py
+++ b/solution.py
@@ -486,36 +486,29 @@
     )(one, two, three)
 
 
-def slices_kernel(unit, ids_ref, gate_ref, up_ref, down_ref, gate_out, rest_out, gate, up, turned, sem):
-    start = pl.multiple_of(ids_ref[1] * unit, unit)
+def slices_kernel(unit, at_ref, gate_ref, up_ref, down_ref, gate_out, up_out, down_out, gate, up, turned, sem):
+    start = pl.multiple_of(at_ref[0] * unit, unit)
     loads = grouped(
         [
             pltpu.make_async_copy(gate_ref, gate, sem.at[0]),
             pltpu.make_async_copy(up_ref, up, sem.at[1]),
-            pltpu.make_async_copy(
-                down_ref.at[pl.ds(start, unit)], rest_out.at[pl.ds(unit, unit)], sem.at[2]
-            ),
+            pltpu.make_async_copy(down_ref.at[pl.ds(start, unit)], down_out, sem.at[2]),
         ]
     )
-    loads[0].wait()
-    turned[...] = gate[...].T
-    gate_out[...] = turned[pl.ds(start, unit)]
-    loads[1].wait()
-    turned[...] = up[...].T
-    rest_out[:unit] = turned[pl.ds(start, unit)]
+    for load, source, out in ((loads[0], gate, gate_out), (loads[1], up, up_out)):
+        load.wait()
+        turned[...] = source[...].T
+        out[...] = turned[pl.ds(start, unit)]
     loads[2].wait()
 
 
-def slices_call(ids, gate, up, down, unit):
+def slices_call(mine, gate, up, down, unit):
     width = gate.shape[0]
     return pl.pallas_call(
         lambda *refs: slices_kernel(unit, *refs),
-        out_shape=[
-            jax.ShapeDtypeStruct((unit, width), gate.dtype),
-            jax.ShapeDtypeStruct((2 * unit, width), gate.dtype),
-        ],
+        out_shape=[jax.ShapeDtypeStruct((unit, width), gate.dtype)] * 3,
         in_specs=specs(SMEM, 1) + specs(HBM, 3),
-        out_specs=specs(VMEM, 2),
+        out_specs=specs(VMEM, 3),
         scratch_shapes=[
             pltpu.VMEM(gate.shape, gate.dtype),
             pltpu.VMEM(up.shape, gate.dtype),
@@ -523,209 +516,215 @@
             pltpu.SemaphoreType.DMA((3,)),
         ],
         name="slices",
-    )(ids, gate, up, down)
+    )(mine, gate, up, down)
+
+
+def combine_kernel(routes_ref, weights_ref, out_ref):
+    expert = lax.broadcasted_iota(jnp.int32, out_ref.shape, 1)
+    total = jnp.zeros(out_ref.shape, jnp.float32)
+    for choice in range(routes_ref.shape[1]):
+        chosen = jnp.broadcast_to(routes_ref[:, choice : choice + 1], out_ref.shape)
+        weight = jnp.broadcast_to(weights_ref[:, choice : choice + 1], out_ref.shape)
+        total += jnp.where(expert == chosen, weight, 0.0)
+    out_ref[...] = total
+
+
+def combine_call(routes, weights):
+    return pl.pallas_call(
+        combine_kernel,
+        out_shape=jax.ShapeDtypeStruct((routes.shape[0], 128), jnp.float32),
+        in_specs=specs(VMEM, 2),
+        out_specs=pl.BlockSpec(memory_space=VMEM),
+        compiler_params=pltpu.CompilerParams(vmem_limit_bytes=2 * MIB),
+        name="combine",
+    )(routes, weights)
 
 
 def silu(v):
     return v / (1.0 + jnp.exp(-v))
 
 
-def stack_kernel(unit, gates_count, rests_count, *refs):
-    refs = list(refs)
-    gates = [refs.pop(0) for _ in range(gates_count)]
-    rests = [refs.pop(0) for _ in range(rests_count)]
-    sg_ref, su_ref, sd_ref, gate_out, up_out, down_out, sg_out, su_out, sem = refs
-    moves = [(sg_ref, sg_out), (su_ref, su_out)]
-    at = 0
-    for ref in gates:
-        moves.append((ref, gate_out.at[pl.ds(at, ref.shape[0])]))
-        at += ref.shape[0]
-    for index, ref in enumerate(rests):
-        moves.append((ref.at[pl.ds(0, unit)], up_out.at[pl.ds(index * unit, unit)]))
-        moves.append((ref.at[pl.ds(unit, unit)], down_out.at[pl.ds(index * unit, unit)]))
-    moves.append((sd_ref, down_out.at[pl.ds(rests_count * unit, sd_ref.shape[0])]))
-    copies = grouped(
-        [pltpu.make_async_copy(a, b, sem.at[k]) for k, (a, b) in enumerate(moves)]
-    )
-    for copy in copies:
+def spread(ids_ref, combine, count, unit):
+    expert = lax.broadcasted_iota(jnp.int32, combine.shape, 1)
+    columns = []
+    for block in range(count):
+        picked = jnp.where(expert == ids_ref[2 + block], combine, 0.0)
+        column = jnp.sum(picked, axis=1, keepdims=True)
+        columns.append(jnp.broadcast_to(column, (combine.shape[0], unit)))
+    return jnp.concatenate(columns, axis=1)
+
+
+def stack_kernel(plan, *refs):
+    sem = refs[-1]
+    outs = refs[-1 - len(plan) : -1]
+    copies = []
+    for out, pieces in zip(outs, plan):
+        at = 0
+        for which, first, rows in pieces:
+            copies.append(
+                pltpu.make_async_copy(
+                    refs[which].at[pl.ds(first, rows)],
+                    out.at[pl.ds(at, rows)],
+                    sem.at[len(copies)],
+                )
+            )
+            at += rows
+    for copy in grouped(copies):
         copy.wait()
 
 
-def stack_call(gates, rests, s_gate, s_up, s_down):
-    unit = rests[0].shape[0] // 2
-    width = rests[0].shape[1]
-    operands = [*gates, *rests, s_gate, s_up, s_down]
-    total = sum(g.shape[0] for g in gates)
-    most = len(rests) * unit
+def whole(array):
+    return (array, 0, array.shape[0])
+
+
+def stack_call(*groups):
+    operands, plan, shapes = [], [], []
+    for group in groups:
+        pieces = []
+        for array, first, rows in group:
+            pieces.append((len(operands), first, rows))
+            operands.append(array)
+        plan.append(tuple(pieces))
+        shapes.append((sum(rows for _, _, rows in group), group[0][0].shape[1]))
     return pl.pallas_call(
-        lambda *refs: stack_kernel(unit, len(gates), len(rests), *refs),
-        out_shape=[
-            pltpu.VMEM((total, width), jnp.bfloat16),
-            pltpu.VMEM((most, width), jnp.bfloat16),
-            pltpu.VMEM((most + s_down.shape[0], width), jnp.bfloat16),
-            pltpu.VMEM(s_gate.shape, jnp.bfloat16),
-            pltpu.VMEM(s_up.shape, jnp.bfloat16),
-        ],
+        lambda *refs: stack_kernel(tuple(plan), *refs),
+        out_shape=[pltpu.VMEM(shape, operands[0].dtype) for shape in shapes],
         in_specs=specs(HBM, len(operands)),
-        out_specs=specs(VMEM, 5),
-        scratch_shapes=[pltpu.SemaphoreType.DMA((len(gates) + 2 * len(rests) + 3,))],
+        out_specs=specs(VMEM, len(groups)),
+        scratch_shapes=[pltpu.SemaphoreType.DMA((len(operands),))],
         cost_estimate=pl.CostEstimate(flops=10**9, bytes_accessed=16 * MIB, transcendentals=0),
         compiler_params=pltpu.CompilerParams(vmem_limit_bytes=2 * MIB),
         name="stack",
     )(*operands)
 
 
-def spread(ids_ref, combine, first, count, unit):
-    expert = lax.broadcasted_iota(jnp.int32, combine.shape, 1)
-    columns = []
-    for block in range(first, first + count):
-        picked = jnp.where(expert == ids_ref[2 + block], combine, 0.0)
-        column = jnp.sum(picked, axis=1, keepdims=True)
-        columns.append(jnp.broadcast_to(column, (combine.shape[0], unit)))
-    return jnp.concatenate(columns, axis=1)
-
-
-def most_kernel(count, unit, ids_ref, one_ref, two_ref, near_ref, far_ref, *refs):
-    refs = list(refs)
-    late = [refs.pop(0) for _ in range(count)]
-    gate_ref, up_ref, down_ref, sg_ref, su_ref, out_ref, x_ref, late_ref, hidden_ref, sem = refs
+def hidden_kernel(unit, ids_ref, one_ref, two_ref, near_ref, far_ref, low_ref, high_ref, gate_ref, up_ref, sg_ref, su_ref, out_ref, x_ref, late_ref, sem):
     half = one_ref.shape[0]
-    moves = [(one_ref, x_ref.at[pl.ds(0, half)]), (two_ref, x_ref.at[pl.ds(half, half)])]
-    moves += [
-        (ref, late_ref.at[pl.ds(2 * unit * index, 2 * unit)]) for index, ref in enumerate(late)
-    ]
-    copies = grouped(
-        [pltpu.make_async_copy(a, b, sem.at[k]) for k, (a, b) in enumerate(moves)]
-    )
-    copies[0].wait()
-    copies[1].wait()
-    x = x_ref[...]
-    begun = up_ref.shape[0]
-    used = begun + count * unit
-    gate = dot_nt(x, gate_ref[:used])
-    for copy in copies[2:]:
-        copy.wait()
-    ups = [late_ref[2 * unit * index : 2 * unit * index + unit] for index in range(count)]
-    up = dot_nt(x, jnp.concatenate([up_ref[...]] + ups, axis=0))
-    combine = jnp.concatenate([near_ref[...], far_ref[...]], axis=0)
-    scale = spread(ids_ref, combine, 0, used // unit, unit)
-    hidden = (silu(gate) * up * scale).astype(jnp.bfloat16)
-    gate = jnp.dot(x, sg_ref[...], preferred_element_type=jnp.float32)
-    up = jnp.dot(x, su_ref[...], preferred_element_type=jnp.float32)
-    shared = (silu(gate) * up).astype(jnp.bfloat16)
-    hidden_ref[:, :begun] = hidden[:, :begun]
-    hidden_ref[:, begun : begun + shared.shape[1]] = shared
-    hidden_ref[:, begun + shared.shape[1] :] = hidden[:, begun:]
-    width = out_ref.shape[1]
-    step = math.gcd(width, 512)
-
-    def body(at, _):
-        cols = pl.ds(pl.multiple_of(at * step, step), step)
-        downs = [
-            late_ref[2 * unit * index + unit : 2 * unit * (index + 1), cols]
-            for index in range(count)
-        ]
-        down = jnp.concatenate([down_ref[:, cols]] + downs, axis=0)
-        out_ref[:, cols] = jnp.dot(hidden_ref[...], down, preferred_element_type=jnp.float32)
-        return 0
-
-    lax.fori_loop(0, width // step, body, 0)
-
-
-def most_call(ids, own, other, combine, late, stacked):
-    unit = late[0].shape[0] // 2
-    half, width = own.shape
-    hidden = stacked[2].shape[0] + len(late) * unit
-    operands = [ids, own, other, *combine, *late, *stacked]
-    return pl.pallas_call(
-        lambda *refs: most_kernel(len(late), unit, *refs),
-        out_shape=pltpu.VMEM((2 * half, width), jnp.float32),
-        in_specs=specs(SMEM, 1)
-        + specs(HBM, 2)
-        + specs(VMEM, 2)
-        + specs(HBM, len(late))
-        + specs(VMEM, 5),
-        out_specs=pl.BlockSpec(memory_space=VMEM),
-        scratch_shapes=[
-            pltpu.VMEM((2 * half, width), jnp.bfloat16),
-            pltpu.VMEM((2 * unit * len(late), width), jnp.bfloat16),
-            pltpu.VMEM((2 * half, hidden), jnp.bfloat16),
-            pltpu.SemaphoreType.DMA((2 + len(late),)),
-        ],
-        cost_estimate=pl.CostEstimate(
-            flops=2 * 2 * half * width * 3 * hidden,
-            bytes_accessed=16 * MIB,
-            transcendentals=2 * half * hidden,
-        ),
-        compiler_params=pltpu.CompilerParams(vmem_limit_bytes=14 * MIB),
-        name="experts_most",
-    )(*operands)
-
-
-def rest_kernel(unit, ids_ref, one_ref, two_ref, near_ref, far_ref, gate_ref, up_ref, down_ref, most_ref, own_ref, send_ref, x_ref, both_ref, d_ref, sem):
-    half = one_ref.shape[0]
+    cut = low_ref.shape[0]
     copies = grouped(
         [
             pltpu.make_async_copy(one_ref, x_ref.at[pl.ds(0, half)], sem.at[0]),
             pltpu.make_async_copy(two_ref, x_ref.at[pl.ds(half, half)], sem.at[1]),
-            pltpu.make_async_copy(up_ref, both_ref.at[pl.ds(unit, unit)], sem.at[2]),
-            pltpu.make_async_copy(down_ref, d_ref, sem.at[3]),
+            pltpu.make_async_copy(low_ref, late_ref.at[pl.ds(0, cut)], sem.at[2]),
+            pltpu.make_async_copy(high_ref, late_ref.at[pl.ds(cut, high_ref.shape[0])], sem.at[3]),
         ]
     )
-    used = gate_ref.shape[0] - unit
-    both_ref[:unit] = gate_ref[used:]
-    for copy in copies[:3]:
+    for copy in copies:
         copy.wait()
-    both = dot_nt(x_ref[...], both_ref[...])
-    gate, up = both[:, :unit], both[:, unit:]
+    x = x_ref[...]
+    gate = dot_nt(x, gate_ref[...])
+    up = dot_nt(x, jnp.concatenate([up_ref[...], late_ref[...]], axis=0))
+    count = gate.shape[1] // unit
     combine = jnp.concatenate([near_ref[...], far_ref[...]], axis=0)
-    scale = spread(ids_ref, combine, used // unit, 1, unit)
-    hidden = (silu(gate) * up * scale).astype(jnp.bfloat16)
-    copies[3].wait()
-    width = most_ref.shape[1]
-    step = math.gcd(width, 512)
-
-    def body(at, _):
-        cols = pl.ds(pl.multiple_of(at * step, step), step)
-        out = most_ref[:, cols] + jnp.dot(
-            hidden, d_ref[:, cols], preferred_element_type=jnp.float32
-        )
-        own_ref[:, cols] = out[:half]
-        send_ref[:, cols] = out[half:].astype(jnp.bfloat16)
-        return 0
-
-    lax.fori_loop(0, width // step, body, 0)
-
-
-def rest_call(ids, own, other, combine, gate, up, down, most):
-    unit = up.shape[0]
+    hidden = silu(gate) * up * spread(ids_ref, combine, count, unit)
+    gate = jnp.dot(x, sg_ref[...], preferred_element_type=jnp.float32)
+    up = jnp.dot(x, su_ref[...], preferred_element_type=jnp.float32)
+    wide = gate.shape[1]
+    out_ref[:, :wide] = (silu(gate) * up).astype(jnp.bfloat16)
+    out_ref[:, wide:] = hidden.astype(jnp.bfloat16)
+
+
+def hidden_call(ids, own, other, combine, low, high, gate, up, s_gate, s_up, unit):
     half, width = own.shape
+    total = s_gate.shape[1] + up.shape[0] + unit
     return pl.pallas_call(
-        lambda *refs: rest_kernel(unit, *refs),
-        out_shape=[
-            pltpu.VMEM((half, width), jnp.float32),
-            jax.ShapeDtypeStruct((half, width), jnp.bfloat16),
-        ],
-        in_specs=specs(SMEM, 1)
-        + specs(HBM, 2)
-        + specs(VMEM, 3)
-        + specs(HBM, 2)
-        + specs(VMEM, 1),
-        out_specs=specs(VMEM, 2),
+        lambda *refs: hidden_kernel(unit, *refs),
+        out_shape=pltpu.VMEM((2 * half, total), jnp.bfloat16),
+        in_specs=specs(SMEM, 1) + specs(HBM, 2) + specs(VMEM, 2) + specs(HBM, 2) + specs(VMEM, 4),
+        out_specs=pl.BlockSpec(memory_space=VMEM),
         scratch_shapes=[
             pltpu.VMEM((2 * half, width), jnp.bfloat16),
-            pltpu.VMEM((2 * unit, width), jnp.bfloat16),
             pltpu.VMEM((unit, width), jnp.bfloat16),
             pltpu.SemaphoreType.DMA((4,)),
         ],
         cost_estimate=pl.CostEstimate(
-            flops=2 * 2 * half * width * 3 * unit,
-            bytes_accessed=10 * MIB,
-            transcendentals=2 * half * unit,
+            flops=2 * 2 * half * width * 2 * total,
+            bytes_accessed=12 * MIB,
+            transcendentals=2 * half * total,
         ),
         compiler_params=pltpu.CompilerParams(vmem_limit_bytes=10 * MIB),
-        name="experts_rest",
-    )(ids, own, other, *combine, gate, up, down, most)
+        name="hidden",
+    )(ids, own, other, *combine, low, high, gate, up, s_gate, s_up)
+
+
+def down_kernel(first, hidden_ref, most_ref, low_ref, high_ref, own_ref, send_ref, late_ref, sem):
+    half, width = own_ref.shape
+    rows = low_ref.shape[0]
+    copies = grouped(
+        [
+            pltpu.make_async_copy(
+                ref.at[:, pl.ds(first, width)], late_ref.at[pl.ds(at * rows, rows)], sem.at[at]
+            )
+            for at, ref in enumerate((low_ref, high_ref))
+        ]
+    )
+    for copy in copies:
+        copy.wait()
+    step = math.gcd(width, 512)
+    for at in range(0, width, step):
+        down = jnp.concatenate(
+            [most_ref[:, first + at : first + at + step], late_ref[:, at : at + step]], axis=0
+        )
+        out = jnp.dot(hidden_ref[...], down, preferred_element_type=jnp.float32)
+        own_ref[:, at : at + step] = out[:half]
+        send_ref[:, at : at + step] = out[half:].astype(jnp.bfloat16)
+
+
+def down_call(hidden, most, low, high, first, width):
+    rows = hidden.shape[0]
+    return pl.pallas_call(
+        lambda *refs: down_kernel(first, *refs),
+        out_shape=[
+            pltpu.VMEM((rows // 2, width), jnp.float32),
+            jax.ShapeDtypeStruct((rows // 2, width), jnp.bfloat16),
+        ],
+        in_specs=specs(VMEM, 2) + specs(HBM, 2),
+        out_specs=specs(VMEM, 2),
+        scratch_shapes=[
+            pltpu.VMEM((2 * low.shape[0], width), jnp.bfloat16),
+            pltpu.SemaphoreType.DMA((2,)),
+        ],
+        cost_estimate=pl.CostEstimate(
+            flops=2 * rows * width * hidden.shape[1], bytes_accessed=8 * MIB, transcendentals=0
+        ),
+        compiler_params=pltpu.CompilerParams(vmem_limit_bytes=6 * MIB),
+    )(hidden, most, low, high)
+
+
+def final_kernel(resid_ref, *refs):
+    out_ref, met, sem = refs[-3:]
+    parts = refs[: -3]
+    count = len(parts) // 2
+    rows = out_ref.shape[0]
+    width = met.shape[2]
+    copies = grouped(
+        [
+            pltpu.make_async_copy(parts[2 * at + 1], met.at[at], sem.at[at])
+            for at in range(count)
+        ]
+    )
+    for at in range(count):
+        copies[at].wait()
+        cols = slice(at * width, (at + 1) * width)
+        total = resid_ref[:rows, cols].astype(jnp.float32) + parts[2 * at][:rows]
+        out_ref[:, cols] = (total + met[at].astype(jnp.float32)).astype(jnp.bfloat16)
+
+
+def final_call(resid, parts, rows):
+    width = parts[0][1].shape[1]
+    operands = [resid] + [array for part in parts for array in part]
+    return pl.pallas_call(
+        final_kernel,
+        out_shape=jax.ShapeDtypeStruct((rows, resid.shape[1]), jnp.bfloat16),
+        in_specs=specs(VMEM, 1) + (specs(VMEM, 1) + specs(HBM, 1)) * len(parts),
+        out_specs=pl.BlockSpec(memory_space=VMEM),
+        scratch_shapes=[
+            pltpu.VMEM((len(parts), rows, width), jnp.bfloat16),
+            pltpu.SemaphoreType.DMA((len(parts),)),
+        ],
+        compiler_params=pltpu.CompilerParams(vmem_limit_bytes=6 * MIB),
+        name="final",
+    )(*operands)
 
 
 def norm_rows(resid, gain):
@@ -782,7 +781,6 @@
     mine = lax.axis_index("tp")
     seq_rows = q_first.shape[0]
     own_rows = seq_rows // members
-    experts = w_gate.shape[0] * count
     unit = w_gate.shape[2] // members
     cores = [(t, t ^ 1) for t in range(members)]
     sides = [(t, t ^ 2) for t in range(members)]
@@ -791,9 +789,10 @@
     ids = jnp.concatenate([jnp.stack([me, mine]).astype(jnp.int32), sources])
     kv = pack_call(k_first, k_second, values)
     blocks, low, high = ring_gather(kv, count)
-    gate, rest = slices_call(ids, w_gate[0], w_up[0], w_down[0], unit)
+    gate, up, down = slices_call(mine[None].astype(jnp.int32), w_gate[0], w_up[0], w_down[0], unit)
     gates, gate_low, gate_high = ring_gather(gate, count)
-    rests, rest_up, rest_down = ring_gather(rest, count)
+    ups, up_low, up_high = ring_gather(up, count)
+    downs, down_low, down_high = ring_gather(down, count)
 
     queries = (q_first, q_second)
     state = None
@@ -816,14 +815,7 @@
         stream_in,
     )
 
-    combine = jnp.sum(
-        jnp.where(
-            routes[:, :, None] == jnp.arange(experts, dtype=jnp.int32)[None, None, :],
-            route_w[:, :, None],
-            0.0,
-        ),
-        axis=1,
-    )
+    combine = combine_call(routes, route_w)
     across = swap(combine, sides)
     paired = jnp.concatenate([combine, across])
     combine = (paired, swap(paired, cores))
@@ -831,7 +823,12 @@
     met = swap(send, cores)
     pair = (own + met.astype(jnp.float32)).astype(jnp.bfloat16)
     met = swap(pair, sides)
-    stacked = stack_call([*gates, gate_low, gate_high], rests[:5], s_gate, s_up, s_down)
+    gate_all, sg, su = stack_call(
+        [whole(block) for block in (*gates, gate_low, gate_high)],
+        [whole(s_gate)],
+        [whole(s_up)],
+    )
+    (up_most,) = stack_call([whole(block) for block in ups])
     resid = (
         pair.astype(jnp.float32)
         + jnp.concatenate([met[own_rows:], met[:own_rows]]).astype(jnp.float32)
@@ -839,16 +836,21 @@
     resid = lax.optimization_barrier(resid)
     normed = norm_rows(resid, norm_gain)
     other = swap(normed, cores)
-    most = most_call(ids, normed, other, combine, rests[5:], stacked)
-    own, send = rest_call(
-        ids, normed, other, combine, stacked[0], rest_up, rest_down, most
-    )
-    met = swap(send, cores)
-    terms = own + met.astype(jnp.float32)
-    met = swap(terms[own_rows:].astype(jnp.bfloat16), sides)
-    return (
-        resid[:own_rows].astype(jnp.float32) + terms[:own_rows] + met.astype(jnp.float32)
-    ).astype(jnp.bfloat16)
+    hidden = hidden_call(
+        ids, normed, other, combine, up_low, up_high, gate_all, up_most, sg, su, unit
+    )
+    (down_most,) = stack_call([whole(s_down)] + [whole(block) for block in downs])
+    width = stream_in.shape[1] // 2
+    sums = []
+    for part in range(2):
+        sums.append(down_call(hidden, down_most, down_low, down_high, part * width, width))
+    parts = []
+    for own, send in sums:
+        met = swap(send, cores)
+        terms = own + met.astype(jnp.float32)
+        met = swap(terms[own_rows:].astype(jnp.bfloat16), sides)
+        parts.append((terms, met))
+    return final_call(resid, parts, own_rows)
 
 
 def weights_travel(count, members, seq_rows, k_first, values, w_gate):
@@ -864,6 +866,7 @@
         and w_gate.shape[2] % (32 * members) == 0
         and seq_rows % (32 * members) == 0
         and count == 8
+        and w_gate.shape[0] * count <= 128
         and gathered <= 16 * 1024 * 1024
     )
 

time: 154 us -> 142 us (0.922)
  local copies, waits for them, and re-layouts: 20.1 us -> 3.92 us
  starting transfers between devices: 30.2 us -> 37.9 us
  Pallas kernels: 24.6 us -> 19.6 us
  waiting for transfers between devices: 75.8 us -> 78.5 us
    unnamed x66 -> x32, local copies, waits for them, and re-layouts: 17.8 us -> 3.02 us
    ppermute x7 -> x9, waiting for transfers between devices: 22.2 us -> 32.8 us  [swap(): return lax.ppermute(rows, 'tp', pairs)]
    ppermute x12 -> x16, waiting for transfers between devices: 49.2 us -> 38.9 us  [ring_step(): ahead = lax.ppermute(ahead, 'sp', pairs[0])]
    ppermute x12 -> x16, starting transfers between devices: 20.3 us -> 28.9 us  [ring_step(): ahead = lax.ppermute(ahead, 'sp', pairs[0])]
    pallas_call x3 -> x8, Pallas kernels: 11.8 us -> 7.49 us  [the longest x1 3.5 us: hidden_call(): pl.pallas_call(lambda *refs: hidden_kernel(unit, *refs), out_shape=pltpu....]
    ppermute x12 -> x16, starting transfers between devices: 5.82 us -> 2.76 us  [ring_step(): back = lax.ppermute(back, 'sp', pairs[1])]
    ppermute x12 -> x16, waiting for transfers between devices: 4.36 us -> 6.78 us  [ring_step(): back = lax.ppermute(back, 'sp', pairs[1])]
    ppermute x7 -> x9, starting transfers between devices: 4.08 us -> 6.27 us  [swap(): return lax.ppermute(rows, 'tp', pairs)]
  transfers between devices with their start and end apart: 31 -> 41, of which waited for: 18 -> 27; matrix products, arithmetic and copies ran while one was open for 2% -> 2% of each run, Pallas kernels for 10% -> 8%
where the time goes in v2:
time: 142 us
  waiting for transfers between devices  78.5 us (55%)
  starting transfers between devices  37.9 us (27%)
  Pallas kernels  19.6 us (14%)
  local copies, waits for them, and re-layouts  3.92 us (3%)
  other arithmetic  1.46 us (1%)
    ppermute x16, waiting for transfers between devices, ring_step(): ahead = lax.ppermute(ahead, 'sp', pairs[0])  38.9 us
    ppermute x9, waiting for transfers between devices, swap(): return lax.ppermute(rows, 'tp', pairs)  32.8 us
    ppermute x16, starting transfers between devices, ring_step(): ahead = lax.ppermute(ahead, 'sp', pairs[0])  28.9 us
    pallas_call x4, Pallas kernels, attn_call(): pl.pallas_call(body, out_shape=out_shape, in_specs=in_specs, out_specs=sp...  7.6 us
    ppermute x16, waiting for transfers between devices, ring_step(): back = lax.ppermute(back, 'sp', pairs[1])  6.78 us
    ppermute x9, starting transfers between devices, swap(): return lax.ppermute(rows, 'tp', pairs)  6.27 us
    pallas_call x1, Pallas kernels, hidden_call(): pl.pallas_call(lambda *refs: hidden_kernel(unit, *refs), out_shape=pltpu....  3.5 us
    unnamed x32, local copies, waits for them, and re-layouts  3.02 us
  transfers between devices with their start and end apart: 41, of which 27 were waited for; matrix products, arithmetic and copies ran while one was open for 2% of the time, Pallas kernels for 8%

profile of v2, /device:TPU:0, one launch (start us, length us, event | category | flops | bytes accessed | tf_op | source)
XLA Modules:
  0.0 142.0 jit_solution(17046380567771485749)
XLA Ops:
  0.0 1.7 %pack.1.refs_3_ = bf16[256,512]{1,0:T(8,128)(2,1)} custom-call(bf16[256,128]{1,0:T(8,128)(2,1)} %one_ref.1, bf16[256,128]{1,0:T(8,128)(2,1)} %two_ref.1, bf16[256,256]{1,0:T(8,128)(2,1)} %three_ref.1), custom_call_target="tpu_custom_call" | custom-call | tf_op jit(solution)/shard_map/pack/pallas_call | solution.py:479
  1.7 3.1 %collective-permute-start = (bf16[256,512]{1,0:T(8,128)(2,1)}, bf16[256,512]{1,0:T(8,128)(2,1)S(1)}, u32[]{:S(2)}, u32[]{:S(2)}) collective-permute-start(bf16[256,512]{1,0:T(8,128)(2,1)} %pack.1.refs_3_), channel_id=1, source_target_pairs={{0,8},{8,16},{16,24},{24,28},{28,20},{20,12},{12,4},{4,0},{1,9},{9... | collective-permute-start | bytes 786440 | tf_op jit(solution)/shard_map/ppermute | solution.py:738
  4.8 6.5 %collective-permute-done.refs_4_ = bf16[256,512]{1,0:T(8,128)(2,1)S(1)} collective-permute-done((bf16[256,512]{1,0:T(8,128)(2,1)}, bf16[256,512]{1,0:T(8,128)(2,1)S(1)}, u32[]{:S(2)}, u32[]{:S(2)}) %collective-permute-start) | collective-permute-done | bytes 262176 | tf_op jit(solution)/shard_map/ppermute | solution.py:738
  11.3 1.8 %collective-permute-start.2 = (bf16[256,512]{1,0:T(8,128)(2,1)S(1)}, bf16[256,512]{1,0:T(8,128)(2,1)S(1)}, u32[]{:S(2)}, u32[]{:S(2)}) collective-permute-start(bf16[256,512]{1,0:T(8,128)(2,1)S(1)} %collective-permute-done.refs_4_), channel_id=1, source_target_pairs={{0,8},{8,16},{16,24},{24,28},{28,20},{20,12},{12,4},{4,0},{1,9},{9... | collective-permute-start | bytes 786440 | tf_op jit(solution)/shard_map/ppermute | solution.py:738
  13.3 5.4 %collective-permute-done.2.refs_3_ = bf16[256,512]{1,0:T(8,128)(2,1)S(1)} collective-permute-done((bf16[256,512]{1,0:T(8,128)(2,1)S(1)}, bf16[256,512]{1,0:T(8,128)(2,1)S(1)}, u32[]{:S(2)}, u32[]{:S(2)}) %collective-permute-start.2) | collective-permute-done | bytes 262176 | tf_op jit(solution)/shard_map/ppermute | solution.py:738
  18.7 1.5 %collective-permute-start.3 = (bf16[256,512]{1,0:T(8,128)(2,1)S(1)}, bf16[256,512]{1,0:T(8,128)(2,1)S(1)}, u32[]{:S(2)}, u32[]{:S(2)}) collective-permute-start(bf16[256,512]{1,0:T(8,128)(2,1)S(1)} %collective-permute-done.2.refs_3_), channel_id=1, source_target_pairs={{0,8},{8,16},{16,24},{24,28},{28,20},{20,12},{12,4},{4,0},{1,9},{9... | collective-permute-start | bytes 786440 | tf_op jit(solution)/shard_map/ppermute | solution.py:738
  21.5 0.9 copy-done.7
  22.5 0.9 copy-done.10
  23.4 0.9 copy-done.11
  24.3 1.7 %shard_map.172 = (bf16[256,256]{1,0:T(8,128)(2,1)S(1)}, bf16[256,256]{1,0:T(8,128)(2,1)S(1)}, f32[4,256,128]{2,1,0:T(8,128)S(1)}, f32[4,256,128]{2,1,0:T(8,128)S(1)}, f32[4,256,256]{2,1,0:T(8,128)S(1)}) custom-call(s32[10]{0:T(128)S(1)} %pad_add_fusion.refs_0_, bf16[256,256]{1,0:T(8,128)(2,1)S(1)} %copy-done.10, bf16[256,256]{1,0:T(8,128)(2,1)S(1)} %copy-done.11, ...), custom_call_target="tpu_custom_call" | custom-call | flops 1207959552 | bytes 4194304 | tf_op jit(solution)/shard_map/pallas_call | solution.py:449
  26.0 2.3 %collective-permute-start.4 = (bf16[128,512]{1,0:T(8,128)(2,1)S(1)}, bf16[128,512]{1,0:T(8,128)(2,1)S(1)}, u32[]{:S(2)}, u32[]{:S(2)}) collective-permute-start(bf16[128,512]{1,0:T(8,128)(2,1)S(1)} %slice.50), channel_id=1, source_target_pairs={{0,8},{8,16},{16,24},{24,28},{28,20},{20,12},{12,4},{4,0},{1,9},{9... | collective-permute-start | bytes 393224 | tf_op jit(solution)/shard_map/ppermute | solution.py:738
  28.4 0.8 shard_map.173
  29.3 0.8 shard_map.174
  30.1 1.1 collective-permute-done.4.refs_4_
  31.2 2.1 %collective-permute-done.7.refs_5_ = bf16[128,512]{1,0:T(8,128)(2,1)S(1)} collective-permute-done((bf16[128,512]{1,0:T(8,128)(2,1)S(1)}, bf16[128,512]{1,0:T(8,128)(2,1)S(1)}, u32[]{:S(2)}, u32[]{:S(2)}) %collective-permute-start.7) | collective-permute-done | bytes 131104 | tf_op jit(solution)/shard_map/ppermute | solution.py:739
  33.4 4.3 %shard_map.175 = (f32[128,4096]{1,0:T(8,128)S(1)}, bf16[128,4096]{1,0:T(8,128)(2,1)S(1)}) custom-call(s32[10]{0:T(128)S(1)} %pad_add_fusion.refs_0_, f32[2]{0:T(128)S(1)} %copy-done.8, bf16[256,256]{1,0:T(8,128)(2,1)S(1)} %get-tuple-element.28.refs_1_.refs_2_, bf16[256,256]{1,0:T(8,128)(2,1)S(1)} %get-tuple-element.29.refs_2_.refs_3_, ...), custom_call_target="tpu_custom_call" | custom-call | flops 402653184 | bytes 4194304 | tf_op jit(solution)/shard_map/pallas_call | solution.py:449
  37.7 2.6 %collective-permute-done.8 = bf16[128,4096]{1,0:T(8,128)(2,1)S(1)} collective-permute-done((bf16[128,4096]{1,0:T(8,128)(2,1)S(1)}, bf16[128,4096]{1,0:T(8,128)(2,1)S(1)}, u32[]{:S(2)}, u32[]{:S(2)}) %collective-permute-start.8) | collective-permute-done | bytes 1048608 | tf_op jit(solution)/shard_map/ppermute | solution.py:756
  40.6 1.6 %collective-permute-start.9 = (bf16[128,4096]{1,0:T(8,128)(2,1)S(1)}, bf16[128,4096]{1,0:T(8,128)(2,1)S(1)}, u32[]{:S(2)}, u32[]{:S(2)}) collective-permute-start(bf16[128,4096]{1,0:T(8,128)(2,1)S(1)} %add_convert_fusion.1), channel_id=1, source_target_pairs={{0,2},{1,3},{2,0},{3,1},{4,6},{5,7},{6,4},{7,5},{8,10},{9,11},{10,... | collective-permute-start | bytes 3145736 | tf_op jit(solution)/shard_map/ppermute | solution.py:756
  42.2 2.8 %slices.1 = (bf16[32,4096]{1,0:T(8,128)(2,1)}, bf16[32,4096]{1,0:T(8,128)(2,1)}, bf16[32,4096]{1,0:T(8,128)(2,1)}) custom-call(s32[1]{0:T(128)} %bitcast.1.refs_0_, bf16[4096,128]{1,0:T(8,128)(2,1)} %bitcast.7, bf16[4096,128]{1,0:T(8,128)(2,1)} %bitcast.8, bf16[128,4096]{1,0:T(8,128)(2,1)} %bitcast.9), custom_call_target="tpu_custom_call" | custom-call | tf_op jit(solution)/shard_map/slices/pallas_call | solution.py:507
  45.0 1.6 %collective-permute-start.21 = (bf16[32,4096]{1,0:T(8,128)(2,1)}, bf16[32,4096]{1,0:T(8,128)(2,1)S(1)}, u32[]{:S(2)}, u32[]{:S(2)}) collective-permute-start(bf16[32,4096]{1,0:T(8,128)(2,1)} %get-tuple-element.42.refs_0_), channel_id=1, source_target_pairs={{0,8},{8,16},{16,24},{24,28},{28,20},{20,12},{12,4},{4,0},{1,9},{9... | collective-permute-start | bytes 786440 | tf_op jit(solution)/shard_map/ppermute | solution.py:738
  47.1 1.9 %collective-permute-start.13 = (bf16[32,4096]{1,0:T(8,128)(2,1)}, bf16[32,4096]{1,0:T(8,128)(2,1)S(1)}, u32[]{:S(2)}, u32[]{:S(2)}) collective-permute-start(bf16[32,4096]{1,0:T(8,128)(2,1)} %get-tuple-element.41.refs_0_), channel_id=1, source_target_pairs={{0,8},{8,16},{16,24},{24,28},{28,20},{20,12},{12,4},{4,0},{1,9},{9... | collective-permute-start | bytes 786440 | tf_op jit(solution)/shard_map/ppermute | solution.py:738
  49.5 16.4 %collective-permute-done.9 = bf16[128,4096]{1,0:T(8,128)(2,1)S(1)} collective-permute-done((bf16[128,4096]{1,0:T(8,128)(2,1)S(1)}, bf16[128,4096]{1,0:T(8,128)(2,1)S(1)}, u32[]{:S(2)}, u32[]{:S(2)}) %collective-permute-start.9) | collective-permute-done | bytes 1048608 | tf_op jit(solution)/shard_map/ppermute | solution.py:756
  65.9 1.5 %collective-permute-start.11 = (f32[64,128]{1,0:T(8,128)S(1)}, f32[64,128]{1,0:T(8,128)S(1)}, u32[]{:S(2)}, u32[]{:S(2)}) collective-permute-start(f32[64,128]{1,0:T(8,128)S(1)} %combine.1), channel_id=1, source_target_pairs={{0,2},{1,3},{2,0},{3,1},{4,6},{5,7},{6,4},{7,5},{8,10},{9,11},{10,... | collective-permute-start | bytes 98312 | tf_op jit(solution)/shard_map/ppermute | solution.py:756
  68.1 1.8 %collective-permute-done.11 = f32[64,128]{1,0:T(8,128)S(1)} collective-permute-done((f32[64,128]{1,0:T(8,128)S(1)}, f32[64,128]{1,0:T(8,128)S(1)}, u32[]{:S(2)}, u32[]{:S(2)}) %collective-permute-start.11) | collective-permute-done | bytes 32800 | tf_op jit(solution)/shard_map/ppermute | solution.py:756
  69.8 1.6 %collective-permute-start.29 = (bf16[32,4096]{1,0:T(8,128)(2,1)S(1)}, bf16[32,4096]{1,0:T(8,128)(2,1)S(1)}, u32[]{:S(2)}, u32[]{:S(2)}) collective-permute-start(bf16[32,4096]{1,0:T(8,128)(2,1)S(1)} %copy-done.6), channel_id=1, source_target_pairs={{0,8},{8,16},{16,24},{24,28},{28,20},{20,12},{12,4},{4,0},{1,9},{9... | collective-permute-start | bytes 786440 | tf_op jit(solution)/shard_map/ppermute | solution.py:738
  71.9 2.0 %collective-permute-start.23 = (bf16[32,4096]{1,0:T(8,128)(2,1)S(1)}, bf16[32,4096]{1,0:T(8,128)(2,1)S(1)}, u32[]{:S(2)}, u32[]{:S(2)}) collective-permute-start(bf16[32,4096]{1,0:T(8,128)(2,1)S(1)} %collective-permute-done.21.refs_1_), channel_id=1, source_target_pairs={{0,8},{8,16},{16,24},{24,28},{28,20},{20,12},{12,4},{4,0},{1,9},{9... | collective-permute-start | bytes 786440 | tf_op jit(solution)/shard_map/ppermute | solution.py:738
  74.3 4.7 %collective-permute-done.29.refs_2_ = bf16[32,4096]{1,0:T(8,128)(2,1)S(1)} collective-permute-done((bf16[32,4096]{1,0:T(8,128)(2,1)S(1)}, bf16[32,4096]{1,0:T(8,128)(2,1)S(1)}, u32[]{:S(2)}, u32[]{:S(2)}) %collective-permute-start.29) | collective-permute-done | bytes 262176 | tf_op jit(solution)/shard_map/ppermute | solution.py:738
  79.0 1.6 %collective-permute-start.14 = (bf16[32,4096]{1,0:T(8,128)(2,1)S(1)}, bf16[32,4096]{1,0:T(8,128)(2,1)S(1)}, u32[]{:S(2)}, u32[]{:S(2)}) collective-permute-start(bf16[32,4096]{1,0:T(8,128)(2,1)S(1)} %collective-permute-done.13.refs_1_), channel_id=1, source_target_pairs={{0,8},{8,16},{16,24},{24,28},{28,20},{20,12},{12,4},{4,0},{1,9},{9... | collective-permute-start | bytes 786440 | tf_op jit(solution)/shard_map/ppermute | solution.py:738
  81.0 3.6 %collective-permute-done.23.refs_3_ = bf16[32,4096]{1,0:T(8,128)(2,1)S(1)} collective-permute-done((bf16[32,4096]{1,0:T(8,128)(2,1)S(1)}, bf16[32,4096]{1,0:T(8,128)(2,1)S(1)}, u32[]{:S(2)}, u32[]{:S(2)}) %collective-permute-start.23) | collective-permute-done | bytes 262176 | tf_op jit(solution)/shard_map/ppermute | solution.py:738
  84.6 1.6 %collective-permute-start.31 = (bf16[32,4096]{1,0:T(8,128)(2,1)S(1)}, bf16[32,4096]{1,0:T(8,128)(2,1)S(1)}, u32[]{:S(2)}, u32[]{:S(2)}) collective-permute-start(bf16[32,4096]{1,0:T(8,128)(2,1)S(1)} %collective-permute-done.29.refs_2_), channel_id=1, source_target_pairs={{0,8},{8,16},{16,24},{24,28},{28,20},{20,12},{12,4},{4,0},{1,9},{9... | collective-permute-start | bytes 786440 | tf_op jit(solution)/shard_map/ppermute | solution.py:738
  86.7 3.6 %collective-permute-done.14.refs_3_ = bf16[32,4096]{1,0:T(8,128)(2,1)S(1)} collective-permute-done((bf16[32,4096]{1,0:T(8,128)(2,1)S(1)}, bf16[32,4096]{1,0:T(8,128)(2,1)S(1)}, u32[]{:S(2)}, u32[]{:S(2)}) %collective-permute-start.14) | collective-permute-done | bytes 262176 | tf_op jit(solution)/shard_map/ppermute | solution.py:738
  90.2 1.6 %collective-permute-start.25 = (bf16[32,4096]{1,0:T(8,128)(2,1)S(1)}, bf16[32,4096]{1,0:T(8,128)(2,1)S(1)}, u32[]{:S(2)}, u32[]{:S(2)}) collective-permute-start(bf16[32,4096]{1,0:T(8,128)(2,1)S(1)} %collective-permute-done.23.refs_3_), channel_id=1, source_target_pairs={{0,8},{8,16},{16,24},{24,28},{28,20},{20,12},{12,4},{4,0},{1,9},{9... | collective-permute-start | bytes 786440 | tf_op jit(solution)/shard_map/ppermute | solution.py:738
  92.3 3.6 %collective-permute-done.31.refs_4_ = bf16[32,4096]{1,0:T(8,128)(2,1)S(1)} collective-permute-done((bf16[32,4096]{1,0:T(8,128)(2,1)S(1)}, bf16[32,4096]{1,0:T(8,128)(2,1)S(1)}, u32[]{:S(2)}, u32[]{:S(2)}) %collective-permute-start.31) | collective-permute-done | bytes 262176 | tf_op jit(solution)/shard_map/ppermute | solution.py:738
  95.9 1.6 %collective-permute-start.15 = (bf16[32,4096]{1,0:T(8,128)(2,1)S(1)}, bf16[32,4096]{1,0:T(8,128)(2,1)S(1)}, u32[]{:S(2)}, u32[]{:S(2)}) collective-permute-start(bf16[32,4096]{1,0:T(8,128)(2,1)S(1)} %collective-permute-done.14.refs_3_), channel_id=1, source_target_pairs={{0,8},{8,16},{16,24},{24,28},{28,20},{20,12},{12,4},{4,0},{1,9},{9... | collective-permute-start | bytes 786440 | tf_op jit(solution)/shard_map/ppermute | solution.py:738
  97.9 3.6 %collective-permute-done.25.refs_5_ = bf16[32,4096]{1,0:T(8,128)(2,1)S(1)} collective-permute-done((bf16[32,4096]{1,0:T(8,128)(2,1)S(1)}, bf16[32,4096]{1,0:T(8,128)(2,1)S(1)}, u32[]{:S(2)}, u32[]{:S(2)}) %collective-permute-start.25) | collective-permute-done | bytes 262176 | tf_op jit(solution)/shard_map/ppermute | solution.py:738
  101.5 1.6 %collective-permute-start.33 = (bf16[32,4096]{1,0:T(8,128)(2,1)S(1)}, bf16[32,4096]{1,0:T(8,128)(2,1)S(1)}, u32[]{:S(2)}, u32[]{:S(2)}) collective-permute-start(bf16[32,4096]{1,0:T(8,128)(2,1)S(1)} %collective-permute-done.31.refs_4_), channel_id=1, source_target_pairs={{0,8},{8,16},{16,24},{24,28},{28,20},{20,12},{12,4},{4,0},{1,9},{9... | collective-permute-start | bytes 786440 | tf_op jit(solution)/shard_map/ppermute | solution.py:738
  103.6 3.5 %collective-permute-done.15.refs_5_ = bf16[32,4096]{1,0:T(8,128)(2,1)S(1)} collective-permute-done((bf16[32,4096]{1,0:T(8,128)(2,1)S(1)}, bf16[32,4096]{1,0:T(8,128)(2,1)S(1)}, u32[]{:S(2)}, u32[]{:S(2)}) %collective-permute-start.15) | collective-permute-done | bytes 262176 | tf_op jit(solution)/shard_map/ppermute | solution.py:738
  107.1 1.6 %collective-permute-start.27 = (bf16[16,4096]{1,0:T(8,128)(2,1)S(1)}, bf16[16,4096]{1,0:T(8,128)(2,1)S(1)}, u32[]{:S(2)}, u32[]{:S(2)}) collective-permute-start(bf16[16,4096]{1,0:T(8,128)(2,1)S(1)} %slice.56), channel_id=1, source_target_pairs={{0,8},{8,16},{16,24},{24,28},{28,20},{20,12},{12,4},{4,0},{1,9},{9... | collective-permute-start | bytes 393224 | tf_op jit(solution)/shard_map/ppermute | solution.py:738
  109.4 3.3 %collective-permute-done.33.refs_6_ = bf16[32,4096]{1,0:T(8,128)(2,1)S(1)} collective-permute-done((bf16[32,4096]{1,0:T(8,128)(2,1)S(1)}, bf16[32,4096]{1,0:T(8,128)(2,1)S(1)}, u32[]{:S(2)}, u32[]{:S(2)}) %collective-permute-start.33) | collective-permute-done | bytes 262176 | tf_op jit(solution)/shard_map/ppermute | solution.py:738
  112.7 1.6 %collective-permute-start.16 = (bf16[16,4096]{1,0:T(8,128)(2,1)S(1)}, bf16[16,4096]{1,0:T(8,128)(2,1)S(1)}, u32[]{:S(2)}, u32[]{:S(2)}) collective-permute-start(bf16[16,4096]{1,0:T(8,128)(2,1)S(1)} %slice.54), channel_id=1, source_target_pairs={{0,8},{8,16},{16,24},{24,28},{28,20},{20,12},{12,4},{4,0},{1,9},{9... | collective-permute-start | bytes 393224 | tf_op jit(solution)/shard_map/ppermute | solution.py:738
  115.1 0.9 collective-permute-done.28.refs_8_
  116.0 2.0 %collective-permute-start.35 = (bf16[16,4096]{1,0:T(8,128)(2,1)S(1)}, bf16[16,4096]{1,0:T(8,128)(2,1)S(1)}, u32[]{:S(2)}, u32[]{:S(2)}) collective-permute-start(bf16[16,4096]{1,0:T(8,128)(2,1)S(1)} %slice.58), channel_id=1, source_target_pairs={{0,8},{8,16},{16,24},{24,28},{28,20},{20,12},{12,4},{4,0},{1,9},{9... | collective-permute-start | bytes 393224 | tf_op jit(solution)/shard_map/ppermute | solution.py:738
  119.6 3.5 %hidden.1.refs_0_ = bf16[256,384]{1,0:T(8,128)(2,1)S(1)} custom-call(s32[10]{0:T(128)S(1)} %pad_add_fusion.refs_0_, bf16[128,4096]{1,0:T(8,128)(2,1)S(1)} %fusion.2.refs_1_, bf16[128,4096]{1,0:T(8,128)(2,1)S(1)} %collective-permute-done.10.refs_2_, f32[128,128]{1,0:T(8,128)S(1)} %pad_maximum_fusion.refs_3_, f32[128,128]{1,0:T(8,128)S(1)} %collective-permute-done.12.refs_4_, ...), custom_call_target="tpu_custom_call" | custom-call | flops 1610612736 | bytes 12582912 | tf_op jit(solution)/shard_map/hidden/pallas_call | solution.py:630
  126.8 1.6 %collective-permute-start.40 = (bf16[64,2048]{1,0:T(8,128)(2,1)S(1)}, bf16[64,2048]{1,0:T(8,128)(2,1)S(1)}, u32[]{:S(2)}, u32[]{:S(2)}) collective-permute-start(bf16[64,2048]{1,0:T(8,128)(2,1)S(1)} %slice.64), channel_id=1, source_target_pairs={{0,2},{1,3},{2,0},{3,1},{4,6},{5,7},{6,4},{7,5},{8,10},{9,11},{10,... | collective-permute-start | bytes 786440 | tf_op jit(solution)/shard_map/ppermute | solution.py:756
  128.5 0.8 collective-permute-start.38
  129.3 6.7 %collective-permute-done.40.refs_3_ = bf16[64,2048]{1,0:T(8,128)(2,1)S(1)} collective-permute-done((bf16[64,2048]{1,0:T(8,128)(2,1)S(1)}, bf16[64,2048]{1,0:T(8,128)(2,1)S(1)}, u32[]{:S(2)}, u32[]{:S(2)}) %collective-permute-start.40) | collective-permute-done | bytes 262176 | tf_op jit(solution)/shard_map/ppermute | solution.py:756
  136.0 4.8 %collective-permute-done.38.refs_1_ = bf16[64,2048]{1,0:T(8,128)(2,1)S(1)} collective-permute-done((bf16[64,2048]{1,0:T(8,128)(2,1)S(1)}, bf16[64,2048]{1,0:T(8,128)(2,1)S(1)}, u32[]{:S(2)}, u32[]{:S(2)}) %collective-permute-start.38) | collective-permute-done | bytes 262176 | tf_op jit(solution)/shard_map/ppermute | solution.py:756
  140.8 1.0 final.1
  (101 shorter events, 13.5 us)
Async XLA Ops:
  1.7 9.6 %collective-permute-start = (bf16[256,512]{1,0:T(8,128)(2,1)}, bf16[256,512]{1,0:T(8,128)(2,1)S(1)}, u32[]{:S(2)}, u32[]{:S(2)}) collective-permute-start(bf16[256,512]{1,0:T(8,128)(2,1)} %pack.1.refs_3_), channel_id=1, source_target_pairs={{0,8},{8,16},{16,24},{24,28},{28,20},{20,12},{12,4},{4,0},{1,9},{9... | collective-permute-start | bytes 786440 | tf_op jit(solution)/shard_map/ppermute | solution.py:738
  4.8 8.3 %collective-permute-start.1 = (bf16[256,512]{1,0:T(8,128)(2,1)}, bf16[256,512]{1,0:T(8,128)(2,1)S(1)}, u32[]{:S(2)}, u32[]{:S(2)}) collective-permute-start(bf16[256,512]{1,0:T(8,128)(2,1)} %pack.1.refs_3_), channel_id=1, source_target_pairs={{8,0},{16,8},{24,16},{28,24},{20,28},{12,20},{4,12},{0,4},{9,1},{1... | collective-permute-start | bytes 786440 | tf_op jit(solution)/shard_map/ppermute | solution.py:739
  11.3 7.5 %collective-permute-start.2 = (bf16[256,512]{1,0:T(8,128)(2,1)S(1)}, bf16[256,512]{1,0:T(8,128)(2,1)S(1)}, u32[]{:S(2)}, u32[]{:S(2)}) collective-permute-start(bf16[256,512]{1,0:T(8,128)(2,1)S(1)} %collective-permute-done.refs_4_), channel_id=1, source_target_pairs={{0,8},{8,16},{16,24},{24,28},{28,20},{20,12},{12,4},{4,0},{1,9},{9... | collective-permute-start | bytes 786440 | tf_op jit(solution)/shard_map/ppermute | solution.py:738
  13.1 7.2 %collective-permute-start.5 = (bf16[256,512]{1,0:T(8,128)(2,1)S(1)}, bf16[256,512]{1,0:T(8,128)(2,1)S(1)}, u32[]{:S(2)}, u32[]{:S(2)}) collective-permute-start(bf16[256,512]{1,0:T(8,128)(2,1)S(1)} %collective-permute-done.1.refs_5_), channel_id=1, source_target_pairs={{8,0},{16,8},{24,16},{28,24},{20,28},{12,20},{4,12},{0,4},{9,1},{1... | collective-permute-start | bytes 786440 | tf_op jit(solution)/shard_map/ppermute | solution.py:739
  18.7 7.3 %collective-permute-start.3 = (bf16[256,512]{1,0:T(8,128)(2,1)S(1)}, bf16[256,512]{1,0:T(8,128)(2,1)S(1)}, u32[]{:S(2)}, u32[]{:S(2)}) collective-permute-start(bf16[256,512]{1,0:T(8,128)(2,1)S(1)} %collective-permute-done.2.refs_3_), channel_id=1, source_target_pairs={{0,8},{8,16},{16,24},{24,28},{28,20},{20,12},{12,4},{4,0},{1,9},{9... | collective-permute-start | bytes 786440 | tf_op jit(solution)/shard_map/ppermute | solution.py:738
  20.3 8.0 %collective-permute-start.6 = (bf16[256,512]{1,0:T(8,128)(2,1)S(1)}, bf16[256,512]{1,0:T(8,128)(2,1)S(1)}, u32[]{:S(2)}, u32[]{:S(2)}) collective-permute-start(bf16[256,512]{1,0:T(8,128)(2,1)S(1)} %collective-permute-done.5.refs_4_), channel_id=1, source_target_pairs={{8,0},{16,8},{24,16},{28,24},{20,28},{12,20},{4,12},{0,4},{9,1},{1... | collective-permute-start | bytes 786440 | tf_op jit(solution)/shard_map/ppermute | solution.py:739
  26.0 5.2 %collective-permute-start.4 = (bf16[128,512]{1,0:T(8,128)(2,1)S(1)}, bf16[128,512]{1,0:T(8,128)(2,1)S(1)}, u32[]{:S(2)}, u32[]{:S(2)}) collective-permute-start(bf16[128,512]{1,0:T(8,128)(2,1)S(1)} %slice.50), channel_id=1, source_target_pairs={{0,8},{8,16},{16,24},{24,28},{28,20},{20,12},{12,4},{4,0},{1,9},{9... | collective-permute-start | bytes 393224 | tf_op jit(solution)/shard_map/ppermute | solution.py:738
  28.3 5.0 %collective-permute-start.7 = (bf16[128,512]{1,0:T(8,128)(2,1)S(1)}, bf16[128,512]{1,0:T(8,128)(2,1)S(1)}, u32[]{:S(2)}, u32[]{:S(2)}) collective-permute-start(bf16[128,512]{1,0:T(8,128)(2,1)S(1)} %slice.51), channel_id=1, source_target_pairs={{8,0},{16,8},{24,16},{28,24},{20,28},{12,20},{4,12},{0,4},{9,1},{1... | collective-permute-start | bytes 393224 | tf_op jit(solution)/shard_map/ppermute | solution.py:739
  37.6 2.7 %collective-permute-start.8 = (bf16[128,4096]{1,0:T(8,128)(2,1)S(1)}, bf16[128,4096]{1,0:T(8,128)(2,1)S(1)}, u32[]{:S(2)}, u32[]{:S(2)}) collective-permute-start(bf16[128,4096]{1,0:T(8,128)(2,1)S(1)} %get-tuple-element.40), channel_id=1, source_target_pairs={{0,1},{1,0},{2,3},{3,2},{4,5},{5,4},{6,7},{7,6},{8,9},{9,8},{10,11... | collective-permute-start | bytes 3145736 | tf_op jit(solution)/shard_map/ppermute | solution.py:756
  40.6 8.5 %copy-start.13 = (s32[64,4]{0,1:T(4,128)S(1)}, s32[64,4]{0,1:T(4,128)}, u32[]{:S(2)}) copy-start(s32[64,4]{0,1:T(4,128)} %param.27) | copy-start | bytes 3076
  40.6 8.6 %copy-start.14 = (f32[64,4]{0,1:T(4,128)S(1)}, f32[64,4]{0,1:T(4,128)}, u32[]{:S(2)}) copy-start(f32[64,4]{0,1:T(4,128)} %param.28) | copy-start | bytes 3076
  40.6 25.3 %collective-permute-start.9 = (bf16[128,4096]{1,0:T(8,128)(2,1)S(1)}, bf16[128,4096]{1,0:T(8,128)(2,1)S(1)}, u32[]{:S(2)}, u32[]{:S(2)}) collective-permute-start(bf16[128,4096]{1,0:T(8,128)(2,1)S(1)} %add_convert_fusion.1), channel_id=1, source_target_pairs={{0,2},{1,3},{2,0},{3,1},{4,6},{5,7},{6,4},{7,5},{8,10},{9,11},{10,... | collective-permute-start | bytes 3145736 | tf_op jit(solution)/shard_map/ppermute | solution.py:756
  45.0 26.4 %collective-permute-start.21 = (bf16[32,4096]{1,0:T(8,128)(2,1)}, bf16[32,4096]{1,0:T(8,128)(2,1)S(1)}, u32[]{:S(2)}, u32[]{:S(2)}) collective-permute-start(bf16[32,4096]{1,0:T(8,128)(2,1)} %get-tuple-element.42.refs_0_), channel_id=1, source_target_pairs={{0,8},{8,16},{16,24},{24,28},{28,20},{20,12},{12,4},{4,0},{1,9},{9... | collective-permute-start | bytes 786440 | tf_op jit(solution)/shard_map/ppermute | solution.py:738
  46.7 25.2 %collective-permute-start.22 = (bf16[32,4096]{1,0:T(8,128)(2,1)}, bf16[32,4096]{1,0:T(8,128)(2,1)S(1)}, u32[]{:S(2)}, u32[]{:S(2)}) collective-permute-start(bf16[32,4096]{1,0:T(8,128)(2,1)} %get-tuple-element.42.refs_0_), channel_id=1, source_target_pairs={{8,0},{16,8},{24,16},{28,24},{20,28},{12,20},{4,12},{0,4},{9,1},{1... | collective-permute-start | bytes 786440 | tf_op jit(solution)/shard_map/ppermute | solution.py:739
  47.1 26.7 %collective-permute-start.13 = (bf16[32,4096]{1,0:T(8,128)(2,1)}, bf16[32,4096]{1,0:T(8,128)(2,1)S(1)}, u32[]{:S(2)}, u32[]{:S(2)}) collective-permute-start(bf16[32,4096]{1,0:T(8,128)(2,1)} %get-tuple-element.41.refs_0_), channel_id=1, source_target_pairs={{0,8},{8,16},{16,24},{24,28},{28,20},{20,12},{12,4},{4,0},{1,9},{9... | collective-permute-start | bytes 786440 | tf_op jit(solution)/shard_map/ppermute | solution.py:738
  49.0 25.2 %collective-permute-start.17 = (bf16[32,4096]{1,0:T(8,128)(2,1)}, bf16[32,4096]{1,0:T(8,128)(2,1)S(1)}, u32[]{:S(2)}, u32[]{:S(2)}) collective-permute-start(bf16[32,4096]{1,0:T(8,128)(2,1)} %get-tuple-element.41.refs_0_), channel_id=1, source_target_pairs={{8,0},{16,8},{24,16},{28,24},{20,28},{12,20},{4,12},{0,4},{9,1},{1... | collective-permute-start | bytes 786440 | tf_op jit(solution)/shard_map/ppermute | solution.py:739
  65.9 3.9 %collective-permute-start.11 = (f32[64,128]{1,0:T(8,128)S(1)}, f32[64,128]{1,0:T(8,128)S(1)}, u32[]{:S(2)}, u32[]{:S(2)}) collective-permute-start(f32[64,128]{1,0:T(8,128)S(1)} %combine.1), channel_id=1, source_target_pairs={{0,2},{1,3},{2,0},{3,1},{4,6},{5,7},{6,4},{7,5},{8,10},{9,11},{10,... | collective-permute-start | bytes 98312 | tf_op jit(solution)/shard_map/ppermute | solution.py:756
  67.8 41.4 %copy-start.9 = (bf16[32,4096]{1,0:T(8,128)(2,1)S(1)}, bf16[32,4096]{1,0:T(8,128)(2,1)}, u32[]{:S(2)}) copy-start(bf16[32,4096]{1,0:T(8,128)(2,1)} %get-tuple-element.41.refs_0_) | copy-start | bytes 786436
  69.8 9.2 %collective-permute-start.29 = (bf16[32,4096]{1,0:T(8,128)(2,1)S(1)}, bf16[32,4096]{1,0:T(8,128)(2,1)S(1)}, u32[]{:S(2)}, u32[]{:S(2)}) collective-permute-start(bf16[32,4096]{1,0:T(8,128)(2,1)S(1)} %copy-done.6), channel_id=1, source_target_pairs={{0,8},{8,16},{16,24},{24,28},{28,20},{20,12},{12,4},{4,0},{1,9},{9... | collective-permute-start | bytes 786440 | tf_op jit(solution)/shard_map/ppermute | solution.py:738
  71.4 9.5 %collective-permute-start.30 = (bf16[32,4096]{1,0:T(8,128)(2,1)S(1)}, bf16[32,4096]{1,0:T(8,128)(2,1)S(1)}, u32[]{:S(2)}, u32[]{:S(2)}) collective-permute-start(bf16[32,4096]{1,0:T(8,128)(2,1)S(1)} %copy-done.6), channel_id=1, source_target_pairs={{8,0},{16,8},{24,16},{28,24},{20,28},{12,20},{4,12},{0,4},{9,1},{1... | collective-permute-start | bytes 786440 | tf_op jit(solution)/shard_map/ppermute | solution.py:739
  71.9 12.8 %collective-permute-start.23 = (bf16[32,4096]{1,0:T(8,128)(2,1)S(1)}, bf16[32,4096]{1,0:T(8,128)(2,1)S(1)}, u32[]{:S(2)}, u32[]{:S(2)}) collective-permute-start(bf16[32,4096]{1,0:T(8,128)(2,1)S(1)} %collective-permute-done.21.refs_1_), channel_id=1, source_target_pairs={{0,8},{8,16},{16,24},{24,28},{28,20},{20,12},{12,4},{4,0},{1,9},{9... | collective-permute-start | bytes 786440 | tf_op jit(solution)/shard_map/ppermute | solution.py:738
  73.8 12.7 %collective-permute-start.24 = (bf16[32,4096]{1,0:T(8,128)(2,1)S(1)}, bf16[32,4096]{1,0:T(8,128)(2,1)S(1)}, u32[]{:S(2)}, u32[]{:S(2)}) collective-permute-start(bf16[32,4096]{1,0:T(8,128)(2,1)S(1)} %collective-permute-done.22.refs_2_), channel_id=1, source_target_pairs={{8,0},{16,8},{24,16},{28,24},{20,28},{12,20},{4,12},{0,4},{9,1},{1... | collective-permute-start | bytes 786440 | tf_op jit(solution)/shard_map/ppermute | solution.py:739
  74.2 45.4 %collective-permute-start.10 = (bf16[128,4096]{1,0:T(8,128)(2,1)S(1)}, bf16[128,4096]{1,0:T(8,128)(2,1)S(1)}, u32[]{:S(2)}, u32[]{:S(2)}) collective-permute-start(bf16[128,4096]{1,0:T(8,128)(2,1)S(1)} %fusion.2.refs_1_), channel_id=1, source_target_pairs={{0,1},{1,0},{2,3},{3,2},{4,5},{5,4},{6,7},{7,6},{8,9},{9,8},{10,11... | collective-permute-start | bytes 3145736 | tf_op jit(solution)/shard_map/ppermute | solution.py:756
  79.0 11.2 %collective-permute-start.14 = (bf16[32,4096]{1,0:T(8,128)(2,1)S(1)}, bf16[32,4096]{1,0:T(8,128)(2,1)S(1)}, u32[]{:S(2)}, u32[]{:S(2)}) collective-permute-start(bf16[32,4096]{1,0:T(8,128)(2,1)S(1)} %collective-permute-done.13.refs_1_), channel_id=1, source_target_pairs={{0,8},{8,16},{16,24},{24,28},{28,20},{20,12},{12,4},{4,0},{1,9},{9... | collective-permute-start | bytes 786440 | tf_op jit(solution)/shard_map/ppermute | solution.py:738
  80.9 11.2 %collective-permute-start.18 = (bf16[32,4096]{1,0:T(8,128)(2,1)S(1)}, bf16[32,4096]{1,0:T(8,128)(2,1)S(1)}, u32[]{:S(2)}, u32[]{:S(2)}) collective-permute-start(bf16[32,4096]{1,0:T(8,128)(2,1)S(1)} %collective-permute-done.17.refs_2_), channel_id=1, source_target_pairs={{8,0},{16,8},{24,16},{28,24},{20,28},{12,20},{4,12},{0,4},{9,1},{1... | collective-permute-start | bytes 786440 | tf_op jit(solution)/shard_map/ppermute | solution.py:739
  84.6 11.2 %collective-permute-start.31 = (bf16[32,4096]{1,0:T(8,128)(2,1)S(1)}, bf16[32,4096]{1,0:T(8,128)(2,1)S(1)}, u32[]{:S(2)}, u32[]{:S(2)}) collective-permute-start(bf16[32,4096]{1,0:T(8,128)(2,1)S(1)} %collective-permute-done.29.refs_2_), channel_id=1, source_target_pairs={{0,8},{8,16},{16,24},{24,28},{28,20},{20,12},{12,4},{4,0},{1,9},{9... | collective-permute-start | bytes 786440 | tf_op jit(solution)/shard_map/ppermute | solution.py:738
  86.6 11.2 %collective-permute-start.32 = (bf16[32,4096]{1,0:T(8,128)(2,1)S(1)}, bf16[32,4096]{1,0:T(8,128)(2,1)S(1)}, u32[]{:S(2)}, u32[]{:S(2)}) collective-permute-start(bf16[32,4096]{1,0:T(8,128)(2,1)S(1)} %collective-permute-done.30.refs_3_), channel_id=1, source_target_pairs={{8,0},{16,8},{24,16},{28,24},{20,28},{12,20},{4,12},{0,4},{9,1},{1... | collective-permute-start | bytes 786440 | tf_op jit(solution)/shard_map/ppermute | solution.py:739
  90.2 11.2 %collective-permute-start.25 = (bf16[32,4096]{1,0:T(8,128)(2,1)S(1)}, bf16[32,4096]{1,0:T(8,128)(2,1)S(1)}, u32[]{:S(2)}, u32[]{:S(2)}) collective-permute-start(bf16[32,4096]{1,0:T(8,128)(2,1)S(1)} %collective-permute-done.23.refs_3_), channel_id=1, source_target_pairs={{0,8},{8,16},{16,24},{24,28},{28,20},{20,12},{12,4},{4,0},{1,9},{9... | collective-permute-start | bytes 786440 | tf_op jit(solution)/shard_map/ppermute | solution.py:738
  92.2 11.2 %collective-permute-start.26 = (bf16[32,4096]{1,0:T(8,128)(2,1)S(1)}, bf16[32,4096]{1,0:T(8,128)(2,1)S(1)}, u32[]{:S(2)}, u32[]{:S(2)}) collective-permute-start(bf16[32,4096]{1,0:T(8,128)(2,1)S(1)} %collective-permute-done.24.refs_4_), channel_id=1, source_target_pairs={{8,0},{16,8},{24,16},{28,24},{20,28},{12,20},{4,12},{0,4},{9,1},{1... | collective-permute-start | bytes 786440 | tf_op jit(solution)/shard_map/ppermute | solution.py:739
  95.9 11.2 %collective-permute-start.15 = (bf16[32,4096]{1,0:T(8,128)(2,1)S(1)}, bf16[32,4096]{1,0:T(8,128)(2,1)S(1)}, u32[]{:S(2)}, u32[]{:S(2)}) collective-permute-start(bf16[32,4096]{1,0:T(8,128)(2,1)S(1)} %collective-permute-done.14.refs_3_), channel_id=1, source_target_pairs={{0,8},{8,16},{16,24},{24,28},{28,20},{20,12},{12,4},{4,0},{1,9},{9... | collective-permute-start | bytes 786440 | tf_op jit(solution)/shard_map/ppermute | solution.py:738
  97.8 11.2 %collective-permute-start.19 = (bf16[32,4096]{1,0:T(8,128)(2,1)S(1)}, bf16[32,4096]{1,0:T(8,128)(2,1)S(1)}, u32[]{:S(2)}, u32[]{:S(2)}) collective-permute-start(bf16[32,4096]{1,0:T(8,128)(2,1)S(1)} %collective-permute-done.18.refs_4_), channel_id=1, source_target_pairs={{8,0},{16,8},{24,16},{28,24},{20,28},{12,20},{4,12},{0,4},{9,1},{1... | collective-permute-start | bytes 786440 | tf_op jit(solution)/shard_map/ppermute | solution.py:739
  101.5 11.2 %collective-permute-start.33 = (bf16[32,4096]{1,0:T(8,128)(2,1)S(1)}, bf16[32,4096]{1,0:T(8,128)(2,1)S(1)}, u32[]{:S(2)}, u32[]{:S(2)}) collective-permute-start(bf16[32,4096]{1,0:T(8,128)(2,1)S(1)} %collective-permute-done.31.refs_4_), channel_id=1, source_target_pairs={{0,8},{8,16},{16,24},{24,28},{28,20},{20,12},{12,4},{4,0},{1,9},{9... | collective-permute-start | bytes 786440 | tf_op jit(solution)/shard_map/ppermute | solution.py:738
  103.4 11.1 %collective-permute-start.34 = (bf16[32,4096]{1,0:T(8,128)(2,1)S(1)}, bf16[32,4096]{1,0:T(8,128)(2,1)S(1)}, u32[]{:S(2)}, u32[]{:S(2)}) collective-permute-start(bf16[32,4096]{1,0:T(8,128)(2,1)S(1)} %collective-permute-done.32.refs_5_), channel_id=1, source_target_pairs={{8,0},{16,8},{24,16},{28,24},{20,28},{12,20},{4,12},{0,4},{9,1},{1... | collective-permute-start | bytes 786440 | tf_op jit(solution)/shard_map/ppermute | solution.py:739
  103.6 11.2 %copy-start.1 = (bf16[128,4096]{1,0:T(8,128)(2,1)S(1)}, bf16[128,4096]{1,0:T(8,128)(2,1)}, u32[]{:S(2)}) copy-start(bf16[128,4096]{1,0:T(8,128)(2,1)} %refs_0_.1) | copy-start | bytes 3145732
  107.1 8.0 %collective-permute-start.27 = (bf16[16,4096]{1,0:T(8,128)(2,1)S(1)}, bf16[16,4096]{1,0:T(8,128)(2,1)S(1)}, u32[]{:S(2)}, u32[]{:S(2)}) collective-permute-start(bf16[16,4096]{1,0:T(8,128)(2,1)S(1)} %slice.56), channel_id=1, source_target_pairs={{0,8},{8,16},{16,24},{24,28},{28,20},{20,12},{12,4},{4,0},{1,9},{9... | collective-permute-start | bytes 393224 | tf_op jit(solution)/shard_map/ppermute | solution.py:738
  109.0 7.0 %collective-permute-start.28 = (bf16[16,4096]{1,0:T(8,128)(2,1)S(1)}, bf16[16,4096]{1,0:T(8,128)(2,1)S(1)}, u32[]{:S(2)}, u32[]{:S(2)}) collective-permute-start(bf16[16,4096]{1,0:T(8,128)(2,1)S(1)} %slice.57), channel_id=1, source_target_pairs={{8,0},{16,8},{24,16},{28,24},{20,28},{12,20},{4,12},{0,4},{9,1},{1... | collective-permute-start | bytes 393224 | tf_op jit(solution)/shard_map/ppermute | solution.py:739
  109.4 8.7 %copy-start.2 = (bf16[4096,128]{1,0:T(8,128)(2,1)S(1)}, bf16[4096,128]{1,0:T(8,128)(2,1)}, u32[]{:S(2)}) copy-start(bf16[4096,128]{1,0:T(8,128)(2,1)} %refs_9_.3) | copy-start | bytes 3145732
  109.4 8.7 %copy-start.3 = (bf16[4096,128]{1,0:T(8,128)(2,1)S(1)}, bf16[4096,128]{1,0:T(8,128)(2,1)}, u32[]{:S(2)}) copy-start(bf16[4096,128]{1,0:T(8,128)(2,1)} %refs_10_.3) | copy-start | bytes 3145732
  109.4 8.7 %copy-start.5 = (bf16[32,4096]{1,0:T(8,128)(2,1)S(1)}, bf16[32,4096]{1,0:T(8,128)(2,1)}, u32[]{:S(2)}) copy-start(bf16[32,4096]{1,0:T(8,128)(2,1)} %get-tuple-element.42.refs_0_) | copy-start | bytes 786436
  112.7 6.2 %collective-permute-start.16 = (bf16[16,4096]{1,0:T(8,128)(2,1)S(1)}, bf16[16,4096]{1,0:T(8,128)(2,1)S(1)}, u32[]{:S(2)}, u32[]{:S(2)}) collective-permute-start(bf16[16,4096]{1,0:T(8,128)(2,1)S(1)} %slice.54), channel_id=1, source_target_pairs={{0,8},{8,16},{16,24},{24,28},{28,20},{20,12},{12,4},{4,0},{1,9},{9... | collective-permute-start | bytes 393224 | tf_op jit(solution)/shard_map/ppermute | solution.py:738
  114.5 5.1 %collective-permute-start.20 = (bf16[16,4096]{1,0:T(8,128)(2,1)S(1)}, bf16[16,4096]{1,0:T(8,128)(2,1)S(1)}, u32[]{:S(2)}, u32[]{:S(2)}) collective-permute-start(bf16[16,4096]{1,0:T(8,128)(2,1)S(1)} %slice.55), channel_id=1, source_target_pairs={{8,0},{16,8},{24,16},{28,24},{20,28},{12,20},{4,12},{0,4},{9,1},{1... | collective-permute-start | bytes 393224 | tf_op jit(solution)/shard_map/ppermute | solution.py:739
  115.1 3.7 %collective-permute-start.12 = (f32[128,128]{1,0:T(8,128)S(1)}, f32[128,128]{1,0:T(8,128)S(1)}, u32[]{:S(2)}, u32[]{:S(2)}) collective-permute-start(f32[128,128]{1,0:T(8,128)S(1)} %pad_maximum_fusion.refs_3_), channel_id=1, source_target_pairs={{0,1},{1,0},{2,3},{3,2},{4,5},{5,4},{6,7},{7,6},{8,9},{9,8},{10,11... | collective-permute-start | bytes 196616 | tf_op jit(solution)/shard_map/ppermute | solution.py:756
  116.0 7.1 %collective-permute-start.35 = (bf16[16,4096]{1,0:T(8,128)(2,1)S(1)}, bf16[16,4096]{1,0:T(8,128)(2,1)S(1)}, u32[]{:S(2)}, u32[]{:S(2)}) collective-permute-start(bf16[16,4096]{1,0:T(8,128)(2,1)S(1)} %slice.58), channel_id=1, source_target_pairs={{0,8},{8,16},{16,24},{24,28},{28,20},{20,12},{12,4},{4,0},{1,9},{9... | collective-permute-start | bytes 393224 | tf_op jit(solution)/shard_map/ppermute | solution.py:738
  118.8 5.0 %collective-permute-start.36 = (bf16[16,4096]{1,0:T(8,128)(2,1)S(1)}, bf16[16,4096]{1,0:T(8,128)(2,1)S(1)}, u32[]{:S(2)}, u32[]{:S(2)}) collective-permute-start(bf16[16,4096]{1,0:T(8,128)(2,1)S(1)} %slice.59), channel_id=1, source_target_pairs={{8,0},{16,8},{24,16},{28,24},{20,28},{12,20},{4,12},{0,4},{9,1},{1... | collective-permute-start | bytes 393224 | tf_op jit(solution)/shard_map/ppermute | solution.py:739
  124.6 2.0 %collective-permute-start.39 = (bf16[128,2048]{1,0:T(8,128)(2,1)S(1)}, bf16[128,2048]{1,0:T(8,128)(2,1)S(1)}, u32[]{:S(2)}, u32[]{:S(2)}) collective-permute-start(bf16[128,2048]{1,0:T(8,128)(2,1)S(1)} %get-tuple-element.50), channel_id=1, source_target_pairs={{0,1},{1,0},{2,3},{3,2},{4,5},{5,4},{6,7},{7,6},{8,9},{9,8},{10,11... | collective-permute-start | bytes 1572872 | tf_op jit(solution)/shard_map/ppermute | solution.py:756
  125.5 2.8 %collective-permute-start.37 = (bf16[128,2048]{1,0:T(8,128)(2,1)S(1)}, bf16[128,2048]{1,0:T(8,128)(2,1)S(1)}, u32[]{:S(2)}, u32[]{:S(2)}) collective-permute-start(bf16[128,2048]{1,0:T(8,128)(2,1)S(1)} %get-tuple-element.48), channel_id=1, source_target_pairs={{0,1},{1,0},{2,3},{3,2},{4,5},{5,4},{6,7},{7,6},{8,9},{9,8},{10,11... | collective-permute-start | bytes 1572872 | tf_op jit(solution)/shard_map/ppermute | solution.py:756
  126.8 9.2 %collective-permute-start.40 = (bf16[64,2048]{1,0:T(8,128)(2,1)S(1)}, bf16[64,2048]{1,0:T(8,128)(2,1)S(1)}, u32[]{:S(2)}, u32[]{:S(2)}) collective-permute-start(bf16[64,2048]{1,0:T(8,128)(2,1)S(1)} %slice.64), channel_id=1, source_target_pairs={{0,2},{1,3},{2,0},{3,1},{4,6},{5,7},{6,4},{7,5},{8,10},{9,11},{10,... | collective-permute-start | bytes 786440 | tf_op jit(solution)/shard_map/ppermute | solution.py:756
  128.5 12.3 %collective-permute-start.38 = (bf16[64,2048]{1,0:T(8,128)(2,1)S(1)}, bf16[64,2048]{1,0:T(8,128)(2,1)S(1)}, u32[]{:S(2)}, u32[]{:S(2)}) collective-permute-start(bf16[64,2048]{1,0:T(8,128)(2,1)S(1)} %slice.65), channel_id=1, source_target_pairs={{0,2},{1,3},{2,0},{3,1},{4,6},{5,7},{6,4},{7,5},{8,10},{9,11},{10,... | collective-permute-start | bytes 786440 | tf_op jit(solution)/shard_map/ppermute | solution.py:756
  (8 other events, 24.7 us)

commit v3 on v2

--- a/solution.py
+++ b/solution.py
@@ -241,67 +241,41 @@
     return copies
 
 
-def attn_kernel(spans, first, last, scale, own_rows, *refs):
+def attn_kernel(blocks, first, last, scale, own_rows, *refs):
     refs = list(refs)
     ids_ref = refs.pop(0)
     if last:
         lam_ref = refs.pop(0)
     q_in = [refs.pop(0), refs.pop(0)]
-    kv_in = [refs.pop(0) for _ in spans]
+    kv_in = [[refs.pop(0) for _ in range(pieces)] for _, pieces in blocks]
     if not first:
         state_in = [refs.pop(0) for _ in range(3)]
     if last:
-        w_ref, stream_ref = refs.pop(0), refs.pop(0)
-        own_ref, send_ref, m_ref, l_ref, acc_ref, mixed_ref, w, stream, w_sem = refs[:9]
-        del refs[:9]
-        load = pltpu.make_async_copy(w_ref, w, w_sem.at[0])
-        feed = pltpu.make_async_copy(stream_ref, stream, w_sem.at[1])
+        w, stream, own_ref, send_ref, m_ref, l_ref, acc_ref, mixed_ref = refs
+        q_refs = q_in
     elif first:
-        q_refs = [refs.pop(0), refs.pop(0)]
-        m_ref, l_ref, acc_ref = refs.pop(0), refs.pop(0), refs.pop(0)
+        *q_refs, m_ref, l_ref, acc_ref = refs
     else:
-        m_ref, l_ref, acc_ref = refs.pop(0), refs.pop(0), refs.pop(0)
-    kv_scratch, sem = refs
+        m_ref, l_ref, acc_ref = refs
+        q_refs = q_in
     rows = q_in[0].shape[0]
     heads = q_in[0].shape[1] // HEAD
-    parts = rows // own_rows
     me, mine = ids_ref[0], ids_ref[1]
     outs = (m_ref, l_ref, acc_ref)
-    starts = [sum(b.shape[0] for b in kv_in[:at]) for at in range(len(spans))]
-    kv_refs = [
-        kv_scratch.at[pl.ds(start, ref.shape[0])] for start, ref in zip(starts, kv_in)
-    ]
-    copies = grouped(
-        [
-            pltpu.make_async_copy(source, into, sem.at[at])
-            for at, (source, into) in enumerate(zip(kv_in, kv_refs))
-        ]
-    )
-    if last:
-        load.start()
-        feed.start()
     if first:
-        loads = grouped(
-            [
-                pltpu.make_async_copy(
-                    q_in[which].at[
-                        pl.ds(pl.multiple_of((mine ^ turn) * own_rows, own_rows), own_rows)
-                    ],
-                    q_refs[which].at[pl.ds(index * own_rows, own_rows)],
-                    sem.at[len(spans) + which * parts + index],
-                )
-                for which in range(2)
-                for index, turn in enumerate(TURNS)
-            ]
-        )
-        for copy in loads:
-            copy.wait()
-    else:
-        q_refs = q_in
-
-    def fold(kv_ref, diagonal, old_refs=outs):
-        keys = kv_ref.shape[0]
-        v = kv_ref[:, 2 * HEAD :]
+        for index, turn in enumerate(TURNS):
+            start = pl.multiple_of((mine ^ turn) * own_rows, own_rows)
+            for which in range(2):
+                q_refs[which][index * own_rows : (index + 1) * own_rows] = q_in[which][
+                    pl.ds(start, own_rows)
+                ]
+
+    def columns(kv_refs, start, stop):
+        return jnp.concatenate([ref[:, start:stop] for ref in kv_refs], axis=0)
+
+    def fold(kv_refs, diagonal, old_refs=outs):
+        keys = sum(ref.shape[0] for ref in kv_refs)
+        v = columns(kv_refs, 2 * HEAD, kv_refs[0].shape[1])
         old_m, old_l, old_acc = old_refs
         if diagonal:
             row_at = lax.broadcasted_iota(jnp.int32, (rows, keys), 0)
@@ -315,7 +289,7 @@
             for which in range(2):
                 pair = 2 * head + which
                 q = q_refs[which][:, head * HEAD : (head + 1) * HEAD]
-                k = kv_ref[:, which * HEAD : (which + 1) * HEAD]
+                k = columns(kv_refs, which * HEAD, (which + 1) * HEAD)
                 s = dot_nt(q, k)
                 if diagonal:
                     s = jnp.where(allowed, s, FLOOR)
@@ -341,26 +315,16 @@
                     fades = jnp.concatenate([fade] * (prod.shape[1] // 128), axis=1)
                     acc_ref[pair] = old_acc[pair] * fades + prod
 
-    for index, (place, pieces) in enumerate(spans):
-        copies[index].wait()
-        if pieces == 2:
-            copies[index + 1].wait()
-            kv_ref = kv_scratch.at[
-                pl.ds(starts[index], kv_in[index].shape[0] + kv_in[index + 1].shape[0])
-            ]
-        elif pieces == 0:
-            continue
-        else:
-            kv_ref = kv_refs[index]
+    for index, ((place, _), kv_refs) in enumerate(zip(blocks, kv_in)):
         if first and index == 0:
-            fold(kv_ref, True)
+            fold(kv_refs, True)
             continue
         earlier = ids_ref[2 + place] < me
         carry = not first and index == 0
 
         @pl.when(earlier)
-        def _(kv_ref=kv_ref, carry=carry):
-            fold(kv_ref, False, state_in if carry else outs)
+        def _(kv_refs=kv_refs, carry=carry):
+            fold(kv_refs, False, state_in if carry else outs)
 
         if carry:
 
@@ -368,9 +332,6 @@
             def _():
                 for into, source in zip(outs, state_in):
                     into[...] = source[...]
-
-        if pieces == 2:
-            break
 
     if last:
         for head in range(heads):
@@ -384,8 +345,6 @@
             mixed = mixed * lax.rsqrt(square + 1e-05)
             width = mixed.shape[1]
             mixed_ref[:, head * width : (head + 1) * width] = mixed.astype(jnp.bfloat16)
-        load.wait()
-        feed.wait()
         half = rows // 2
         step = math.gcd(w.shape[1], 512)
 
@@ -404,52 +363,40 @@
     return [pl.BlockSpec(memory_space=space)] * count
 
 
-def attn_call(ids, q_first, q_second, blocks, spans, state, own_rows, lam=None, w_out=None, stream_in=None):
+def attn_call(ids, q_first, q_second, blocks, state, own_rows, lam=None, w_out=None, stream_in=None):
     rows = q_first.shape[0]
     heads = q_first.shape[1] // HEAD
-    value_dim = blocks[0].shape[1] - 2 * HEAD
+    pieces = [piece for _, block in blocks for piece in block]
+    value_dim = pieces[0].shape[1] - 2 * HEAD
     first, last = state is None, w_out is not None
     states = [
         pltpu.VMEM((2 * heads, rows, 128), jnp.float32),
         pltpu.VMEM((2 * heads, rows, 128), jnp.float32),
         pltpu.VMEM((2 * heads, rows, value_dim), jnp.float32),
     ]
-    operands = [ids] + ([lam] if last else []) + [q_first, q_second, *blocks]
-    in_specs = specs(SMEM, 2 if last else 1)
-    in_specs += specs(HBM if first else VMEM, 2) + specs(HBM, len(blocks))
-    if not first:
-        operands += list(state)
-        in_specs += specs(VMEM, 3)
+    operands = [ids] + ([lam] if last else [])
+    smem = len(operands)
+    operands += [q_first, q_second, *pieces, *(() if first else state)]
     scratch = []
     if last:
         operands += [w_out, stream_in]
-        in_specs += specs(HBM, 2)
         width = w_out.shape[1]
         out_shape = [
             pltpu.VMEM((rows // 2, width), jnp.float32),
             jax.ShapeDtypeStruct((rows // 2, width), jnp.bfloat16),
         ]
-        scratch = [
-            *states,
-            pltpu.VMEM((rows, heads * value_dim), jnp.bfloat16),
-            pltpu.VMEM(w_out.shape, jnp.bfloat16),
-            pltpu.VMEM(stream_in.shape, jnp.bfloat16),
-            pltpu.SemaphoreType.DMA((2,)),
-        ]
+        scratch = [*states, pltpu.VMEM((rows, heads * value_dim), jnp.bfloat16)]
     else:
         out_shape = list(states)
         if first:
             out_shape = [pltpu.VMEM(q_first.shape, q_first.dtype)] * 2 + out_shape
-    keys = sum(b.shape[0] for b in blocks)
-    scratch += [
-        pltpu.VMEM((keys, blocks[0].shape[1]), jnp.bfloat16),
-        pltpu.SemaphoreType.DMA((len(blocks) + 2 * rows // own_rows,)),
-    ]
-    body = lambda *refs: attn_kernel(spans, first, last, HEAD**-0.5, own_rows, *refs)
+    keys = sum(piece.shape[0] for piece in pieces)
+    plan = tuple((place, len(block)) for place, block in blocks)
+    body = lambda *refs: attn_kernel(plan, first, last, HEAD**-0.5, own_rows, *refs)
     return pl.pallas_call(
         body,
         out_shape=out_shape,
-        in_specs=in_specs,
+        in_specs=specs(SMEM, smem) + specs(VMEM, len(operands) - smem),
         out_specs=specs(VMEM, len(out_shape)),
         scratch_shapes=scratch,
         cost_estimate=pl.CostEstimate(
@@ -457,7 +404,7 @@
             bytes_accessed=4 * 1024 * 1024,
             transcendentals=2 * heads * rows * keys,
         ),
-        compiler_params=pltpu.CompilerParams(vmem_limit_bytes=(22 if last else 12) * MIB),
+        compiler_params=pltpu.CompilerParams(vmem_limit_bytes=(16 if last else 10) * MIB),
     )(*operands)
 
 
@@ -478,7 +425,7 @@
     width = one.shape[1] + two.shape[1] + three.shape[1]
     return pl.pallas_call(
         pack_kernel,
-        out_shape=jax.ShapeDtypeStruct((one.shape[0], width), one.dtype),
+        out_shape=pltpu.VMEM((one.shape[0], width), one.dtype),
         in_specs=specs(HBM, 3),
         out_specs=pl.BlockSpec(memory_space=VMEM),
         scratch_shapes=[pltpu.SemaphoreType.DMA((3,))],
@@ -506,7 +453,7 @@
     width = gate.shape[0]
     return pl.pallas_call(
         lambda *refs: slices_kernel(unit, *refs),
-        out_shape=[jax.ShapeDtypeStruct((unit, width), gate.dtype)] * 3,
+        out_shape=[pltpu.VMEM((unit, width), gate.dtype)] * 3,
         in_specs=specs(SMEM, 1) + specs(HBM, 3),
         out_specs=specs(VMEM, 3),
         scratch_shapes=[
@@ -598,22 +545,11 @@
     )(*operands)
 
 
-def hidden_kernel(unit, ids_ref, one_ref, two_ref, near_ref, far_ref, low_ref, high_ref, gate_ref, up_ref, sg_ref, su_ref, out_ref, x_ref, late_ref, sem):
-    half = one_ref.shape[0]
-    cut = low_ref.shape[0]
-    copies = grouped(
-        [
-            pltpu.make_async_copy(one_ref, x_ref.at[pl.ds(0, half)], sem.at[0]),
-            pltpu.make_async_copy(two_ref, x_ref.at[pl.ds(half, half)], sem.at[1]),
-            pltpu.make_async_copy(low_ref, late_ref.at[pl.ds(0, cut)], sem.at[2]),
-            pltpu.make_async_copy(high_ref, late_ref.at[pl.ds(cut, high_ref.shape[0])], sem.at[3]),
-        ]
-    )
-    for copy in copies:
-        copy.wait()
-    x = x_ref[...]
+def hidden_kernel(unit, ids_ref, one_ref, two_ref, near_ref, far_ref, gate_ref, sg_ref, su_ref, *refs):
+    *up_refs, out_ref = refs
+    x = jnp.concatenate([one_ref[...], two_ref[...]], axis=0)
     gate = dot_nt(x, gate_ref[...])
-    up = dot_nt(x, jnp.concatenate([up_ref[...], late_ref[...]], axis=0))
+    up = dot_nt(x, jnp.concatenate([ref[...] for ref in up_refs], axis=0))
     count = gate.shape[1] // unit
     combine = jnp.concatenate([near_ref[...], far_ref[...]], axis=0)
     hidden = silu(gate) * up * spread(ids_ref, combine, count, unit)
@@ -624,53 +560,38 @@
     out_ref[:, wide:] = hidden.astype(jnp.bfloat16)
 
 
-def hidden_call(ids, own, other, combine, low, high, gate, up, s_gate, s_up, unit):
+def hidden_call(ids, own, other, combine, ups, gate, s_gate, s_up, unit):
     half, width = own.shape
-    total = s_gate.shape[1] + up.shape[0] + unit
+    total = s_gate.shape[1] + gate.shape[0]
+    operands = [ids, own, other, *combine, gate, s_gate, s_up, *ups]
     return pl.pallas_call(
         lambda *refs: hidden_kernel(unit, *refs),
         out_shape=pltpu.VMEM((2 * half, total), jnp.bfloat16),
-        in_specs=specs(SMEM, 1) + specs(HBM, 2) + specs(VMEM, 2) + specs(HBM, 2) + specs(VMEM, 4),
+        in_specs=specs(SMEM, 1) + specs(VMEM, len(operands) - 1),
         out_specs=pl.BlockSpec(memory_space=VMEM),
-        scratch_shapes=[
-            pltpu.VMEM((2 * half, width), jnp.bfloat16),
-            pltpu.VMEM((unit, width), jnp.bfloat16),
-            pltpu.SemaphoreType.DMA((4,)),
-        ],
         cost_estimate=pl.CostEstimate(
             flops=2 * 2 * half * width * 2 * total,
             bytes_accessed=12 * MIB,
             transcendentals=2 * half * total,
         ),
-        compiler_params=pltpu.CompilerParams(vmem_limit_bytes=10 * MIB),
+        compiler_params=pltpu.CompilerParams(vmem_limit_bytes=12 * MIB),
         name="hidden",
-    )(ids, own, other, *combine, low, high, gate, up, s_gate, s_up)
-
-
-def down_kernel(first, hidden_ref, most_ref, low_ref, high_ref, own_ref, send_ref, late_ref, sem):
+    )(*operands)
+
+
+def down_kernel(first, hidden_ref, *refs):
+    *down_refs, own_ref, send_ref = refs
     half, width = own_ref.shape
-    rows = low_ref.shape[0]
-    copies = grouped(
-        [
-            pltpu.make_async_copy(
-                ref.at[:, pl.ds(first, width)], late_ref.at[pl.ds(at * rows, rows)], sem.at[at]
-            )
-            for at, ref in enumerate((low_ref, high_ref))
-        ]
-    )
-    for copy in copies:
-        copy.wait()
     step = math.gcd(width, 512)
     for at in range(0, width, step):
-        down = jnp.concatenate(
-            [most_ref[:, first + at : first + at + step], late_ref[:, at : at + step]], axis=0
-        )
+        cols = slice(first + at, first + at + step)
+        down = jnp.concatenate([ref[:, cols] for ref in down_refs], axis=0)
         out = jnp.dot(hidden_ref[...], down, preferred_element_type=jnp.float32)
         own_ref[:, at : at + step] = out[:half]
         send_ref[:, at : at + step] = out[half:].astype(jnp.bfloat16)
 
 
-def down_call(hidden, most, low, high, first, width):
+def down_call(hidden, downs, first, width):
     rows = hidden.shape[0]
     return pl.pallas_call(
         lambda *refs: down_kernel(first, *refs),
@@ -678,50 +599,34 @@
             pltpu.VMEM((rows // 2, width), jnp.float32),
             jax.ShapeDtypeStruct((rows // 2, width), jnp.bfloat16),
         ],
-        in_specs=specs(VMEM, 2) + specs(HBM, 2),
+        in_specs=specs(VMEM, 1 + len(downs)),
         out_specs=specs(VMEM, 2),
-        scratch_shapes=[
-            pltpu.VMEM((2 * low.shape[0], width), jnp.bfloat16),
-            pltpu.SemaphoreType.DMA((2,)),
-        ],
         cost_estimate=pl.CostEstimate(
             flops=2 * rows * width * hidden.shape[1], bytes_accessed=8 * MIB, transcendentals=0
         ),
-        compiler_params=pltpu.CompilerParams(vmem_limit_bytes=6 * MIB),
-    )(hidden, most, low, high)
+        compiler_params=pltpu.CompilerParams(vmem_limit_bytes=10 * MIB),
+    )(hidden, *downs)
 
 
 def final_kernel(resid_ref, *refs):
-    out_ref, met, sem = refs[-3:]
-    parts = refs[: -3]
-    count = len(parts) // 2
+    *parts, out_ref = refs
     rows = out_ref.shape[0]
-    width = met.shape[2]
-    copies = grouped(
-        [
-            pltpu.make_async_copy(parts[2 * at + 1], met.at[at], sem.at[at])
-            for at in range(count)
-        ]
-    )
-    for at in range(count):
-        copies[at].wait()
+    width = parts[0].shape[1]
+    for at in range(len(parts) // 2):
         cols = slice(at * width, (at + 1) * width)
         total = resid_ref[:rows, cols].astype(jnp.float32) + parts[2 * at][:rows]
-        out_ref[:, cols] = (total + met[at].astype(jnp.float32)).astype(jnp.bfloat16)
+        out_ref[:, cols] = (total + parts[2 * at + 1][...].astype(jnp.float32)).astype(
+            jnp.bfloat16
+        )
 
 
 def final_call(resid, parts, rows):
-    width = parts[0][1].shape[1]
     operands = [resid] + [array for part in parts for array in part]
     return pl.pallas_call(
         final_kernel,
         out_shape=jax.ShapeDtypeStruct((rows, resid.shape[1]), jnp.bfloat16),
-        in_specs=specs(VMEM, 1) + (specs(VMEM, 1) + specs(HBM, 1)) * len(parts),
+        in_specs=specs(VMEM, len(operands)),
         out_specs=pl.BlockSpec(memory_space=VMEM),
-        scratch_shapes=[
-            pltpu.VMEM((len(parts), rows, width), jnp.bfloat16),
-            pltpu.SemaphoreType.DMA((len(parts),)),
-        ],
         compiler_params=pltpu.CompilerParams(vmem_limit_bytes=6 * MIB),
         name="final",
     )(*operands)
@@ -798,21 +703,18 @@
     state = None
     for step in range(1, count // 2):
         begin, end = (0 if step == 1 else 2 * step - 1), 2 * step + 1
-        spans = tuple((place, 1) for place in range(begin, end))
-        result = attn_call(ids, *queries, blocks[begin:end], spans, state, own_rows)
+        result = attn_call(
+            ids,
+            *queries,
+            [(place, [blocks[place]]) for place in range(begin, end)],
+            state,
+            own_rows,
+        )
         if step == 1:
             queries = result[:2]
         state = result[-3:]
     own, send = attn_call(
-        ids,
-        *queries,
-        [low, high],
-        ((count - 1, 2), (count - 1, 0)),
-        state,
-        own_rows,
-        head_lambda,
-        w_out,
-        stream_in,
+        ids, *queries, [(count - 1, [low, high])], state, own_rows, head_lambda, w_out, stream_in
     )
 
     combine = combine_call(routes, route_w)
@@ -828,7 +730,6 @@
         [whole(s_gate)],
         [whole(s_up)],
     )
-    (up_most,) = stack_call([whole(block) for block in ups])
     resid = (
         pair.astype(jnp.float32)
         + jnp.concatenate([met[own_rows:], met[:own_rows]]).astype(jnp.float32)
@@ -837,13 +738,13 @@
     normed = norm_rows(resid, norm_gain)
     other = swap(normed, cores)
     hidden = hidden_call(
-        ids, normed, other, combine, up_low, up_high, gate_all, up_most, sg, su, unit
-    )
-    (down_most,) = stack_call([whole(s_down)] + [whole(block) for block in downs])
+        ids, normed, other, combine, [*ups, up_low, up_high], gate_all, sg, su, unit
+    )
+    downs = [s_down, *downs, down_low, down_high]
     width = stream_in.shape[1] // 2
     sums = []
     for part in range(2):
-        sums.append(down_call(hidden, down_most, down_low, down_high, part * width, width))
+        sums.append(down_call(hidden, downs, part * width, width))
     parts = []
     for own, send in sums:
         met = swap(send, cores)

time: 142 us -> 139 us (0.979)
  Pallas kernels: 19.6 us -> 15.2 us
  waiting for transfers between devices: 78.5 us -> 81 us
    pallas_call x6, Pallas kernels: 12.1 us -> 9 us  [the longest x4 6.06 us: attn_call(): pl.pallas_call(body, out_shape=out_shape, in_specs=specs(SMEM, smem) + sp...]
    ppermute x16, waiting for transfers between devices: 6.78 us -> 8.49 us  [ring_step(): back = lax.ppermute(back, 'sp', pairs[1])]
    unnamed x32 -> x24, local copies, waits for them, and re-layouts: 3.02 us -> 2.05 us
  transfers between devices with their start and end apart: 41 -> 41, of which waited for: 27 -> 28; matrix products, arithmetic and copies ran while one was open for 2% -> 2% of each run, Pallas kernels for 8% -> 7%
where the time goes in v3:
time: 139 us
  waiting for transfers between devices  81 us (58%)
  starting transfers between devices  36.9 us (27%)
  Pallas kernels  15.2 us (11%)
  local copies, waits for them, and re-layouts  4.15 us (3%)
    ppermute x16, waiting for transfers between devices, ring_step(): ahead = lax.ppermute(ahead, 'sp', pairs[0])  39.5 us
    ppermute x9, waiting for transfers between devices, swap(): return lax.ppermute(rows, 'tp', pairs)  33 us
    ppermute x16, starting transfers between devices, ring_step(): ahead = lax.ppermute(ahead, 'sp', pairs[0])  28.1 us
    ppermute x16, waiting for transfers between devices, ring_step(): back = lax.ppermute(back, 'sp', pairs[1])  8.49 us
    pallas_call x4, Pallas kernels, attn_call(): pl.pallas_call(body, out_shape=out_shape, in_specs=specs(SMEM, smem) + sp...  6.06 us
    ppermute x9, starting transfers between devices, swap(): return lax.ppermute(rows, 'tp', pairs)  5.97 us
    pallas_call x1, Pallas kernels, hidden_call(): pl.pallas_call(lambda *refs: hidden_kernel(unit, *refs), out_shape=pltpu....  3 us
    ppermute x16, starting transfers between devices, ring_step(): back = lax.ppermute(back, 'sp', pairs[1])  2.79 us
  transfers between devices with their start and end apart: 41, of which 28 were waited for; matrix products, arithmetic and copies ran while one was open for 2% of the time, Pallas kernels for 7%

profile of v3, /device:TPU:0, one launch (start us, length us, event | category | flops | bytes accessed | tf_op | source)
XLA Modules:
  0.0 139.0 jit_solution(5584757361354893381)
XLA Ops:
  0.0 1.0 pack.1.refs_3_
  1.0 3.1 %collective-permute-start = (bf16[256,512]{1,0:T(8,128)(2,1)S(1)}, bf16[256,512]{1,0:T(8,128)(2,1)S(1)}, u32[]{:S(2)}, u32[]{:S(2)}) collective-permute-start(bf16[256,512]{1,0:T(8,128)(2,1)S(1)} %pack.1.refs_3_), channel_id=1, source_target_pairs={{0,8},{8,16},{16,24},{24,28},{28,20},{20,12},{12,4},{4,0},{1,9},{9... | collective-permute-start | bytes 786440 | tf_op jit(solution)/shard_map/ppermute | solution.py:643
  4.1 6.2 %collective-permute-done.refs_4_ = bf16[256,512]{1,0:T(8,128)(2,1)S(1)} collective-permute-done((bf16[256,512]{1,0:T(8,128)(2,1)S(1)}, bf16[256,512]{1,0:T(8,128)(2,1)S(1)}, u32[]{:S(2)}, u32[]{:S(2)}) %collective-permute-start) | collective-permute-done | bytes 262176 | tf_op jit(solution)/shard_map/ppermute | solution.py:643
  10.4 1.8 %collective-permute-start.2 = (bf16[256,512]{1,0:T(8,128)(2,1)S(1)}, bf16[256,512]{1,0:T(8,128)(2,1)S(1)}, u32[]{:S(2)}, u32[]{:S(2)}) collective-permute-start(bf16[256,512]{1,0:T(8,128)(2,1)S(1)} %collective-permute-done.refs_4_), channel_id=1, source_target_pairs={{0,8},{8,16},{16,24},{24,28},{28,20},{20,12},{12,4},{4,0},{1,9},{9... | collective-permute-start | bytes 786440 | tf_op jit(solution)/shard_map/ppermute | solution.py:643
  12.4 5.4 %collective-permute-done.2.refs_3_ = bf16[256,512]{1,0:T(8,128)(2,1)S(1)} collective-permute-done((bf16[256,512]{1,0:T(8,128)(2,1)S(1)}, bf16[256,512]{1,0:T(8,128)(2,1)S(1)}, u32[]{:S(2)}, u32[]{:S(2)}) %collective-permute-start.2) | collective-permute-done | bytes 262176 | tf_op jit(solution)/shard_map/ppermute | solution.py:643
  17.8 1.5 %collective-permute-start.3 = (bf16[256,512]{1,0:T(8,128)(2,1)S(1)}, bf16[256,512]{1,0:T(8,128)(2,1)S(1)}, u32[]{:S(2)}, u32[]{:S(2)}) collective-permute-start(bf16[256,512]{1,0:T(8,128)(2,1)S(1)} %collective-permute-done.2.refs_3_), channel_id=1, source_target_pairs={{0,8},{8,16},{16,24},{24,28},{28,20},{20,12},{12,4},{4,0},{1,9},{9... | collective-permute-start | bytes 786440 | tf_op jit(solution)/shard_map/ppermute | solution.py:643
  20.6 0.9 copy-done.6
  21.5 0.9 copy-done.7
  22.4 1.2 shard_map.172
  23.6 0.8 collective-permute-done.3.refs_3_
  24.5 1.5 %collective-permute-start.4 = (bf16[128,512]{1,0:T(8,128)(2,1)S(1)}, bf16[128,512]{1,0:T(8,128)(2,1)S(1)}, u32[]{:S(2)}, u32[]{:S(2)}) collective-permute-start(bf16[128,512]{1,0:T(8,128)(2,1)S(1)} %slice.50), channel_id=1, source_target_pairs={{0,8},{8,16},{16,24},{24,28},{28,20},{20,12},{12,4},{4,0},{1,9},{9... | collective-permute-start | bytes 393224 | tf_op jit(solution)/shard_map/ppermute | solution.py:643
  28.0 1.4 %collective-permute-done.4.refs_4_ = bf16[128,512]{1,0:T(8,128)(2,1)S(1)} collective-permute-done((bf16[128,512]{1,0:T(8,128)(2,1)S(1)}, bf16[128,512]{1,0:T(8,128)(2,1)S(1)}, u32[]{:S(2)}, u32[]{:S(2)}) %collective-permute-start.4) | collective-permute-done | bytes 131104 | tf_op jit(solution)/shard_map/ppermute | solution.py:643
  29.5 1.5 %collective-permute-done.7.refs_5_ = bf16[128,512]{1,0:T(8,128)(2,1)S(1)} collective-permute-done((bf16[128,512]{1,0:T(8,128)(2,1)S(1)}, bf16[128,512]{1,0:T(8,128)(2,1)S(1)}, u32[]{:S(2)}, u32[]{:S(2)}) %collective-permute-start.7) | collective-permute-done | bytes 131104 | tf_op jit(solution)/shard_map/ppermute | solution.py:644
  31.0 3.5 %shard_map.175 = (f32[128,4096]{1,0:T(8,128)S(1)}, bf16[128,4096]{1,0:T(8,128)(2,1)S(1)}) custom-call(s32[10]{0:T(128)S(1)} %pad_add_fusion.refs_0_, f32[2]{0:T(128)S(1)} %copy-done.5, bf16[256,256]{1,0:T(8,128)(2,1)S(1)} %get-tuple-element.28.refs_1_.refs_2_, bf16[256,256]{1,0:T(8,128)(2,1)S(1)} %get-tuple-element.29.refs_2_.refs_3_, ...), custom_call_target="tpu_custom_call" | custom-call | flops 402653184 | bytes 4194304 | tf_op jit(solution)/shard_map/pallas_call | solution.py:396
  34.6 2.6 %collective-permute-done.8 = bf16[128,4096]{1,0:T(8,128)(2,1)S(1)} collective-permute-done((bf16[128,4096]{1,0:T(8,128)(2,1)S(1)}, bf16[128,4096]{1,0:T(8,128)(2,1)S(1)}, u32[]{:S(2)}, u32[]{:S(2)}) %collective-permute-start.8) | collective-permute-done | bytes 1048608 | tf_op jit(solution)/shard_map/ppermute | solution.py:661
  37.5 1.6 %collective-permute-start.9 = (bf16[128,4096]{1,0:T(8,128)(2,1)S(1)}, bf16[128,4096]{1,0:T(8,128)(2,1)}, u32[]{:S(2)}, u32[]{:S(2)}) collective-permute-start(bf16[128,4096]{1,0:T(8,128)(2,1)S(1)} %add_convert_fusion.1), channel_id=1, source_target_pairs={{0,2},{1,3},{2,0},{3,1},{4,6},{5,7},{6,4},{7,5},{8,10},{9,11},{10,... | collective-permute-start | bytes 3145736 | tf_op jit(solution)/shard_map/ppermute | solution.py:661
  39.0 1.9 %slices.1 = (bf16[32,4096]{1,0:T(8,128)(2,1)S(1)}, bf16[32,4096]{1,0:T(8,128)(2,1)S(1)}, bf16[32,4096]{1,0:T(8,128)(2,1)S(1)}) custom-call(s32[1]{0:T(128)} %bitcast.1.refs_0_, bf16[4096,128]{1,0:T(8,128)(2,1)} %bitcast.7, bf16[4096,128]{1,0:T(8,128)(2,1)} %bitcast.8, bf16[128,4096]{1,0:T(8,128)(2,1)} %bitcast.9), custom_call_target="tpu_custom_call" | custom-call | tf_op jit(solution)/shard_map/slices/pallas_call | solution.py:454
  41.0 1.6 %collective-permute-start.13 = (bf16[32,4096]{1,0:T(8,128)(2,1)S(1)}, bf16[32,4096]{1,0:T(8,128)(2,1)S(1)}, u32[]{:S(2)}, u32[]{:S(2)}) collective-permute-start(bf16[32,4096]{1,0:T(8,128)(2,1)S(1)} %get-tuple-element.41.refs_0_), channel_id=1, source_target_pairs={{0,8},{8,16},{16,24},{24,28},{28,20},{20,12},{12,4},{4,0},{1,9},{9... | collective-permute-start | bytes 786440 | tf_op jit(solution)/shard_map/ppermute | solution.py:643
  43.1 2.0 %collective-permute-start.21 = (bf16[32,4096]{1,0:T(8,128)(2,1)S(1)}, bf16[32,4096]{1,0:T(8,128)(2,1)S(1)}, u32[]{:S(2)}, u32[]{:S(2)}) collective-permute-start(bf16[32,4096]{1,0:T(8,128)(2,1)S(1)} %get-tuple-element.45.refs_8_), channel_id=1, source_target_pairs={{0,8},{8,16},{16,24},{24,28},{28,20},{20,12},{12,4},{4,0},{1,9},{9... | collective-permute-start | bytes 786440 | tf_op jit(solution)/shard_map/ppermute | solution.py:643
  45.4 17.4 %collective-permute-done.9 = bf16[128,4096]{1,0:T(8,128)(2,1)} collective-permute-done((bf16[128,4096]{1,0:T(8,128)(2,1)S(1)}, bf16[128,4096]{1,0:T(8,128)(2,1)}, u32[]{:S(2)}, u32[]{:S(2)}) %collective-permute-start.9) | collective-permute-done | bytes 1048608 | tf_op jit(solution)/shard_map/ppermute | solution.py:661
  62.9 1.5 %collective-permute-start.11 = (f32[64,128]{1,0:T(8,128)S(1)}, f32[64,128]{1,0:T(8,128)S(1)}, u32[]{:S(2)}, u32[]{:S(2)}) collective-permute-start(f32[64,128]{1,0:T(8,128)S(1)} %combine.1), channel_id=1, source_target_pairs={{0,2},{1,3},{2,0},{3,1},{4,6},{5,7},{6,4},{7,5},{8,10},{9,11},{10,... | collective-permute-start | bytes 98312 | tf_op jit(solution)/shard_map/ppermute | solution.py:661
  64.3 1.3 fusion.3
  66.8 1.6 %collective-permute-start.29 = (bf16[32,4096]{1,0:T(8,128)(2,1)S(1)}, bf16[32,4096]{1,0:T(8,128)(2,1)S(1)}, u32[]{:S(2)}, u32[]{:S(2)}) collective-permute-start(bf16[32,4096]{1,0:T(8,128)(2,1)S(1)} %get-tuple-element.46.refs_2_), channel_id=1, source_target_pairs={{0,8},{8,16},{16,24},{24,28},{28,20},{20,12},{12,4},{4,0},{1,9},{9... | collective-permute-start | bytes 786440 | tf_op jit(solution)/shard_map/ppermute | solution.py:643
  69.2 2.1 %collective-permute-start.15 = (bf16[32,4096]{1,0:T(8,128)(2,1)S(1)}, bf16[32,4096]{1,0:T(8,128)(2,1)S(1)}, u32[]{:S(2)}, u32[]{:S(2)}) collective-permute-start(bf16[32,4096]{1,0:T(8,128)(2,1)S(1)} %collective-permute-done.13.refs_1_), channel_id=1, source_target_pairs={{0,8},{8,16},{16,24},{24,28},{28,20},{20,12},{12,4},{4,0},{1,9},{9... | collective-permute-start | bytes 786440 | tf_op jit(solution)/shard_map/ppermute | solution.py:643
  71.3 3.3 %collective-permute-done.29.refs_3_ = bf16[32,4096]{1,0:T(8,128)(2,1)S(1)} collective-permute-done((bf16[32,4096]{1,0:T(8,128)(2,1)S(1)}, bf16[32,4096]{1,0:T(8,128)(2,1)S(1)}, u32[]{:S(2)}, u32[]{:S(2)}) %collective-permute-start.29) | collective-permute-done | bytes 262176 | tf_op jit(solution)/shard_map/ppermute | solution.py:643
  74.6 1.5 %collective-permute-start.23 = (bf16[32,4096]{1,0:T(8,128)(2,1)S(1)}, bf16[32,4096]{1,0:T(8,128)(2,1)S(1)}, u32[]{:S(2)}, u32[]{:S(2)}) collective-permute-start(bf16[32,4096]{1,0:T(8,128)(2,1)S(1)} %collective-permute-done.21.refs_9_), channel_id=1, source_target_pairs={{0,8},{8,16},{16,24},{24,28},{28,20},{20,12},{12,4},{4,0},{1,9},{9... | collective-permute-start | bytes 786440 | tf_op jit(solution)/shard_map/ppermute | solution.py:643
  76.7 3.6 %collective-permute-done.15.refs_3_ = bf16[32,4096]{1,0:T(8,128)(2,1)S(1)} collective-permute-done((bf16[32,4096]{1,0:T(8,128)(2,1)S(1)}, bf16[32,4096]{1,0:T(8,128)(2,1)S(1)}, u32[]{:S(2)}, u32[]{:S(2)}) %collective-permute-start.15) | collective-permute-done | bytes 262176 | tf_op jit(solution)/shard_map/ppermute | solution.py:643
  80.3 1.5 %collective-permute-start.31 = (bf16[32,4096]{1,0:T(8,128)(2,1)S(1)}, bf16[32,4096]{1,0:T(8,128)(2,1)S(1)}, u32[]{:S(2)}, u32[]{:S(2)}) collective-permute-start(bf16[32,4096]{1,0:T(8,128)(2,1)S(1)} %collective-permute-done.29.refs_3_), channel_id=1, source_target_pairs={{0,8},{8,16},{16,24},{24,28},{28,20},{20,12},{12,4},{4,0},{1,9},{9... | collective-permute-start | bytes 786440 | tf_op jit(solution)/shard_map/ppermute | solution.py:643
  82.3 3.6 %collective-permute-done.23.refs_11_ = bf16[32,4096]{1,0:T(8,128)(2,1)S(1)} collective-permute-done((bf16[32,4096]{1,0:T(8,128)(2,1)S(1)}, bf16[32,4096]{1,0:T(8,128)(2,1)S(1)}, u32[]{:S(2)}, u32[]{:S(2)}) %collective-permute-start.23) | collective-permute-done | bytes 262176 | tf_op jit(solution)/shard_map/ppermute | solution.py:643
  85.9 1.5 %collective-permute-start.17 = (bf16[32,4096]{1,0:T(8,128)(2,1)S(1)}, bf16[32,4096]{1,0:T(8,128)(2,1)S(1)}, u32[]{:S(2)}, u32[]{:S(2)}) collective-permute-start(bf16[32,4096]{1,0:T(8,128)(2,1)S(1)} %collective-permute-done.15.refs_3_), channel_id=1, source_target_pairs={{0,8},{8,16},{16,24},{24,28},{28,20},{20,12},{12,4},{4,0},{1,9},{9... | collective-permute-start | bytes 786440 | tf_op jit(solution)/shard_map/ppermute | solution.py:643
  87.9 3.6 %collective-permute-done.31.refs_5_ = bf16[32,4096]{1,0:T(8,128)(2,1)S(1)} collective-permute-done((bf16[32,4096]{1,0:T(8,128)(2,1)S(1)}, bf16[32,4096]{1,0:T(8,128)(2,1)S(1)}, u32[]{:S(2)}, u32[]{:S(2)}) %collective-permute-start.31) | collective-permute-done | bytes 262176 | tf_op jit(solution)/shard_map/ppermute | solution.py:643
  91.5 1.5 %collective-permute-start.25 = (bf16[32,4096]{1,0:T(8,128)(2,1)S(1)}, bf16[32,4096]{1,0:T(8,128)(2,1)S(1)}, u32[]{:S(2)}, u32[]{:S(2)}) collective-permute-start(bf16[32,4096]{1,0:T(8,128)(2,1)S(1)} %collective-permute-done.23.refs_11_), channel_id=1, source_target_pairs={{0,8},{8,16},{16,24},{24,28},{28,20},{20,12},{12,4},{4,0},{1,9},{9... | collective-permute-start | bytes 786440 | tf_op jit(solution)/shard_map/ppermute | solution.py:643
  93.5 3.6 %collective-permute-done.17.refs_5_ = bf16[32,4096]{1,0:T(8,128)(2,1)S(1)} collective-permute-done((bf16[32,4096]{1,0:T(8,128)(2,1)S(1)}, bf16[32,4096]{1,0:T(8,128)(2,1)S(1)}, u32[]{:S(2)}, u32[]{:S(2)}) %collective-permute-start.17) | collective-permute-done | bytes 262176 | tf_op jit(solution)/shard_map/ppermute | solution.py:643
  97.1 1.5 %collective-permute-start.33 = (bf16[32,4096]{1,0:T(8,128)(2,1)S(1)}, bf16[32,4096]{1,0:T(8,128)(2,1)S(1)}, u32[]{:S(2)}, u32[]{:S(2)}) collective-permute-start(bf16[32,4096]{1,0:T(8,128)(2,1)S(1)} %collective-permute-done.31.refs_5_), channel_id=1, source_target_pairs={{0,8},{8,16},{16,24},{24,28},{28,20},{20,12},{12,4},{4,0},{1,9},{9... | collective-permute-start | bytes 786440 | tf_op jit(solution)/shard_map/ppermute | solution.py:643
  99.2 3.6 %collective-permute-done.25.refs_13_ = bf16[32,4096]{1,0:T(8,128)(2,1)S(1)} collective-permute-done((bf16[32,4096]{1,0:T(8,128)(2,1)S(1)}, bf16[32,4096]{1,0:T(8,128)(2,1)S(1)}, u32[]{:S(2)}, u32[]{:S(2)}) %collective-permute-start.25) | collective-permute-done | bytes 262176 | tf_op jit(solution)/shard_map/ppermute | solution.py:643
  102.7 1.5 %collective-permute-start.19 = (bf16[16,4096]{1,0:T(8,128)(2,1)S(1)}, bf16[16,4096]{1,0:T(8,128)(2,1)S(1)}, u32[]{:S(2)}, u32[]{:S(2)}) collective-permute-start(bf16[16,4096]{1,0:T(8,128)(2,1)S(1)} %slice.54), channel_id=1, source_target_pairs={{0,8},{8,16},{16,24},{24,28},{28,20},{20,12},{12,4},{4,0},{1,9},{9... | collective-permute-start | bytes 393224 | tf_op jit(solution)/shard_map/ppermute | solution.py:643
  104.8 3.6 %collective-permute-done.33.refs_7_ = bf16[32,4096]{1,0:T(8,128)(2,1)S(1)} collective-permute-done((bf16[32,4096]{1,0:T(8,128)(2,1)S(1)}, bf16[32,4096]{1,0:T(8,128)(2,1)S(1)}, u32[]{:S(2)}, u32[]{:S(2)}) %collective-permute-start.33) | collective-permute-done | bytes 262176 | tf_op jit(solution)/shard_map/ppermute | solution.py:643
  108.4 1.5 %collective-permute-start.27 = (bf16[16,4096]{1,0:T(8,128)(2,1)S(1)}, bf16[16,4096]{1,0:T(8,128)(2,1)S(1)}, u32[]{:S(2)}, u32[]{:S(2)}) collective-permute-start(bf16[16,4096]{1,0:T(8,128)(2,1)S(1)} %slice.56), channel_id=1, source_target_pairs={{0,8},{8,16},{16,24},{24,28},{28,20},{20,12},{12,4},{4,0},{1,9},{9... | collective-permute-start | bytes 393224 | tf_op jit(solution)/shard_map/ppermute | solution.py:643
  110.4 0.7 collective-permute-done.19.refs_7_
  111.2 1.8 %collective-permute-done.20.refs_8_ = bf16[16,4096]{1,0:T(8,128)(2,1)S(1)} collective-permute-done((bf16[16,4096]{1,0:T(8,128)(2,1)S(1)}, bf16[16,4096]{1,0:T(8,128)(2,1)S(1)}, u32[]{:S(2)}, u32[]{:S(2)}) %collective-permute-start.20) | collective-permute-done | bytes 131104 | tf_op jit(solution)/shard_map/ppermute | solution.py:644
  113.0 2.2 %collective-permute-start.35 = (bf16[16,4096]{1,0:T(8,128)(2,1)S(1)}, bf16[16,4096]{1,0:T(8,128)(2,1)S(1)}, u32[]{:S(2)}, u32[]{:S(2)}) collective-permute-start(bf16[16,4096]{1,0:T(8,128)(2,1)S(1)} %slice.58), channel_id=1, source_target_pairs={{0,8},{8,16},{16,24},{24,28},{28,20},{20,12},{12,4},{4,0},{1,9},{9... | collective-permute-start | bytes 393224 | tf_op jit(solution)/shard_map/ppermute | solution.py:643
  116.2 3.0 %hidden.1.refs_0_ = bf16[256,384]{1,0:T(8,128)(2,1)S(1)} custom-call(s32[10]{0:T(128)S(1)} %pad_add_fusion.refs_0_, bf16[128,4096]{1,0:T(8,128)(2,1)S(1)} %fusion.2.refs_1_, bf16[128,4096]{1,0:T(8,128)(2,1)S(1)} %collective-permute-done.10.refs_2_, f32[128,128]{1,0:T(8,128)S(1)} %pad_maximum_fusion.refs_3_, f32[128,128]{1,0:T(8,128)S(1)} %collective-permute-done.12.refs_4_, ...), custom_call_target="tpu_custom_call" | custom-call | flops 1610612736 | bytes 12582912 | tf_op jit(solution)/shard_map/hidden/pallas_call | solution.py:567
  119.2 1.9 %collective-permute-done.36.refs_10_ = bf16[16,4096]{1,0:T(8,128)(2,1)S(1)} collective-permute-done((bf16[16,4096]{1,0:T(8,128)(2,1)S(1)}, bf16[16,4096]{1,0:T(8,128)(2,1)S(1)}, u32[]{:S(2)}, u32[]{:S(2)}) %collective-permute-start.36) | collective-permute-done | bytes 131104 | tf_op jit(solution)/shard_map/ppermute | solution.py:644
  124.0 1.2 collective-permute-start.40
  125.3 1.0 collective-permute-start.38
  126.3 6.9 %collective-permute-done.40.refs_3_ = bf16[64,2048]{1,0:T(8,128)(2,1)S(1)} collective-permute-done((bf16[64,2048]{1,0:T(8,128)(2,1)S(1)}, bf16[64,2048]{1,0:T(8,128)(2,1)S(1)}, u32[]{:S(2)}, u32[]{:S(2)}) %collective-permute-start.40) | collective-permute-done | bytes 262176 | tf_op jit(solution)/shard_map/ppermute | solution.py:661
  133.2 4.8 %collective-permute-done.38.refs_1_ = bf16[64,2048]{1,0:T(8,128)(2,1)S(1)} collective-permute-done((bf16[64,2048]{1,0:T(8,128)(2,1)S(1)}, bf16[64,2048]{1,0:T(8,128)(2,1)S(1)}, u32[]{:S(2)}, u32[]{:S(2)}) %collective-permute-start.38) | collective-permute-done | bytes 262176 | tf_op jit(solution)/shard_map/ppermute | solution.py:661
  138.0 1.0 final.1
  (91 shorter events, 14.1 us)
Async XLA Ops:
  1.0 9.4 %collective-permute-start = (bf16[256,512]{1,0:T(8,128)(2,1)S(1)}, bf16[256,512]{1,0:T(8,128)(2,1)S(1)}, u32[]{:S(2)}, u32[]{:S(2)}) collective-permute-start(bf16[256,512]{1,0:T(8,128)(2,1)S(1)} %pack.1.refs_3_), channel_id=1, source_target_pairs={{0,8},{8,16},{16,24},{24,28},{28,20},{20,12},{12,4},{4,0},{1,9},{9... | collective-permute-start | bytes 786440 | tf_op jit(solution)/shard_map/ppermute | solution.py:643
  4.1 8.0 %collective-permute-start.1 = (bf16[256,512]{1,0:T(8,128)(2,1)S(1)}, bf16[256,512]{1,0:T(8,128)(2,1)S(1)}, u32[]{:S(2)}, u32[]{:S(2)}) collective-permute-start(bf16[256,512]{1,0:T(8,128)(2,1)S(1)} %pack.1.refs_3_), channel_id=1, source_target_pairs={{8,0},{16,8},{24,16},{28,24},{20,28},{12,20},{4,12},{0,4},{9,1},{1... | collective-permute-start | bytes 786440 | tf_op jit(solution)/shard_map/ppermute | solution.py:644
  10.4 7.5 %collective-permute-start.2 = (bf16[256,512]{1,0:T(8,128)(2,1)S(1)}, bf16[256,512]{1,0:T(8,128)(2,1)S(1)}, u32[]{:S(2)}, u32[]{:S(2)}) collective-permute-start(bf16[256,512]{1,0:T(8,128)(2,1)S(1)} %collective-permute-done.refs_4_), channel_id=1, source_target_pairs={{0,8},{8,16},{16,24},{24,28},{28,20},{20,12},{12,4},{4,0},{1,9},{9... | collective-permute-start | bytes 786440 | tf_op jit(solution)/shard_map/ppermute | solution.py:643
  12.2 7.2 %collective-permute-start.5 = (bf16[256,512]{1,0:T(8,128)(2,1)S(1)}, bf16[256,512]{1,0:T(8,128)(2,1)S(1)}, u32[]{:S(2)}, u32[]{:S(2)}) collective-permute-start(bf16[256,512]{1,0:T(8,128)(2,1)S(1)} %collective-permute-done.1.refs_5_), channel_id=1, source_target_pairs={{8,0},{16,8},{24,16},{28,24},{20,28},{12,20},{4,12},{0,4},{9,1},{1... | collective-permute-start | bytes 786440 | tf_op jit(solution)/shard_map/ppermute | solution.py:644
  17.8 6.6 %collective-permute-start.3 = (bf16[256,512]{1,0:T(8,128)(2,1)S(1)}, bf16[256,512]{1,0:T(8,128)(2,1)S(1)}, u32[]{:S(2)}, u32[]{:S(2)}) collective-permute-start(bf16[256,512]{1,0:T(8,128)(2,1)S(1)} %collective-permute-done.2.refs_3_), channel_id=1, source_target_pairs={{0,8},{8,16},{16,24},{24,28},{28,20},{20,12},{12,4},{4,0},{1,9},{9... | collective-permute-start | bytes 786440 | tf_op jit(solution)/shard_map/ppermute | solution.py:643
  19.4 6.6 %collective-permute-start.6 = (bf16[256,512]{1,0:T(8,128)(2,1)S(1)}, bf16[256,512]{1,0:T(8,128)(2,1)S(1)}, u32[]{:S(2)}, u32[]{:S(2)}) collective-permute-start(bf16[256,512]{1,0:T(8,128)(2,1)S(1)} %collective-permute-done.5.refs_4_), channel_id=1, source_target_pairs={{8,0},{16,8},{24,16},{28,24},{20,28},{12,20},{4,12},{0,4},{9,1},{1... | collective-permute-start | bytes 786440 | tf_op jit(solution)/shard_map/ppermute | solution.py:644
  24.5 5.0 %collective-permute-start.4 = (bf16[128,512]{1,0:T(8,128)(2,1)S(1)}, bf16[128,512]{1,0:T(8,128)(2,1)S(1)}, u32[]{:S(2)}, u32[]{:S(2)}) collective-permute-start(bf16[128,512]{1,0:T(8,128)(2,1)S(1)} %slice.50), channel_id=1, source_target_pairs={{0,8},{8,16},{16,24},{24,28},{28,20},{20,12},{12,4},{4,0},{1,9},{9... | collective-permute-start | bytes 393224 | tf_op jit(solution)/shard_map/ppermute | solution.py:643
  26.0 5.0 %collective-permute-start.7 = (bf16[128,512]{1,0:T(8,128)(2,1)S(1)}, bf16[128,512]{1,0:T(8,128)(2,1)S(1)}, u32[]{:S(2)}, u32[]{:S(2)}) collective-permute-start(bf16[128,512]{1,0:T(8,128)(2,1)S(1)} %slice.51), channel_id=1, source_target_pairs={{8,0},{16,8},{24,16},{28,24},{20,28},{12,20},{4,12},{0,4},{9,1},{1... | collective-permute-start | bytes 393224 | tf_op jit(solution)/shard_map/ppermute | solution.py:644
  26.6 4.4 %copy-start.1 = (bf16[512,4096]{1,0:T(8,128)(2,1)S(1)}, bf16[512,4096]{1,0:T(8,128)(2,1)}, u32[]{:S(2)}) copy-start(bf16[512,4096]{1,0:T(8,128)(2,1)} %refs_9_.2) | copy-start | bytes 12582916
  27.3 3.7 %copy-start.4 = (bf16[64,4096]{1,0:T(8,128)(2,1)S(1)}, bf16[64,4096]{1,0:T(8,128)(2,1)}, u32[]{:S(2)}) copy-start(bf16[64,4096]{1,0:T(8,128)(2,1)} %refs_10_.2) | copy-start | bytes 1572868
  34.5 2.7 %collective-permute-start.8 = (bf16[128,4096]{1,0:T(8,128)(2,1)S(1)}, bf16[128,4096]{1,0:T(8,128)(2,1)S(1)}, u32[]{:S(2)}, u32[]{:S(2)}) collective-permute-start(bf16[128,4096]{1,0:T(8,128)(2,1)S(1)} %get-tuple-element.40), channel_id=1, source_target_pairs={{0,1},{1,0},{2,3},{3,2},{4,5},{5,4},{6,7},{7,6},{8,9},{9,8},{10,11... | collective-permute-start | bytes 3145736 | tf_op jit(solution)/shard_map/ppermute | solution.py:661
  37.5 7.6 %copy-start.9 = (s32[64,4]{0,1:T(4,128)S(1)}, s32[64,4]{0,1:T(4,128)}, u32[]{:S(2)}) copy-start(s32[64,4]{0,1:T(4,128)} %param.27) | copy-start | bytes 3076
  37.5 7.7 %copy-start.10 = (f32[64,4]{0,1:T(4,128)S(1)}, f32[64,4]{0,1:T(4,128)}, u32[]{:S(2)}) copy-start(f32[64,4]{0,1:T(4,128)} %param.28) | copy-start | bytes 3076
  37.5 25.4 %collective-permute-start.9 = (bf16[128,4096]{1,0:T(8,128)(2,1)S(1)}, bf16[128,4096]{1,0:T(8,128)(2,1)}, u32[]{:S(2)}, u32[]{:S(2)}) collective-permute-start(bf16[128,4096]{1,0:T(8,128)(2,1)S(1)} %add_convert_fusion.1), channel_id=1, source_target_pairs={{0,2},{1,3},{2,0},{3,1},{4,6},{5,7},{6,4},{7,5},{8,10},{9,11},{10,... | collective-permute-start | bytes 3145736 | tf_op jit(solution)/shard_map/ppermute | solution.py:661
  41.0 27.4 %collective-permute-start.13 = (bf16[32,4096]{1,0:T(8,128)(2,1)S(1)}, bf16[32,4096]{1,0:T(8,128)(2,1)S(1)}, u32[]{:S(2)}, u32[]{:S(2)}) collective-permute-start(bf16[32,4096]{1,0:T(8,128)(2,1)S(1)} %get-tuple-element.41.refs_0_), channel_id=1, source_target_pairs={{0,8},{8,16},{16,24},{24,28},{28,20},{20,12},{12,4},{4,0},{1,9},{9... | collective-permute-start | bytes 786440 | tf_op jit(solution)/shard_map/ppermute | solution.py:643
  42.6 26.5 %collective-permute-start.14 = (bf16[32,4096]{1,0:T(8,128)(2,1)S(1)}, bf16[32,4096]{1,0:T(8,128)(2,1)S(1)}, u32[]{:S(2)}, u32[]{:S(2)}) collective-permute-start(bf16[32,4096]{1,0:T(8,128)(2,1)S(1)} %get-tuple-element.41.refs_0_), channel_id=1, source_target_pairs={{8,0},{16,8},{24,16},{28,24},{20,28},{12,20},{4,12},{0,4},{9,1},{1... | collective-permute-start | bytes 786440 | tf_op jit(solution)/shard_map/ppermute | solution.py:644
  43.1 26.2 %collective-permute-start.21 = (bf16[32,4096]{1,0:T(8,128)(2,1)S(1)}, bf16[32,4096]{1,0:T(8,128)(2,1)S(1)}, u32[]{:S(2)}, u32[]{:S(2)}) collective-permute-start(bf16[32,4096]{1,0:T(8,128)(2,1)S(1)} %get-tuple-element.45.refs_8_), channel_id=1, source_target_pairs={{0,8},{8,16},{16,24},{24,28},{28,20},{20,12},{12,4},{4,0},{1,9},{9... | collective-permute-start | bytes 786440 | tf_op jit(solution)/shard_map/ppermute | solution.py:643
  45.1 26.2 %collective-permute-start.22 = (bf16[32,4096]{1,0:T(8,128)(2,1)S(1)}, bf16[32,4096]{1,0:T(8,128)(2,1)S(1)}, u32[]{:S(2)}, u32[]{:S(2)}) collective-permute-start(bf16[32,4096]{1,0:T(8,128)(2,1)S(1)} %get-tuple-element.45.refs_8_), channel_id=1, source_target_pairs={{8,0},{16,8},{24,16},{28,24},{20,28},{12,20},{4,12},{0,4},{9,1},{1... | collective-permute-start | bytes 786440 | tf_op jit(solution)/shard_map/ppermute | solution.py:644
  62.9 3.9 %collective-permute-start.11 = (f32[64,128]{1,0:T(8,128)S(1)}, f32[64,128]{1,0:T(8,128)S(1)}, u32[]{:S(2)}, u32[]{:S(2)}) collective-permute-start(f32[64,128]{1,0:T(8,128)S(1)} %combine.1), channel_id=1, source_target_pairs={{0,2},{1,3},{2,0},{3,1},{4,6},{5,7},{6,4},{7,5},{8,10},{9,11},{10,... | collective-permute-start | bytes 98312 | tf_op jit(solution)/shard_map/ppermute | solution.py:661
  66.2 49.0 %copy-start.2 = (bf16[4096,128]{1,0:T(8,128)(2,1)S(1)}, bf16[4096,128]{1,0:T(8,128)(2,1)}, u32[]{:S(2)}) copy-start(bf16[4096,128]{1,0:T(8,128)(2,1)} %refs_9_.3) | copy-start | bytes 3145732
  66.2 49.0 %copy-start.3 = (bf16[4096,128]{1,0:T(8,128)(2,1)S(1)}, bf16[4096,128]{1,0:T(8,128)(2,1)}, u32[]{:S(2)}) copy-start(bf16[4096,128]{1,0:T(8,128)(2,1)} %refs_10_.3) | copy-start | bytes 3145732
  66.8 7.9 %collective-permute-start.29 = (bf16[32,4096]{1,0:T(8,128)(2,1)S(1)}, bf16[32,4096]{1,0:T(8,128)(2,1)S(1)}, u32[]{:S(2)}, u32[]{:S(2)}) collective-permute-start(bf16[32,4096]{1,0:T(8,128)(2,1)S(1)} %get-tuple-element.46.refs_2_), channel_id=1, source_target_pairs={{0,8},{8,16},{16,24},{24,28},{28,20},{20,12},{12,4},{4,0},{1,9},{9... | collective-permute-start | bytes 786440 | tf_op jit(solution)/shard_map/ppermute | solution.py:643
  68.4 8.3 %collective-permute-start.30 = (bf16[32,4096]{1,0:T(8,128)(2,1)S(1)}, bf16[32,4096]{1,0:T(8,128)(2,1)S(1)}, u32[]{:S(2)}, u32[]{:S(2)}) collective-permute-start(bf16[32,4096]{1,0:T(8,128)(2,1)S(1)} %get-tuple-element.46.refs_2_), channel_id=1, source_target_pairs={{8,0},{16,8},{24,16},{28,24},{20,28},{12,20},{4,12},{0,4},{9,1},{1... | collective-permute-start | bytes 786440 | tf_op jit(solution)/shard_map/ppermute | solution.py:644
  69.1 47.0 %collective-permute-start.10 = (bf16[128,4096]{1,0:T(8,128)(2,1)S(1)}, bf16[128,4096]{1,0:T(8,128)(2,1)S(1)}, u32[]{:S(2)}, u32[]{:S(2)}) collective-permute-start(bf16[128,4096]{1,0:T(8,128)(2,1)S(1)} %fusion.2.refs_1_), channel_id=1, source_target_pairs={{0,1},{1,0},{2,3},{3,2},{4,5},{5,4},{6,7},{7,6},{8,9},{9,8},{10,11... | collective-permute-start | bytes 3145736 | tf_op jit(solution)/shard_map/ppermute | solution.py:661
  69.2 11.0 %collective-permute-start.15 = (bf16[32,4096]{1,0:T(8,128)(2,1)S(1)}, bf16[32,4096]{1,0:T(8,128)(2,1)S(1)}, u32[]{:S(2)}, u32[]{:S(2)}) collective-permute-start(bf16[32,4096]{1,0:T(8,128)(2,1)S(1)} %collective-permute-done.13.refs_1_), channel_id=1, source_target_pairs={{0,8},{8,16},{16,24},{24,28},{28,20},{20,12},{12,4},{4,0},{1,9},{9... | collective-permute-start | bytes 786440 | tf_op jit(solution)/shard_map/ppermute | solution.py:643
  71.3 11.0 %collective-permute-start.16 = (bf16[32,4096]{1,0:T(8,128)(2,1)S(1)}, bf16[32,4096]{1,0:T(8,128)(2,1)S(1)}, u32[]{:S(2)}, u32[]{:S(2)}) collective-permute-start(bf16[32,4096]{1,0:T(8,128)(2,1)S(1)} %collective-permute-done.14.refs_2_), channel_id=1, source_target_pairs={{8,0},{16,8},{24,16},{28,24},{20,28},{12,20},{4,12},{0,4},{9,1},{1... | collective-permute-start | bytes 786440 | tf_op jit(solution)/shard_map/ppermute | solution.py:644
  74.6 11.2 %collective-permute-start.23 = (bf16[32,4096]{1,0:T(8,128)(2,1)S(1)}, bf16[32,4096]{1,0:T(8,128)(2,1)S(1)}, u32[]{:S(2)}, u32[]{:S(2)}) collective-permute-start(bf16[32,4096]{1,0:T(8,128)(2,1)S(1)} %collective-permute-done.21.refs_9_), channel_id=1, source_target_pairs={{0,8},{8,16},{16,24},{24,28},{28,20},{20,12},{12,4},{4,0},{1,9},{9... | collective-permute-start | bytes 786440 | tf_op jit(solution)/shard_map/ppermute | solution.py:643
  76.6 11.2 %collective-permute-start.24 = (bf16[32,4096]{1,0:T(8,128)(2,1)S(1)}, bf16[32,4096]{1,0:T(8,128)(2,1)S(1)}, u32[]{:S(2)}, u32[]{:S(2)}) collective-permute-start(bf16[32,4096]{1,0:T(8,128)(2,1)S(1)} %collective-permute-done.22.refs_10_), channel_id=1, source_target_pairs={{8,0},{16,8},{24,16},{28,24},{20,28},{12,20},{4,12},{0,4},{9,1},{1... | collective-permute-start | bytes 786440 | tf_op jit(solution)/shard_map/ppermute | solution.py:644
  80.3 11.2 %collective-permute-start.31 = (bf16[32,4096]{1,0:T(8,128)(2,1)S(1)}, bf16[32,4096]{1,0:T(8,128)(2,1)S(1)}, u32[]{:S(2)}, u32[]{:S(2)}) collective-permute-start(bf16[32,4096]{1,0:T(8,128)(2,1)S(1)} %collective-permute-done.29.refs_3_), channel_id=1, source_target_pairs={{0,8},{8,16},{16,24},{24,28},{28,20},{20,12},{12,4},{4,0},{1,9},{9... | collective-permute-start | bytes 786440 | tf_op jit(solution)/shard_map/ppermute | solution.py:643
  82.3 11.2 %collective-permute-start.32 = (bf16[32,4096]{1,0:T(8,128)(2,1)S(1)}, bf16[32,4096]{1,0:T(8,128)(2,1)S(1)}, u32[]{:S(2)}, u32[]{:S(2)}) collective-permute-start(bf16[32,4096]{1,0:T(8,128)(2,1)S(1)} %collective-permute-done.30.refs_4_), channel_id=1, source_target_pairs={{8,0},{16,8},{24,16},{28,24},{20,28},{12,20},{4,12},{0,4},{9,1},{1... | collective-permute-start | bytes 786440 | tf_op jit(solution)/shard_map/ppermute | solution.py:644
  85.9 11.2 %collective-permute-start.17 = (bf16[32,4096]{1,0:T(8,128)(2,1)S(1)}, bf16[32,4096]{1,0:T(8,128)(2,1)S(1)}, u32[]{:S(2)}, u32[]{:S(2)}) collective-permute-start(bf16[32,4096]{1,0:T(8,128)(2,1)S(1)} %collective-permute-done.15.refs_3_), channel_id=1, source_target_pairs={{0,8},{8,16},{16,24},{24,28},{28,20},{20,12},{12,4},{4,0},{1,9},{9... | collective-permute-start | bytes 786440 | tf_op jit(solution)/shard_map/ppermute | solution.py:643
  87.9 11.2 %collective-permute-start.18 = (bf16[32,4096]{1,0:T(8,128)(2,1)S(1)}, bf16[32,4096]{1,0:T(8,128)(2,1)S(1)}, u32[]{:S(2)}, u32[]{:S(2)}) collective-permute-start(bf16[32,4096]{1,0:T(8,128)(2,1)S(1)} %collective-permute-done.16.refs_4_), channel_id=1, source_target_pairs={{8,0},{16,8},{24,16},{28,24},{20,28},{12,20},{4,12},{0,4},{9,1},{1... | collective-permute-start | bytes 786440 | tf_op jit(solution)/shard_map/ppermute | solution.py:644
  91.5 11.2 %collective-permute-start.25 = (bf16[32,4096]{1,0:T(8,128)(2,1)S(1)}, bf16[32,4096]{1,0:T(8,128)(2,1)S(1)}, u32[]{:S(2)}, u32[]{:S(2)}) collective-permute-start(bf16[32,4096]{1,0:T(8,128)(2,1)S(1)} %collective-permute-done.23.refs_11_), channel_id=1, source_target_pairs={{0,8},{8,16},{16,24},{24,28},{28,20},{20,12},{12,4},{4,0},{1,9},{9... | collective-permute-start | bytes 786440 | tf_op jit(solution)/shard_map/ppermute | solution.py:643
  93.5 11.2 %collective-permute-start.26 = (bf16[32,4096]{1,0:T(8,128)(2,1)S(1)}, bf16[32,4096]{1,0:T(8,128)(2,1)S(1)}, u32[]{:S(2)}, u32[]{:S(2)}) collective-permute-start(bf16[32,4096]{1,0:T(8,128)(2,1)S(1)} %collective-permute-done.24.refs_12_), channel_id=1, source_target_pairs={{8,0},{16,8},{24,16},{28,24},{20,28},{12,20},{4,12},{0,4},{9,1},{1... | collective-permute-start | bytes 786440 | tf_op jit(solution)/shard_map/ppermute | solution.py:644
  97.1 11.2 %collective-permute-start.33 = (bf16[32,4096]{1,0:T(8,128)(2,1)S(1)}, bf16[32,4096]{1,0:T(8,128)(2,1)S(1)}, u32[]{:S(2)}, u32[]{:S(2)}) collective-permute-start(bf16[32,4096]{1,0:T(8,128)(2,1)S(1)} %collective-permute-done.31.refs_5_), channel_id=1, source_target_pairs={{0,8},{8,16},{16,24},{24,28},{28,20},{20,12},{12,4},{4,0},{1,9},{9... | collective-permute-start | bytes 786440 | tf_op jit(solution)/shard_map/ppermute | solution.py:643
  99.1 11.2 %collective-permute-start.34 = (bf16[32,4096]{1,0:T(8,128)(2,1)S(1)}, bf16[32,4096]{1,0:T(8,128)(2,1)S(1)}, u32[]{:S(2)}, u32[]{:S(2)}) collective-permute-start(bf16[32,4096]{1,0:T(8,128)(2,1)S(1)} %collective-permute-done.32.refs_6_), channel_id=1, source_target_pairs={{8,0},{16,8},{24,16},{28,24},{20,28},{12,20},{4,12},{0,4},{9,1},{1... | collective-permute-start | bytes 786440 | tf_op jit(solution)/shard_map/ppermute | solution.py:644
  102.7 8.4 %collective-permute-start.19 = (bf16[16,4096]{1,0:T(8,128)(2,1)S(1)}, bf16[16,4096]{1,0:T(8,128)(2,1)S(1)}, u32[]{:S(2)}, u32[]{:S(2)}) collective-permute-start(bf16[16,4096]{1,0:T(8,128)(2,1)S(1)} %slice.54), channel_id=1, source_target_pairs={{0,8},{8,16},{16,24},{24,28},{28,20},{20,12},{12,4},{4,0},{1,9},{9... | collective-permute-start | bytes 393224 | tf_op jit(solution)/shard_map/ppermute | solution.py:643
  104.7 8.3 %collective-permute-start.20 = (bf16[16,4096]{1,0:T(8,128)(2,1)S(1)}, bf16[16,4096]{1,0:T(8,128)(2,1)S(1)}, u32[]{:S(2)}, u32[]{:S(2)}) collective-permute-start(bf16[16,4096]{1,0:T(8,128)(2,1)S(1)} %slice.55), channel_id=1, source_target_pairs={{8,0},{16,8},{24,16},{28,24},{20,28},{12,20},{4,12},{0,4},{9,1},{1... | collective-permute-start | bytes 393224 | tf_op jit(solution)/shard_map/ppermute | solution.py:644
  108.4 7.8 %collective-permute-start.27 = (bf16[16,4096]{1,0:T(8,128)(2,1)S(1)}, bf16[16,4096]{1,0:T(8,128)(2,1)S(1)}, u32[]{:S(2)}, u32[]{:S(2)}) collective-permute-start(bf16[16,4096]{1,0:T(8,128)(2,1)S(1)} %slice.56), channel_id=1, source_target_pairs={{0,8},{8,16},{16,24},{24,28},{28,20},{20,12},{12,4},{4,0},{1,9},{9... | collective-permute-start | bytes 393224 | tf_op jit(solution)/shard_map/ppermute | solution.py:643
  110.4 5.8 %collective-permute-start.28 = (bf16[16,4096]{1,0:T(8,128)(2,1)S(1)}, bf16[16,4096]{1,0:T(8,128)(2,1)S(1)}, u32[]{:S(2)}, u32[]{:S(2)}) collective-permute-start(bf16[16,4096]{1,0:T(8,128)(2,1)S(1)} %slice.57), channel_id=1, source_target_pairs={{8,0},{16,8},{24,16},{28,24},{20,28},{12,20},{4,12},{0,4},{9,1},{1... | collective-permute-start | bytes 393224 | tf_op jit(solution)/shard_map/ppermute | solution.py:644
  111.2 4.8 %collective-permute-start.12 = (f32[128,128]{1,0:T(8,128)S(1)}, f32[128,128]{1,0:T(8,128)S(1)}, u32[]{:S(2)}, u32[]{:S(2)}) collective-permute-start(f32[128,128]{1,0:T(8,128)S(1)} %pad_maximum_fusion.refs_3_), channel_id=1, source_target_pairs={{0,1},{1,0},{2,3},{3,2},{4,5},{5,4},{6,7},{7,6},{8,9},{9,8},{10,11... | collective-permute-start | bytes 196616 | tf_op jit(solution)/shard_map/ppermute | solution.py:661
  113.0 6.2 %collective-permute-start.35 = (bf16[16,4096]{1,0:T(8,128)(2,1)S(1)}, bf16[16,4096]{1,0:T(8,128)(2,1)S(1)}, u32[]{:S(2)}, u32[]{:S(2)}) collective-permute-start(bf16[16,4096]{1,0:T(8,128)(2,1)S(1)} %slice.58), channel_id=1, source_target_pairs={{0,8},{8,16},{16,24},{24,28},{28,20},{20,12},{12,4},{4,0},{1,9},{9... | collective-permute-start | bytes 393224 | tf_op jit(solution)/shard_map/ppermute | solution.py:643
  115.9 5.2 %collective-permute-start.36 = (bf16[16,4096]{1,0:T(8,128)(2,1)S(1)}, bf16[16,4096]{1,0:T(8,128)(2,1)S(1)}, u32[]{:S(2)}, u32[]{:S(2)}) collective-permute-start(bf16[16,4096]{1,0:T(8,128)(2,1)S(1)} %slice.59), channel_id=1, source_target_pairs={{8,0},{16,8},{24,16},{28,24},{20,28},{12,20},{4,12},{0,4},{9,1},{1... | collective-permute-start | bytes 393224 | tf_op jit(solution)/shard_map/ppermute | solution.py:644
  116.2 4.9 %copy-start = (bf16[128,4096]{1,0:T(8,128)(2,1)S(1)}, bf16[128,4096]{1,0:T(8,128)(2,1)}, u32[]{:S(2)}) copy-start(bf16[128,4096]{1,0:T(8,128)(2,1)} %refs_1_.7) | copy-start | bytes 3145732
  121.8 2.0 %collective-permute-start.39 = (bf16[128,2048]{1,0:T(8,128)(2,1)S(1)}, bf16[128,2048]{1,0:T(8,128)(2,1)S(1)}, u32[]{:S(2)}, u32[]{:S(2)}) collective-permute-start(bf16[128,2048]{1,0:T(8,128)(2,1)S(1)} %get-tuple-element.50), channel_id=1, source_target_pairs={{0,1},{1,0},{2,3},{3,2},{4,5},{5,4},{6,7},{7,6},{8,9},{9,8},{10,11... | collective-permute-start | bytes 1572872 | tf_op jit(solution)/shard_map/ppermute | solution.py:661
  122.6 2.5 %collective-permute-start.37 = (bf16[128,2048]{1,0:T(8,128)(2,1)S(1)}, bf16[128,2048]{1,0:T(8,128)(2,1)S(1)}, u32[]{:S(2)}, u32[]{:S(2)}) collective-permute-start(bf16[128,2048]{1,0:T(8,128)(2,1)S(1)} %get-tuple-element.48), channel_id=1, source_target_pairs={{0,1},{1,0},{2,3},{3,2},{4,5},{5,4},{6,7},{7,6},{8,9},{9,8},{10,11... | collective-permute-start | bytes 1572872 | tf_op jit(solution)/shard_map/ppermute | solution.py:661
  124.0 9.2 %collective-permute-start.40 = (bf16[64,2048]{1,0:T(8,128)(2,1)S(1)}, bf16[64,2048]{1,0:T(8,128)(2,1)S(1)}, u32[]{:S(2)}, u32[]{:S(2)}) collective-permute-start(bf16[64,2048]{1,0:T(8,128)(2,1)S(1)} %slice.64), channel_id=1, source_target_pairs={{0,2},{1,3},{2,0},{3,1},{4,6},{5,7},{6,4},{7,5},{8,10},{9,11},{10,... | collective-permute-start | bytes 786440 | tf_op jit(solution)/shard_map/ppermute | solution.py:661
  125.3 12.7 %collective-permute-start.38 = (bf16[64,2048]{1,0:T(8,128)(2,1)S(1)}, bf16[64,2048]{1,0:T(8,128)(2,1)S(1)}, u32[]{:S(2)}, u32[]{:S(2)}) collective-permute-start(bf16[64,2048]{1,0:T(8,128)(2,1)S(1)} %slice.65), channel_id=1, source_target_pairs={{0,2},{1,3},{2,0},{3,1},{4,6},{5,7},{6,4},{7,5},{8,10},{9,11},{10,... | collective-permute-start | bytes 786440 | tf_op jit(solution)/shard_map/ppermute | solution.py:661
  (4 other events, 8.7 us)

commit v4 on v3

--- a/solution.py
+++ b/solution.py
@@ -657,6 +657,21 @@
     return out, low, high
 
 
+def ring_gather_fine(block, count):
+    pairs = ring_pairs(count)
+    out = [block]
+    ahead = back = block
+    last = count // 2
+    for _ in range(1, last - 1):
+        ahead, back = ring_step(ahead, back, pairs)
+        out += [ahead, back]
+    half = block.shape[0] // 2
+    ahead_low, back_high = ring_step(ahead[:half], back[half:], pairs)
+    ahead_high, back_low = ring_step(ahead[half:], back[:half], pairs)
+    low, high = ring_step(ahead_low, back_high, pairs)
+    return out + [ahead_low, ahead_high, back_low, back_high, low, high]
+
+
 def swap(rows, pairs):
     return lax.ppermute(rows, "tp", pairs)
 
@@ -697,7 +712,7 @@
     gate, up, down = slices_call(mine[None].astype(jnp.int32), w_gate[0], w_up[0], w_down[0], unit)
     gates, gate_low, gate_high = ring_gather(gate, count)
     ups, up_low, up_high = ring_gather(up, count)
-    downs, down_low, down_high = ring_gather(down, count)
+    downs = ring_gather_fine(down, count)
 
     queries = (q_first, q_second)
     state = None
@@ -740,7 +755,7 @@
     hidden = hidden_call(
         ids, normed, other, combine, [*ups, up_low, up_high], gate_all, sg, su, unit
     )
-    downs = [s_down, *downs, down_low, down_high]
+    downs = [s_down, *downs]
     width = stream_in.shape[1] // 2
     sums = []
     for part in range(2):

time: 139 us -> 141 us (1.014)
  starting transfers between devices: 36.9 us -> 46.3 us
  waiting for transfers between devices: 81 us -> 74.2 us
    ppermute x16 -> x17, waiting for transfers between devices: 39.5 us -> 24 us  [ring_step(): ahead = lax.ppermute(ahead, 'sp', pairs[0])]
    ppermute x16 -> x17, waiting for transfers between devices: 8.49 us -> 17.8 us  [ring_step(): back = lax.ppermute(back, 'sp', pairs[1])]
    ppermute x16 -> x17, starting transfers between devices: 2.79 us -> 7.8 us  [ring_step(): back = lax.ppermute(back, 'sp', pairs[1])]
    ppermute x16 -> x17, starting transfers between devices: 28.1 us -> 32.8 us  [ring_step(): ahead = lax.ppermute(ahead, 'sp', pairs[0])]
  transfers between devices with their start and end apart: 41 -> 43, of which waited for: 28 -> 22; matrix products, arithmetic and copies ran while one was open for 2% -> 2% of each run, Pallas kernels for 7% -> 6%
where the time goes in v4:
time: 141 us; the launch traced here: 140 us
  waiting for transfers between devices  74.2 us (53%)
  starting transfers between devices  46.3 us (33%)
  Pallas kernels  15.2 us (11%)
  local copies, waits for them, and re-layouts  2.97 us (2%)
    ppermute x17, starting transfers between devices, ring_step(): ahead = lax.ppermute(ahead, 'sp', pairs[0])  32.8 us
    ppermute x9, waiting for transfers between devices, swap(): return lax.ppermute(rows, 'tp', pairs)  32.3 us
    ppermute x17, waiting for transfers between devices, ring_step(): ahead = lax.ppermute(ahead, 'sp', pairs[0])  24 us
    ppermute x17, waiting for transfers between devices, ring_step(): back = lax.ppermute(back, 'sp', pairs[1])  17.8 us
    ppermute x17, starting transfers between devices, ring_step(): back = lax.ppermute(back, 'sp', pairs[1])  7.8 us
    pallas_call x4, Pallas kernels, attn_call(): pl.pallas_call(body, out_shape=out_shape, in_specs=specs(SMEM, smem) + sp...  6.06 us
    ppermute x9, starting transfers between devices, swap(): return lax.ppermute(rows, 'tp', pairs)  5.73 us
    pallas_call x1, Pallas kernels, hidden_call(): pl.pallas_call(lambda *refs: hidden_kernel(unit, *refs), out_shape=pltpu....  2.97 us
  transfers between devices with their start and end apart: 43, of which 22 were waited for; matrix products, arithmetic and copies ran while one was open for 2% of the time, Pallas kernels for 6%

profile of v4, /device:TPU:0, one launch (start us, length us, event | category | flops | bytes accessed | tf_op | source)
XLA Modules:
  0.0 140.5 jit_solution(3439319072302906414)
XLA Ops:
  0.0 1.0 pack.1.refs_3_
  1.0 3.1 %collective-permute-start = (bf16[256,512]{1,0:T(8,128)(2,1)S(1)}, bf16[256,512]{1,0:T(8,128)(2,1)S(1)}, u32[]{:S(2)}, u32[]{:S(2)}) collective-permute-start(bf16[256,512]{1,0:T(8,128)(2,1)S(1)} %pack.1.refs_3_), channel_id=1, source_target_pairs={{0,8},{8,16},{16,24},{24,28},{28,20},{20,12},{12,4},{4,0},{1,9},{9... | collective-permute-start | bytes 786440 | tf_op jit(solution)/shard_map/ppermute | solution.py:643
  4.1 6.2 %collective-permute-done.refs_4_ = bf16[256,512]{1,0:T(8,128)(2,1)S(1)} collective-permute-done((bf16[256,512]{1,0:T(8,128)(2,1)S(1)}, bf16[256,512]{1,0:T(8,128)(2,1)S(1)}, u32[]{:S(2)}, u32[]{:S(2)}) %collective-permute-start) | collective-permute-done | bytes 262176 | tf_op jit(solution)/shard_map/ppermute | solution.py:643
  10.4 1.8 %collective-permute-start.2 = (bf16[256,512]{1,0:T(8,128)(2,1)S(1)}, bf16[256,512]{1,0:T(8,128)(2,1)S(1)}, u32[]{:S(2)}, u32[]{:S(2)}) collective-permute-start(bf16[256,512]{1,0:T(8,128)(2,1)S(1)} %collective-permute-done.refs_4_), channel_id=1, source_target_pairs={{0,8},{8,16},{16,24},{24,28},{28,20},{20,12},{12,4},{4,0},{1,9},{9... | collective-permute-start | bytes 786440 | tf_op jit(solution)/shard_map/ppermute | solution.py:643
  12.4 5.4 %collective-permute-done.2.refs_3_ = bf16[256,512]{1,0:T(8,128)(2,1)S(1)} collective-permute-done((bf16[256,512]{1,0:T(8,128)(2,1)S(1)}, bf16[256,512]{1,0:T(8,128)(2,1)S(1)}, u32[]{:S(2)}, u32[]{:S(2)}) %collective-permute-start.2) | collective-permute-done | bytes 262176 | tf_op jit(solution)/shard_map/ppermute | solution.py:643
  17.8 1.5 %collective-permute-start.3 = (bf16[256,512]{1,0:T(8,128)(2,1)S(1)}, bf16[256,512]{1,0:T(8,128)(2,1)S(1)}, u32[]{:S(2)}, u32[]{:S(2)}) collective-permute-start(bf16[256,512]{1,0:T(8,128)(2,1)S(1)} %collective-permute-done.2.refs_3_), channel_id=1, source_target_pairs={{0,8},{8,16},{16,24},{24,28},{28,20},{20,12},{12,4},{4,0},{1,9},{9... | collective-permute-start | bytes 786440 | tf_op jit(solution)/shard_map/ppermute | solution.py:643
  20.6 0.9 copy-done.6
  21.5 0.9 copy-done.7
  22.4 1.2 shard_map.172
  23.6 0.8 collective-permute-done.3.refs_3_
  24.5 1.5 %collective-permute-start.4 = (bf16[128,512]{1,0:T(8,128)(2,1)S(1)}, bf16[128,512]{1,0:T(8,128)(2,1)S(1)}, u32[]{:S(2)}, u32[]{:S(2)}) collective-permute-start(bf16[128,512]{1,0:T(8,128)(2,1)S(1)} %slice.58), channel_id=1, source_target_pairs={{0,8},{8,16},{16,24},{24,28},{28,20},{20,12},{12,4},{4,0},{1,9},{9... | collective-permute-start | bytes 393224 | tf_op jit(solution)/shard_map/ppermute | solution.py:643
  28.0 1.4 %collective-permute-done.4.refs_4_ = bf16[128,512]{1,0:T(8,128)(2,1)S(1)} collective-permute-done((bf16[128,512]{1,0:T(8,128)(2,1)S(1)}, bf16[128,512]{1,0:T(8,128)(2,1)S(1)}, u32[]{:S(2)}, u32[]{:S(2)}) %collective-permute-start.4) | collective-permute-done | bytes 131104 | tf_op jit(solution)/shard_map/ppermute | solution.py:643
  29.5 1.5 %collective-permute-done.7.refs_5_ = bf16[128,512]{1,0:T(8,128)(2,1)S(1)} collective-permute-done((bf16[128,512]{1,0:T(8,128)(2,1)S(1)}, bf16[128,512]{1,0:T(8,128)(2,1)S(1)}, u32[]{:S(2)}, u32[]{:S(2)}) %collective-permute-start.7) | collective-permute-done | bytes 131104 | tf_op jit(solution)/shard_map/ppermute | solution.py:644
  31.0 3.5 %shard_map.175 = (f32[128,4096]{1,0:T(8,128)S(1)}, bf16[128,4096]{1,0:T(8,128)(2,1)S(1)}) custom-call(s32[10]{0:T(128)S(1)} %pad_add_fusion.refs_0_, f32[2]{0:T(128)S(1)} %copy-done.5, bf16[256,256]{1,0:T(8,128)(2,1)S(1)} %get-tuple-element.28.refs_1_.refs_2_, bf16[256,256]{1,0:T(8,128)(2,1)S(1)} %get-tuple-element.29.refs_2_.refs_3_, ...), custom_call_target="tpu_custom_call" | custom-call | flops 402653184 | bytes 4194304 | tf_op jit(solution)/shard_map/pallas_call | solution.py:396
  34.6 2.6 %collective-permute-done.8 = bf16[128,4096]{1,0:T(8,128)(2,1)S(1)} collective-permute-done((bf16[128,4096]{1,0:T(8,128)(2,1)S(1)}, bf16[128,4096]{1,0:T(8,128)(2,1)S(1)}, u32[]{:S(2)}, u32[]{:S(2)}) %collective-permute-start.8) | collective-permute-done | bytes 1048608 | tf_op jit(solution)/shard_map/ppermute | solution.py:676
  37.5 1.6 %collective-permute-start.9 = (bf16[128,4096]{1,0:T(8,128)(2,1)S(1)}, bf16[128,4096]{1,0:T(8,128)(2,1)S(1)}, u32[]{:S(2)}, u32[]{:S(2)}) collective-permute-start(bf16[128,4096]{1,0:T(8,128)(2,1)S(1)} %add_convert_fusion.1), channel_id=1, source_target_pairs={{0,2},{1,3},{2,0},{3,1},{4,6},{5,7},{6,4},{7,5},{8,10},{9,11},{10,... | collective-permute-start | bytes 3145736 | tf_op jit(solution)/shard_map/ppermute | solution.py:676
  39.0 1.9 %slices.1 = (bf16[32,4096]{1,0:T(8,128)(2,1)S(1)}, bf16[32,4096]{1,0:T(8,128)(2,1)S(1)}, bf16[32,4096]{1,0:T(8,128)(2,1)S(1)}) custom-call(s32[1]{0:T(128)} %bitcast.1.refs_0_, bf16[4096,128]{1,0:T(8,128)(2,1)} %bitcast.7, bf16[4096,128]{1,0:T(8,128)(2,1)} %bitcast.8, bf16[128,4096]{1,0:T(8,128)(2,1)} %bitcast.9), custom_call_target="tpu_custom_call" | custom-call | tf_op jit(solution)/shard_map/slices/pallas_call | solution.py:454
  41.0 1.6 %collective-permute-start.13 = (bf16[32,4096]{1,0:T(8,128)(2,1)S(1)}, bf16[32,4096]{1,0:T(8,128)(2,1)S(1)}, u32[]{:S(2)}, u32[]{:S(2)}) collective-permute-start(bf16[32,4096]{1,0:T(8,128)(2,1)S(1)} %get-tuple-element.41.refs_0_), channel_id=1, source_target_pairs={{0,8},{8,16},{16,24},{24,28},{28,20},{20,12},{12,4},{4,0},{1,9},{9... | collective-permute-start | bytes 786440 | tf_op jit(solution)/shard_map/ppermute | solution.py:643
  44.0 2.0 %collective-permute-start.21 = (bf16[32,4096]{1,0:T(8,128)(2,1)S(1)}, bf16[32,4096]{1,0:T(8,128)(2,1)S(1)}, u32[]{:S(2)}, u32[]{:S(2)}) collective-permute-start(bf16[32,4096]{1,0:T(8,128)(2,1)S(1)} %get-tuple-element.45.refs_8_), channel_id=1, source_target_pairs={{0,8},{8,16},{16,24},{24,28},{28,20},{20,12},{12,4},{4,0},{1,9},{9... | collective-permute-start | bytes 786440 | tf_op jit(solution)/shard_map/ppermute | solution.py:643
  46.0 17.5 %collective-permute-done.11 = f32[64,128]{1,0:T(8,128)S(1)} collective-permute-done((f32[64,128]{1,0:T(8,128)S(1)}, f32[64,128]{1,0:T(8,128)S(1)}, u32[]{:S(2)}, u32[]{:S(2)}) %collective-permute-start.11) | collective-permute-done | bytes 32800 | tf_op jit(solution)/shard_map/ppermute | solution.py:676
  64.0 1.5 %collective-permute-start.29 = (bf16[32,4096]{1,0:T(8,128)(2,1)S(1)}, bf16[32,4096]{1,0:T(8,128)(2,1)S(1)}, u32[]{:S(2)}, u32[]{:S(2)}) collective-permute-start(bf16[32,4096]{1,0:T(8,128)(2,1)S(1)} %get-tuple-element.46.refs_2_), channel_id=1, source_target_pairs={{0,8},{8,16},{16,24},{24,28},{28,20},{20,12},{12,4},{4,0},{1,9},{9... | collective-permute-start | bytes 786440 | tf_op jit(solution)/shard_map/ppermute | solution.py:643
  65.5 2.0 %collective-permute-start.15 = (bf16[32,4096]{1,0:T(8,128)(2,1)S(1)}, bf16[32,4096]{1,0:T(8,128)(2,1)S(1)}, u32[]{:S(2)}, u32[]{:S(2)}) collective-permute-start(bf16[32,4096]{1,0:T(8,128)(2,1)S(1)} %collective-permute-done.13.refs_1_), channel_id=1, source_target_pairs={{0,8},{8,16},{16,24},{24,28},{28,20},{20,12},{12,4},{4,0},{1,9},{9... | collective-permute-start | bytes 786440 | tf_op jit(solution)/shard_map/ppermute | solution.py:643
  69.0 3.1 %collective-permute-done.22.refs_10_ = bf16[32,4096]{1,0:T(8,128)(2,1)S(1)} collective-permute-done((bf16[32,4096]{1,0:T(8,128)(2,1)S(1)}, bf16[32,4096]{1,0:T(8,128)(2,1)S(1)}, u32[]{:S(2)}, u32[]{:S(2)}) %collective-permute-start.22) | collective-permute-done | bytes 262176 | tf_op jit(solution)/shard_map/ppermute | solution.py:644
  72.0 2.6 %collective-permute-start.23 = (bf16[32,4096]{1,0:T(8,128)(2,1)S(1)}, bf16[32,4096]{1,0:T(8,128)(2,1)S(1)}, u32[]{:S(2)}, u32[]{:S(2)}) collective-permute-start(bf16[32,4096]{1,0:T(8,128)(2,1)S(1)} %collective-permute-done.21.refs_9_), channel_id=1, source_target_pairs={{0,8},{8,16},{16,24},{24,28},{28,20},{20,12},{12,4},{4,0},{1,9},{9... | collective-permute-start | bytes 786440 | tf_op jit(solution)/shard_map/ppermute | solution.py:643
  74.6 2.0 %collective-permute-start.31 = (bf16[32,4096]{1,0:T(8,128)(2,1)S(1)}, bf16[32,4096]{1,0:T(8,128)(2,1)S(1)}, u32[]{:S(2)}, u32[]{:S(2)}) collective-permute-start(bf16[32,4096]{1,0:T(8,128)(2,1)S(1)} %collective-permute-done.29.refs_3_), channel_id=1, source_target_pairs={{0,8},{8,16},{16,24},{24,28},{28,20},{20,12},{12,4},{4,0},{1,9},{9... | collective-permute-start | bytes 786440 | tf_op jit(solution)/shard_map/ppermute | solution.py:643
  76.6 2.2 %collective-permute-done.15.refs_3_ = bf16[32,4096]{1,0:T(8,128)(2,1)S(1)} collective-permute-done((bf16[32,4096]{1,0:T(8,128)(2,1)S(1)}, bf16[32,4096]{1,0:T(8,128)(2,1)S(1)}, u32[]{:S(2)}, u32[]{:S(2)}) %collective-permute-start.15) | collective-permute-done | bytes 262176 | tf_op jit(solution)/shard_map/ppermute | solution.py:643
  78.9 1.5 %collective-permute-start.17 = (bf16[32,4096]{1,0:T(8,128)(2,1)S(1)}, bf16[32,4096]{1,0:T(8,128)(2,1)S(1)}, u32[]{:S(2)}, u32[]{:S(2)}) collective-permute-start(bf16[32,4096]{1,0:T(8,128)(2,1)S(1)} %collective-permute-done.15.refs_3_), channel_id=1, source_target_pairs={{0,8},{8,16},{16,24},{24,28},{28,20},{20,12},{12,4},{4,0},{1,9},{9... | collective-permute-start | bytes 786440 | tf_op jit(solution)/shard_map/ppermute | solution.py:643
  81.3 2.0 %collective-permute-done.16.refs_4_ = bf16[32,4096]{1,0:T(8,128)(2,1)S(1)} collective-permute-done((bf16[32,4096]{1,0:T(8,128)(2,1)S(1)}, bf16[32,4096]{1,0:T(8,128)(2,1)S(1)}, u32[]{:S(2)}, u32[]{:S(2)}) %collective-permute-start.16) | collective-permute-done | bytes 262176 | tf_op jit(solution)/shard_map/ppermute | solution.py:644
  83.3 1.1 collective-permute-start.32
  84.5 2.0 %collective-permute-start.18 = (bf16[32,4096]{1,0:T(8,128)(2,1)S(1)}, bf16[32,4096]{1,0:T(8,128)(2,1)S(1)}, u32[]{:S(2)}, u32[]{:S(2)}) collective-permute-start(bf16[32,4096]{1,0:T(8,128)(2,1)S(1)} %collective-permute-done.16.refs_4_), channel_id=1, source_target_pairs={{8,0},{16,8},{24,16},{28,24},{20,28},{12,20},{4,12},{0,4},{9,1},{1... | collective-permute-start | bytes 786440 | tf_op jit(solution)/shard_map/ppermute | solution.py:644
  86.5 3.6 %collective-permute-done.31.refs_5_ = bf16[32,4096]{1,0:T(8,128)(2,1)S(1)} collective-permute-done((bf16[32,4096]{1,0:T(8,128)(2,1)S(1)}, bf16[32,4096]{1,0:T(8,128)(2,1)S(1)}, u32[]{:S(2)}, u32[]{:S(2)}) %collective-permute-start.31) | collective-permute-done | bytes 262176 | tf_op jit(solution)/shard_map/ppermute | solution.py:643
  90.1 1.5 %collective-permute-start.25 = (bf16[32,4096]{1,0:T(8,128)(2,1)S(1)}, bf16[32,4096]{1,0:T(8,128)(2,1)S(1)}, u32[]{:S(2)}, u32[]{:S(2)}) collective-permute-start(bf16[32,4096]{1,0:T(8,128)(2,1)S(1)} %collective-permute-done.23.refs_11_), channel_id=1, source_target_pairs={{0,8},{8,16},{16,24},{24,28},{28,20},{20,12},{12,4},{4,0},{1,9},{9... | collective-permute-start | bytes 786440 | tf_op jit(solution)/shard_map/ppermute | solution.py:643
  91.6 4.2 %collective-permute-done.17.refs_5_ = bf16[32,4096]{1,0:T(8,128)(2,1)S(1)} collective-permute-done((bf16[32,4096]{1,0:T(8,128)(2,1)S(1)}, bf16[32,4096]{1,0:T(8,128)(2,1)S(1)}, u32[]{:S(2)}, u32[]{:S(2)}) %collective-permute-start.17) | collective-permute-done | bytes 262176 | tf_op jit(solution)/shard_map/ppermute | solution.py:643
  96.4 2.7 %collective-permute-done.18.refs_6_ = bf16[32,4096]{1,0:T(8,128)(2,1)S(1)} collective-permute-done((bf16[32,4096]{1,0:T(8,128)(2,1)S(1)}, bf16[32,4096]{1,0:T(8,128)(2,1)S(1)}, u32[]{:S(2)}, u32[]{:S(2)}) %collective-permute-start.18) | collective-permute-done | bytes 262176 | tf_op jit(solution)/shard_map/ppermute | solution.py:644
  99.6 1.8 %collective-permute-start.19 = (bf16[16,4096]{1,0:T(8,128)(2,1)S(1)}, bf16[16,4096]{1,0:T(8,128)(2,1)S(1)}, u32[]{:S(2)}, u32[]{:S(2)}) collective-permute-start(bf16[16,4096]{1,0:T(8,128)(2,1)S(1)} %slice.62), channel_id=1, source_target_pairs={{0,8},{8,16},{16,24},{24,28},{28,20},{20,12},{12,4},{4,0},{1,9},{9... | collective-permute-start | bytes 393224 | tf_op jit(solution)/shard_map/ppermute | solution.py:643
  101.8 1.8 %collective-permute-start.33 = (bf16[16,4096]{1,0:T(8,128)(2,1)S(1)}, bf16[16,4096]{1,0:T(8,128)(2,1)S(1)}, u32[]{:S(2)}, u32[]{:S(2)}) collective-permute-start(bf16[16,4096]{1,0:T(8,128)(2,1)S(1)} %get-tuple-element.56), channel_id=1, source_target_pairs={{0,8},{8,16},{16,24},{24,28},{28,20},{20,12},{12,4},{4,0},{1,9},{9... | collective-permute-start | bytes 393224 | tf_op jit(solution)/shard_map/ppermute | solution.py:643
  103.5 4.8 %collective-permute-done.26.refs_14_ = bf16[32,4096]{1,0:T(8,128)(2,1)S(1)} collective-permute-done((bf16[32,4096]{1,0:T(8,128)(2,1)S(1)}, bf16[32,4096]{1,0:T(8,128)(2,1)S(1)}, u32[]{:S(2)}, u32[]{:S(2)}) %collective-permute-start.26) | collective-permute-done | bytes 262176 | tf_op jit(solution)/shard_map/ppermute | solution.py:644
  108.3 2.2 %collective-permute-start.27 = (bf16[16,4096]{1,0:T(8,128)(2,1)S(1)}, bf16[16,4096]{1,0:T(8,128)(2,1)S(1)}, u32[]{:S(2)}, u32[]{:S(2)}) collective-permute-start(bf16[16,4096]{1,0:T(8,128)(2,1)S(1)} %slice.64), channel_id=1, source_target_pairs={{0,8},{8,16},{16,24},{24,28},{28,20},{20,12},{12,4},{4,0},{1,9},{9... | collective-permute-start | bytes 393224 | tf_op jit(solution)/shard_map/ppermute | solution.py:643
  111.9 2.2 %collective-permute-start.34 = (bf16[16,4096]{1,0:T(8,128)(2,1)S(1)}, bf16[16,4096]{1,0:T(8,128)(2,1)S(1)}, u32[]{:S(2)}, u32[]{:S(2)}) collective-permute-start(bf16[16,4096]{1,0:T(8,128)(2,1)S(1)} %get-tuple-element.55), channel_id=1, source_target_pairs={{0,8},{8,16},{16,24},{24,28},{28,20},{20,12},{12,4},{4,0},{1,9},{9... | collective-permute-start | bytes 393224 | tf_op jit(solution)/shard_map/ppermute | solution.py:643
  114.6 2.2 %collective-permute-start.37 = (bf16[16,4096]{1,0:T(8,128)(2,1)S(1)}, bf16[16,4096]{1,0:T(8,128)(2,1)S(1)}, u32[]{:S(2)}, u32[]{:S(2)}) collective-permute-start(bf16[16,4096]{1,0:T(8,128)(2,1)S(1)} %collective-permute-done.33.refs_7_), channel_id=1, source_target_pairs={{0,8},{8,16},{16,24},{24,28},{28,20},{20,12},{12,4},{4,0},{1,9},{9... | collective-permute-start | bytes 393224 | tf_op jit(solution)/shard_map/ppermute | solution.py:643
  116.9 0.8 collective-permute-done.28.refs_16_
  117.6 3.0 %hidden.1.refs_0_ = bf16[256,384]{1,0:T(8,128)(2,1)S(1)} custom-call(s32[10]{0:T(128)S(1)} %pad_add_fusion.refs_0_, bf16[128,4096]{1,0:T(8,128)(2,1)S(1)} %fusion.2.refs_1_, bf16[128,4096]{1,0:T(8,128)(2,1)S(1)} %collective-permute-done.10.refs_2_, f32[128,128]{1,0:T(8,128)S(1)} %pad_maximum_fusion.refs_3_, f32[128,128]{1,0:T(8,128)S(1)} %collective-permute-done.12.refs_4_, ...), custom_call_target="tpu_custom_call" | custom-call | flops 1610612736 | bytes 12582912 | tf_op jit(solution)/shard_map/hidden/pallas_call | solution.py:567
  120.7 2.0 %collective-permute-done.38.refs_12_ = bf16[16,4096]{1,0:T(8,128)(2,1)S(1)} collective-permute-done((bf16[16,4096]{1,0:T(8,128)(2,1)S(1)}, bf16[16,4096]{1,0:T(8,128)(2,1)S(1)}, u32[]{:S(2)}, u32[]{:S(2)}) %collective-permute-start.38) | collective-permute-done | bytes 131104 | tf_op jit(solution)/shard_map/ppermute | solution.py:644
  125.5 1.6 %collective-permute-start.42 = (bf16[64,2048]{1,0:T(8,128)(2,1)S(1)}, bf16[64,2048]{1,0:T(8,128)(2,1)S(1)}, u32[]{:S(2)}, u32[]{:S(2)}) collective-permute-start(bf16[64,2048]{1,0:T(8,128)(2,1)S(1)} %slice.74), channel_id=1, source_target_pairs={{0,2},{1,3},{2,0},{3,1},{4,6},{5,7},{6,4},{7,5},{8,10},{9,11},{10,... | collective-permute-start | bytes 786440 | tf_op jit(solution)/shard_map/ppermute | solution.py:676
  127.2 0.7 collective-permute-start.40
  127.9 6.8 %collective-permute-done.42.refs_3_ = bf16[64,2048]{1,0:T(8,128)(2,1)S(1)} collective-permute-done((bf16[64,2048]{1,0:T(8,128)(2,1)S(1)}, bf16[64,2048]{1,0:T(8,128)(2,1)S(1)}, u32[]{:S(2)}, u32[]{:S(2)}) %collective-permute-start.42) | collective-permute-done | bytes 262176 | tf_op jit(solution)/shard_map/ppermute | solution.py:676
  134.7 4.8 %collective-permute-done.40.refs_1_ = bf16[64,2048]{1,0:T(8,128)(2,1)S(1)} collective-permute-done((bf16[64,2048]{1,0:T(8,128)(2,1)S(1)}, bf16[64,2048]{1,0:T(8,128)(2,1)S(1)}, u32[]{:S(2)}, u32[]{:S(2)}) %collective-permute-start.40) | collective-permute-done | bytes 262176 | tf_op jit(solution)/shard_map/ppermute | solution.py:676
  139.5 1.0 final.1
  (95 shorter events, 14.6 us)
Async XLA Ops:
  1.0 9.4 %collective-permute-start = (bf16[256,512]{1,0:T(8,128)(2,1)S(1)}, bf16[256,512]{1,0:T(8,128)(2,1)S(1)}, u32[]{:S(2)}, u32[]{:S(2)}) collective-permute-start(bf16[256,512]{1,0:T(8,128)(2,1)S(1)} %pack.1.refs_3_), channel_id=1, source_target_pairs={{0,8},{8,16},{16,24},{24,28},{28,20},{20,12},{12,4},{4,0},{1,9},{9... | collective-permute-start | bytes 786440 | tf_op jit(solution)/shard_map/ppermute | solution.py:643
  4.1 8.0 %collective-permute-start.1 = (bf16[256,512]{1,0:T(8,128)(2,1)S(1)}, bf16[256,512]{1,0:T(8,128)(2,1)S(1)}, u32[]{:S(2)}, u32[]{:S(2)}) collective-permute-start(bf16[256,512]{1,0:T(8,128)(2,1)S(1)} %pack.1.refs_3_), channel_id=1, source_target_pairs={{8,0},{16,8},{24,16},{28,24},{20,28},{12,20},{4,12},{0,4},{9,1},{1... | collective-permute-start | bytes 786440 | tf_op jit(solution)/shard_map/ppermute | solution.py:644
  10.4 7.5 %collective-permute-start.2 = (bf16[256,512]{1,0:T(8,128)(2,1)S(1)}, bf16[256,512]{1,0:T(8,128)(2,1)S(1)}, u32[]{:S(2)}, u32[]{:S(2)}) collective-permute-start(bf16[256,512]{1,0:T(8,128)(2,1)S(1)} %collective-permute-done.refs_4_), channel_id=1, source_target_pairs={{0,8},{8,16},{16,24},{24,28},{28,20},{20,12},{12,4},{4,0},{1,9},{9... | collective-permute-start | bytes 786440 | tf_op jit(solution)/shard_map/ppermute | solution.py:643
  12.2 7.2 %collective-permute-start.5 = (bf16[256,512]{1,0:T(8,128)(2,1)S(1)}, bf16[256,512]{1,0:T(8,128)(2,1)S(1)}, u32[]{:S(2)}, u32[]{:S(2)}) collective-permute-start(bf16[256,512]{1,0:T(8,128)(2,1)S(1)} %collective-permute-done.1.refs_5_), channel_id=1, source_target_pairs={{8,0},{16,8},{24,16},{28,24},{20,28},{12,20},{4,12},{0,4},{9,1},{1... | collective-permute-start | bytes 786440 | tf_op jit(solution)/shard_map/ppermute | solution.py:644
  17.8 6.6 %collective-permute-start.3 = (bf16[256,512]{1,0:T(8,128)(2,1)S(1)}, bf16[256,512]{1,0:T(8,128)(2,1)S(1)}, u32[]{:S(2)}, u32[]{:S(2)}) collective-permute-start(bf16[256,512]{1,0:T(8,128)(2,1)S(1)} %collective-permute-done.2.refs_3_), channel_id=1, source_target_pairs={{0,8},{8,16},{16,24},{24,28},{28,20},{20,12},{12,4},{4,0},{1,9},{9... | collective-permute-start | bytes 786440 | tf_op jit(solution)/shard_map/ppermute | solution.py:643
  19.4 6.6 %collective-permute-start.6 = (bf16[256,512]{1,0:T(8,128)(2,1)S(1)}, bf16[256,512]{1,0:T(8,128)(2,1)S(1)}, u32[]{:S(2)}, u32[]{:S(2)}) collective-permute-start(bf16[256,512]{1,0:T(8,128)(2,1)S(1)} %collective-permute-done.5.refs_4_), channel_id=1, source_target_pairs={{8,0},{16,8},{24,16},{28,24},{20,28},{12,20},{4,12},{0,4},{9,1},{1... | collective-permute-start | bytes 786440 | tf_op jit(solution)/shard_map/ppermute | solution.py:644
  24.5 5.0 %collective-permute-start.4 = (bf16[128,512]{1,0:T(8,128)(2,1)S(1)}, bf16[128,512]{1,0:T(8,128)(2,1)S(1)}, u32[]{:S(2)}, u32[]{:S(2)}) collective-permute-start(bf16[128,512]{1,0:T(8,128)(2,1)S(1)} %slice.58), channel_id=1, source_target_pairs={{0,8},{8,16},{16,24},{24,28},{28,20},{20,12},{12,4},{4,0},{1,9},{9... | collective-permute-start | bytes 393224 | tf_op jit(solution)/shard_map/ppermute | solution.py:643
  26.0 5.0 %collective-permute-start.7 = (bf16[128,512]{1,0:T(8,128)(2,1)S(1)}, bf16[128,512]{1,0:T(8,128)(2,1)S(1)}, u32[]{:S(2)}, u32[]{:S(2)}) collective-permute-start(bf16[128,512]{1,0:T(8,128)(2,1)S(1)} %slice.59), channel_id=1, source_target_pairs={{8,0},{16,8},{24,16},{28,24},{20,28},{12,20},{4,12},{0,4},{9,1},{1... | collective-permute-start | bytes 393224 | tf_op jit(solution)/shard_map/ppermute | solution.py:644
  34.5 2.7 %collective-permute-start.8 = (bf16[128,4096]{1,0:T(8,128)(2,1)S(1)}, bf16[128,4096]{1,0:T(8,128)(2,1)S(1)}, u32[]{:S(2)}, u32[]{:S(2)}) collective-permute-start(bf16[128,4096]{1,0:T(8,128)(2,1)S(1)} %get-tuple-element.40), channel_id=1, source_target_pairs={{0,1},{1,0},{2,3},{3,2},{4,5},{5,4},{6,7},{7,6},{8,9},{9,8},{10,11... | collective-permute-start | bytes 3145736 | tf_op jit(solution)/shard_map/ppermute | solution.py:676
  37.5 5.2 %copy-start.9 = (s32[64,4]{0,1:T(4,128)S(1)}, s32[64,4]{0,1:T(4,128)}, u32[]{:S(2)}) copy-start(s32[64,4]{0,1:T(4,128)} %param.27) | copy-start | bytes 3076
  37.5 5.2 %copy-start.10 = (f32[64,4]{0,1:T(4,128)S(1)}, f32[64,4]{0,1:T(4,128)}, u32[]{:S(2)}) copy-start(f32[64,4]{0,1:T(4,128)} %param.28) | copy-start | bytes 3076
  37.5 28.1 %collective-permute-start.9 = (bf16[128,4096]{1,0:T(8,128)(2,1)S(1)}, bf16[128,4096]{1,0:T(8,128)(2,1)S(1)}, u32[]{:S(2)}, u32[]{:S(2)}) collective-permute-start(bf16[128,4096]{1,0:T(8,128)(2,1)S(1)} %add_convert_fusion.1), channel_id=1, source_target_pairs={{0,2},{1,3},{2,0},{3,1},{4,6},{5,7},{6,4},{7,5},{8,10},{9,11},{10,... | collective-permute-start | bytes 3145736 | tf_op jit(solution)/shard_map/ppermute | solution.py:676
  41.0 23.0 %collective-permute-start.13 = (bf16[32,4096]{1,0:T(8,128)(2,1)S(1)}, bf16[32,4096]{1,0:T(8,128)(2,1)S(1)}, u32[]{:S(2)}, u32[]{:S(2)}) collective-permute-start(bf16[32,4096]{1,0:T(8,128)(2,1)S(1)} %get-tuple-element.41.refs_0_), channel_id=1, source_target_pairs={{0,8},{8,16},{16,24},{24,28},{28,20},{20,12},{12,4},{4,0},{1,9},{9... | collective-permute-start | bytes 786440 | tf_op jit(solution)/shard_map/ppermute | solution.py:643
  42.9 20.5 %collective-permute-start.11 = (f32[64,128]{1,0:T(8,128)S(1)}, f32[64,128]{1,0:T(8,128)S(1)}, u32[]{:S(2)}, u32[]{:S(2)}) collective-permute-start(f32[64,128]{1,0:T(8,128)S(1)} %combine.1), channel_id=1, source_target_pairs={{0,2},{1,3},{2,0},{3,1},{4,6},{5,7},{6,4},{7,5},{8,10},{9,11},{10,... | collective-permute-start | bytes 98312 | tf_op jit(solution)/shard_map/ppermute | solution.py:676
  43.6 24.7 %collective-permute-start.14 = (bf16[32,4096]{1,0:T(8,128)(2,1)S(1)}, bf16[32,4096]{1,0:T(8,128)(2,1)S(1)}, u32[]{:S(2)}, u32[]{:S(2)}) collective-permute-start(bf16[32,4096]{1,0:T(8,128)(2,1)S(1)} %get-tuple-element.41.refs_0_), channel_id=1, source_target_pairs={{8,0},{16,8},{24,16},{28,24},{20,28},{12,20},{4,12},{0,4},{9,1},{1... | collective-permute-start | bytes 786440 | tf_op jit(solution)/shard_map/ppermute | solution.py:644
  44.0 24.3 %collective-permute-start.21 = (bf16[32,4096]{1,0:T(8,128)(2,1)S(1)}, bf16[32,4096]{1,0:T(8,128)(2,1)S(1)}, u32[]{:S(2)}, u32[]{:S(2)}) collective-permute-start(bf16[32,4096]{1,0:T(8,128)(2,1)S(1)} %get-tuple-element.45.refs_8_), channel_id=1, source_target_pairs={{0,8},{8,16},{16,24},{24,28},{28,20},{20,12},{12,4},{4,0},{1,9},{9... | collective-permute-start | bytes 786440 | tf_op jit(solution)/shard_map/ppermute | solution.py:643
  63.4 8.6 %collective-permute-start.22 = (bf16[32,4096]{1,0:T(8,128)(2,1)S(1)}, bf16[32,4096]{1,0:T(8,128)(2,1)S(1)}, u32[]{:S(2)}, u32[]{:S(2)}) collective-permute-start(bf16[32,4096]{1,0:T(8,128)(2,1)S(1)} %get-tuple-element.45.refs_8_), channel_id=1, source_target_pairs={{8,0},{16,8},{24,16},{28,24},{20,28},{12,20},{4,12},{0,4},{9,1},{1... | collective-permute-start | bytes 786440 | tf_op jit(solution)/shard_map/ppermute | solution.py:644
  64.0 10.6 %collective-permute-start.29 = (bf16[32,4096]{1,0:T(8,128)(2,1)S(1)}, bf16[32,4096]{1,0:T(8,128)(2,1)S(1)}, u32[]{:S(2)}, u32[]{:S(2)}) collective-permute-start(bf16[32,4096]{1,0:T(8,128)(2,1)S(1)} %get-tuple-element.46.refs_2_), channel_id=1, source_target_pairs={{0,8},{8,16},{16,24},{24,28},{28,20},{20,12},{12,4},{4,0},{1,9},{9... | collective-permute-start | bytes 786440 | tf_op jit(solution)/shard_map/ppermute | solution.py:643
  65.5 13.3 %collective-permute-start.15 = (bf16[32,4096]{1,0:T(8,128)(2,1)S(1)}, bf16[32,4096]{1,0:T(8,128)(2,1)S(1)}, u32[]{:S(2)}, u32[]{:S(2)}) collective-permute-start(bf16[32,4096]{1,0:T(8,128)(2,1)S(1)} %collective-permute-done.13.refs_1_), channel_id=1, source_target_pairs={{0,8},{8,16},{16,24},{24,28},{28,20},{20,12},{12,4},{4,0},{1,9},{9... | collective-permute-start | bytes 786440 | tf_op jit(solution)/shard_map/ppermute | solution.py:643
  67.6 12.7 %copy-start.8 = (f32[4096]{0:T(1024)S(1)}, f32[4096]{0:T(1024)}, u32[]{:S(2)}) copy-start(f32[4096]{0:T(1024)} %param.26) | copy-start | bytes 49156
  68.2 42.9 %copy-start.2 = (bf16[4096,128]{1,0:T(8,128)(2,1)S(1)}, bf16[4096,128]{1,0:T(8,128)(2,1)}, u32[]{:S(2)}) copy-start(bf16[4096,128]{1,0:T(8,128)(2,1)} %refs_9_.3) | copy-start | bytes 3145732
  68.2 42.9 %copy-start.3 = (bf16[4096,128]{1,0:T(8,128)(2,1)S(1)}, bf16[4096,128]{1,0:T(8,128)(2,1)}, u32[]{:S(2)}) copy-start(bf16[4096,128]{1,0:T(8,128)(2,1)} %refs_10_.3) | copy-start | bytes 3145732
  68.2 12.5 %collective-permute-start.30 = (bf16[32,4096]{1,0:T(8,128)(2,1)S(1)}, bf16[32,4096]{1,0:T(8,128)(2,1)S(1)}, u32[]{:S(2)}, u32[]{:S(2)}) collective-permute-start(bf16[32,4096]{1,0:T(8,128)(2,1)S(1)} %get-tuple-element.46.refs_2_), channel_id=1, source_target_pairs={{8,0},{16,8},{24,16},{28,24},{20,28},{12,20},{4,12},{0,4},{9,1},{1... | collective-permute-start | bytes 786440 | tf_op jit(solution)/shard_map/ppermute | solution.py:644
  68.3 15.0 %collective-permute-start.16 = (bf16[32,4096]{1,0:T(8,128)(2,1)S(1)}, bf16[32,4096]{1,0:T(8,128)(2,1)S(1)}, u32[]{:S(2)}, u32[]{:S(2)}) collective-permute-start(bf16[32,4096]{1,0:T(8,128)(2,1)S(1)} %collective-permute-done.14.refs_2_), channel_id=1, source_target_pairs={{8,0},{16,8},{24,16},{28,24},{20,28},{12,20},{4,12},{0,4},{9,1},{1... | collective-permute-start | bytes 786440 | tf_op jit(solution)/shard_map/ppermute | solution.py:644
  72.0 12.5 %collective-permute-start.23 = (bf16[32,4096]{1,0:T(8,128)(2,1)S(1)}, bf16[32,4096]{1,0:T(8,128)(2,1)S(1)}, u32[]{:S(2)}, u32[]{:S(2)}) collective-permute-start(bf16[32,4096]{1,0:T(8,128)(2,1)S(1)} %collective-permute-done.21.refs_9_), channel_id=1, source_target_pairs={{0,8},{8,16},{16,24},{24,28},{28,20},{20,12},{12,4},{4,0},{1,9},{9... | collective-permute-start | bytes 786440 | tf_op jit(solution)/shard_map/ppermute | solution.py:643
  74.6 15.5 %collective-permute-start.31 = (bf16[32,4096]{1,0:T(8,128)(2,1)S(1)}, bf16[32,4096]{1,0:T(8,128)(2,1)S(1)}, u32[]{:S(2)}, u32[]{:S(2)}) collective-permute-start(bf16[32,4096]{1,0:T(8,128)(2,1)S(1)} %collective-permute-done.29.refs_3_), channel_id=1, source_target_pairs={{0,8},{8,16},{16,24},{24,28},{28,20},{20,12},{12,4},{4,0},{1,9},{9... | collective-permute-start | bytes 786440 | tf_op jit(solution)/shard_map/ppermute | solution.py:643
  78.9 16.9 %collective-permute-start.17 = (bf16[32,4096]{1,0:T(8,128)(2,1)S(1)}, bf16[32,4096]{1,0:T(8,128)(2,1)S(1)}, u32[]{:S(2)}, u32[]{:S(2)}) collective-permute-start(bf16[32,4096]{1,0:T(8,128)(2,1)S(1)} %collective-permute-done.15.refs_3_), channel_id=1, source_target_pairs={{0,8},{8,16},{16,24},{24,28},{28,20},{20,12},{12,4},{4,0},{1,9},{9... | collective-permute-start | bytes 786440 | tf_op jit(solution)/shard_map/ppermute | solution.py:643
  80.7 15.1 %collective-permute-start.24 = (bf16[32,4096]{1,0:T(8,128)(2,1)S(1)}, bf16[32,4096]{1,0:T(8,128)(2,1)S(1)}, u32[]{:S(2)}, u32[]{:S(2)}) collective-permute-start(bf16[32,4096]{1,0:T(8,128)(2,1)S(1)} %collective-permute-done.22.refs_10_), channel_id=1, source_target_pairs={{8,0},{16,8},{24,16},{28,24},{20,28},{12,20},{4,12},{0,4},{9,1},{1... | collective-permute-start | bytes 786440 | tf_op jit(solution)/shard_map/ppermute | solution.py:644
  83.3 16.4 %collective-permute-start.32 = (bf16[32,4096]{1,0:T(8,128)(2,1)S(1)}, bf16[32,4096]{1,0:T(8,128)(2,1)S(1)}, u32[]{:S(2)}, u32[]{:S(2)}) collective-permute-start(bf16[32,4096]{1,0:T(8,128)(2,1)S(1)} %collective-permute-done.30.refs_4_), channel_id=1, source_target_pairs={{8,0},{16,8},{24,16},{28,24},{20,28},{12,20},{4,12},{0,4},{9,1},{1... | collective-permute-start | bytes 786440 | tf_op jit(solution)/shard_map/ppermute | solution.py:644
  84.5 14.5 %collective-permute-start.18 = (bf16[32,4096]{1,0:T(8,128)(2,1)S(1)}, bf16[32,4096]{1,0:T(8,128)(2,1)S(1)}, u32[]{:S(2)}, u32[]{:S(2)}) collective-permute-start(bf16[32,4096]{1,0:T(8,128)(2,1)S(1)} %collective-permute-done.16.refs_4_), channel_id=1, source_target_pairs={{8,0},{16,8},{24,16},{28,24},{20,28},{12,20},{4,12},{0,4},{9,1},{1... | collective-permute-start | bytes 786440 | tf_op jit(solution)/shard_map/ppermute | solution.py:644
  90.1 11.3 %collective-permute-start.25 = (bf16[32,4096]{1,0:T(8,128)(2,1)S(1)}, bf16[32,4096]{1,0:T(8,128)(2,1)S(1)}, u32[]{:S(2)}, u32[]{:S(2)}) collective-permute-start(bf16[32,4096]{1,0:T(8,128)(2,1)S(1)} %collective-permute-done.23.refs_11_), channel_id=1, source_target_pairs={{0,8},{8,16},{16,24},{24,28},{28,20},{20,12},{12,4},{4,0},{1,9},{9... | collective-permute-start | bytes 786440 | tf_op jit(solution)/shard_map/ppermute | solution.py:643
  95.7 21.9 %collective-permute-start.10 = (bf16[128,4096]{1,0:T(8,128)(2,1)S(1)}, bf16[128,4096]{1,0:T(8,128)(2,1)S(1)}, u32[]{:S(2)}, u32[]{:S(2)}) collective-permute-start(bf16[128,4096]{1,0:T(8,128)(2,1)S(1)} %fusion.2.refs_1_), channel_id=1, source_target_pairs={{0,1},{1,0},{2,3},{3,2},{4,5},{5,4},{6,7},{7,6},{8,9},{9,8},{10,11... | collective-permute-start | bytes 3145736 | tf_op jit(solution)/shard_map/ppermute | solution.py:676
  95.8 6.0 %collective-permute-start.12 = (f32[128,128]{1,0:T(8,128)S(1)}, f32[128,128]{1,0:T(8,128)S(1)}, u32[]{:S(2)}, u32[]{:S(2)}) collective-permute-start(f32[128,128]{1,0:T(8,128)S(1)} %pad_maximum_fusion.refs_3_), channel_id=1, source_target_pairs={{0,1},{1,0},{2,3},{3,2},{4,5},{5,4},{6,7},{7,6},{8,9},{9,8},{10,11... | collective-permute-start | bytes 196616 | tf_op jit(solution)/shard_map/ppermute | solution.py:676
  99.0 9.3 %collective-permute-start.26 = (bf16[32,4096]{1,0:T(8,128)(2,1)S(1)}, bf16[32,4096]{1,0:T(8,128)(2,1)S(1)}, u32[]{:S(2)}, u32[]{:S(2)}) collective-permute-start(bf16[32,4096]{1,0:T(8,128)(2,1)S(1)} %collective-permute-done.24.refs_12_), channel_id=1, source_target_pairs={{8,0},{16,8},{24,16},{28,24},{20,28},{12,20},{4,12},{0,4},{9,1},{1... | collective-permute-start | bytes 786440 | tf_op jit(solution)/shard_map/ppermute | solution.py:644
  99.6 8.7 %collective-permute-start.19 = (bf16[16,4096]{1,0:T(8,128)(2,1)S(1)}, bf16[16,4096]{1,0:T(8,128)(2,1)S(1)}, u32[]{:S(2)}, u32[]{:S(2)}) collective-permute-start(bf16[16,4096]{1,0:T(8,128)(2,1)S(1)} %slice.62), channel_id=1, source_target_pairs={{0,8},{8,16},{16,24},{24,28},{28,20},{20,12},{12,4},{4,0},{1,9},{9... | collective-permute-start | bytes 393224 | tf_op jit(solution)/shard_map/ppermute | solution.py:643
  101.4 9.7 %collective-permute-start.20 = (bf16[16,4096]{1,0:T(8,128)(2,1)S(1)}, bf16[16,4096]{1,0:T(8,128)(2,1)S(1)}, u32[]{:S(2)}, u32[]{:S(2)}) collective-permute-start(bf16[16,4096]{1,0:T(8,128)(2,1)S(1)} %slice.63), channel_id=1, source_target_pairs={{8,0},{16,8},{24,16},{28,24},{20,28},{12,20},{4,12},{0,4},{9,1},{1... | collective-permute-start | bytes 393224 | tf_op jit(solution)/shard_map/ppermute | solution.py:644
  101.8 10.1 %collective-permute-start.33 = (bf16[16,4096]{1,0:T(8,128)(2,1)S(1)}, bf16[16,4096]{1,0:T(8,128)(2,1)S(1)}, u32[]{:S(2)}, u32[]{:S(2)}) collective-permute-start(bf16[16,4096]{1,0:T(8,128)(2,1)S(1)} %get-tuple-element.56), channel_id=1, source_target_pairs={{0,8},{8,16},{16,24},{24,28},{28,20},{20,12},{12,4},{4,0},{1,9},{9... | collective-permute-start | bytes 393224 | tf_op jit(solution)/shard_map/ppermute | solution.py:643
  108.3 6.4 %collective-permute-start.36 = (bf16[16,4096]{1,0:T(8,128)(2,1)S(1)}, bf16[16,4096]{1,0:T(8,128)(2,1)S(1)}, u32[]{:S(2)}, u32[]{:S(2)}) collective-permute-start(bf16[16,4096]{1,0:T(8,128)(2,1)S(1)} %get-tuple-element.53), channel_id=1, source_target_pairs={{8,0},{16,8},{24,16},{28,24},{20,28},{12,20},{4,12},{0,4},{9,1},{1... | collective-permute-start | bytes 393224 | tf_op jit(solution)/shard_map/ppermute | solution.py:644
  108.3 6.3 %collective-permute-start.27 = (bf16[16,4096]{1,0:T(8,128)(2,1)S(1)}, bf16[16,4096]{1,0:T(8,128)(2,1)S(1)}, u32[]{:S(2)}, u32[]{:S(2)}) collective-permute-start(bf16[16,4096]{1,0:T(8,128)(2,1)S(1)} %slice.64), channel_id=1, source_target_pairs={{0,8},{8,16},{16,24},{24,28},{28,20},{20,12},{12,4},{4,0},{1,9},{9... | collective-permute-start | bytes 393224 | tf_op jit(solution)/shard_map/ppermute | solution.py:643
  111.1 6.5 %collective-permute-start.28 = (bf16[16,4096]{1,0:T(8,128)(2,1)S(1)}, bf16[16,4096]{1,0:T(8,128)(2,1)S(1)}, u32[]{:S(2)}, u32[]{:S(2)}) collective-permute-start(bf16[16,4096]{1,0:T(8,128)(2,1)S(1)} %slice.65), channel_id=1, source_target_pairs={{8,0},{16,8},{24,16},{28,24},{20,28},{12,20},{4,12},{0,4},{9,1},{1... | collective-permute-start | bytes 393224 | tf_op jit(solution)/shard_map/ppermute | solution.py:644
  111.9 8.8 %collective-permute-start.34 = (bf16[16,4096]{1,0:T(8,128)(2,1)S(1)}, bf16[16,4096]{1,0:T(8,128)(2,1)S(1)}, u32[]{:S(2)}, u32[]{:S(2)}) collective-permute-start(bf16[16,4096]{1,0:T(8,128)(2,1)S(1)} %get-tuple-element.55), channel_id=1, source_target_pairs={{0,8},{8,16},{16,24},{24,28},{28,20},{20,12},{12,4},{4,0},{1,9},{9... | collective-permute-start | bytes 393224 | tf_op jit(solution)/shard_map/ppermute | solution.py:643
  114.6 6.0 %collective-permute-start.35 = (bf16[16,4096]{1,0:T(8,128)(2,1)S(1)}, bf16[16,4096]{1,0:T(8,128)(2,1)S(1)}, u32[]{:S(2)}, u32[]{:S(2)}) collective-permute-start(bf16[16,4096]{1,0:T(8,128)(2,1)S(1)} %get-tuple-element.54), channel_id=1, source_target_pairs={{8,0},{16,8},{24,16},{28,24},{20,28},{12,20},{4,12},{0,4},{9,1},{1... | collective-permute-start | bytes 393224 | tf_op jit(solution)/shard_map/ppermute | solution.py:644
  114.6 6.0 %collective-permute-start.37 = (bf16[16,4096]{1,0:T(8,128)(2,1)S(1)}, bf16[16,4096]{1,0:T(8,128)(2,1)S(1)}, u32[]{:S(2)}, u32[]{:S(2)}) collective-permute-start(bf16[16,4096]{1,0:T(8,128)(2,1)S(1)} %collective-permute-done.33.refs_7_), channel_id=1, source_target_pairs={{0,8},{8,16},{16,24},{24,28},{28,20},{20,12},{12,4},{4,0},{1,9},{9... | collective-permute-start | bytes 393224 | tf_op jit(solution)/shard_map/ppermute | solution.py:643
  117.6 5.0 %collective-permute-start.38 = (bf16[16,4096]{1,0:T(8,128)(2,1)S(1)}, bf16[16,4096]{1,0:T(8,128)(2,1)S(1)}, u32[]{:S(2)}, u32[]{:S(2)}) collective-permute-start(bf16[16,4096]{1,0:T(8,128)(2,1)S(1)} %collective-permute-done.36.refs_10_), channel_id=1, source_target_pairs={{8,0},{16,8},{24,16},{28,24},{20,28},{12,20},{4,12},{0,4},{9,1},{1... | collective-permute-start | bytes 393224 | tf_op jit(solution)/shard_map/ppermute | solution.py:644
  123.3 2.0 %collective-permute-start.41 = (bf16[128,2048]{1,0:T(8,128)(2,1)S(1)}, bf16[128,2048]{1,0:T(8,128)(2,1)S(1)}, u32[]{:S(2)}, u32[]{:S(2)}) collective-permute-start(bf16[128,2048]{1,0:T(8,128)(2,1)S(1)} %get-tuple-element.50), channel_id=1, source_target_pairs={{0,1},{1,0},{2,3},{3,2},{4,5},{5,4},{6,7},{7,6},{8,9},{9,8},{10,11... | collective-permute-start | bytes 1572872 | tf_op jit(solution)/shard_map/ppermute | solution.py:676
  124.1 2.9 %collective-permute-start.39 = (bf16[128,2048]{1,0:T(8,128)(2,1)S(1)}, bf16[128,2048]{1,0:T(8,128)(2,1)S(1)}, u32[]{:S(2)}, u32[]{:S(2)}) collective-permute-start(bf16[128,2048]{1,0:T(8,128)(2,1)S(1)} %get-tuple-element.48), channel_id=1, source_target_pairs={{0,1},{1,0},{2,3},{3,2},{4,5},{5,4},{6,7},{7,6},{8,9},{9,8},{10,11... | collective-permute-start | bytes 1572872 | tf_op jit(solution)/shard_map/ppermute | solution.py:676
  125.5 9.2 %collective-permute-start.42 = (bf16[64,2048]{1,0:T(8,128)(2,1)S(1)}, bf16[64,2048]{1,0:T(8,128)(2,1)S(1)}, u32[]{:S(2)}, u32[]{:S(2)}) collective-permute-start(bf16[64,2048]{1,0:T(8,128)(2,1)S(1)} %slice.74), channel_id=1, source_target_pairs={{0,2},{1,3},{2,0},{3,1},{4,6},{5,7},{6,4},{7,5},{8,10},{9,11},{10,... | collective-permute-start | bytes 786440 | tf_op jit(solution)/shard_map/ppermute | solution.py:676
  127.2 12.3 %collective-permute-start.40 = (bf16[64,2048]{1,0:T(8,128)(2,1)S(1)}, bf16[64,2048]{1,0:T(8,128)(2,1)S(1)}, u32[]{:S(2)}, u32[]{:S(2)}) collective-permute-start(bf16[64,2048]{1,0:T(8,128)(2,1)S(1)} %slice.75), channel_id=1, source_target_pairs={{0,2},{1,3},{2,0},{3,1},{4,6},{5,7},{6,4},{7,5},{8,10},{9,11},{10,... | collective-permute-start | bytes 786440 | tf_op jit(solution)/shard_map/ppermute | solution.py:676
  (6 other events, 18.6 us)

commit v5 on v4

--- a/solution.py
+++ b/solution.py
@@ -632,11 +632,33 @@
     )(*operands)
 
 
-def norm_rows(resid, gain):
-    stream = resid.astype(jnp.float32)
-    return (
-        stream * lax.rsqrt(jnp.mean(stream * stream, axis=-1, keepdims=True) + 1e-06) * gain
-    ).astype(jnp.bfloat16)
+def norm_kernel(pair_ref, met_ref, gain_ref, resid_ref, out_ref):
+    rows = resid_ref.shape[0]
+    for mine, theirs in ((0, 1), (1, 0)):
+        here = slice(mine * rows, (mine + 1) * rows)
+        there = slice(theirs * rows, (theirs + 1) * rows)
+        total = pair_ref[here].astype(jnp.float32) + met_ref[there].astype(jnp.float32)
+        resid = total.astype(jnp.bfloat16)
+        if mine == 0:
+            resid_ref[...] = resid
+        stream = resid.astype(jnp.float32)
+        square = jnp.mean(stream * stream, axis=1, keepdims=True)
+        out_ref[here] = (stream * lax.rsqrt(square + 1e-06) * gain_ref[...]).astype(jnp.bfloat16)
+
+
+def norm_call(pair, met, gain):
+    rows, width = pair.shape
+    return pl.pallas_call(
+        norm_kernel,
+        out_shape=[
+            pltpu.VMEM((rows // 2, width), jnp.bfloat16),
+            jax.ShapeDtypeStruct((rows, width), jnp.bfloat16),
+        ],
+        in_specs=specs(VMEM, 3),
+        out_specs=specs(VMEM, 2),
+        compiler_params=pltpu.CompilerParams(vmem_limit_bytes=6 * MIB),
+        name="norm",
+    )(pair, met, gain.reshape(1, width))
 
 
 def ring_step(ahead, back, pairs):
@@ -745,12 +767,7 @@
         [whole(s_gate)],
         [whole(s_up)],
     )
-    resid = (
-        pair.astype(jnp.float32)
-        + jnp.concatenate([met[own_rows:], met[:own_rows]]).astype(jnp.float32)
-    ).astype(jnp.bfloat16)
-    resid = lax.optimization_barrier(resid)
-    normed = norm_rows(resid, norm_gain)
+    resid, normed = norm_call(pair, met, norm_gain)
     other = swap(normed, cores)
     hidden = hidden_call(
         ids, normed, other, combine, [*ups, up_low, up_high], gate_all, sg, su, unit

time: 141 us -> 140 us (level)
    ppermute x17, waiting for transfers between devices: 24 us -> 26.4 us  [ring_step(): ahead = lax.ppermute(ahead, 'sp', pairs[0])]
    ppermute x17, starting transfers between devices: 32.8 us -> 31.1 us  [ring_step(): ahead = lax.ppermute(ahead, 'sp', pairs[0])]
    ppermute x17, waiting for transfers between devices: 17.8 us -> 16.2 us  [ring_step(): back = lax.ppermute(back, 'sp', pairs[1])]
  transfers between devices with their start and end apart: 43 -> 43, of which waited for: 22 -> 22; matrix products, arithmetic and copies ran while one was open for 2% -> 1% of each run, Pallas kernels for 6% -> 7%
where the time goes in v5:
time: 140 us
  waiting for transfers between devices  74.8 us (53%)
  starting transfers between devices  45.4 us (32%)
  Pallas kernels  15.8 us (11%)
  local copies, waits for them, and re-layouts  2.9 us (2%)
    ppermute x9, waiting for transfers between devices, swap(): return lax.ppermute(rows, 'tp', pairs)  32.3 us
    ppermute x17, starting transfers between devices, ring_step(): ahead = lax.ppermute(ahead, 'sp', pairs[0])  31.1 us
    ppermute x17, waiting for transfers between devices, ring_step(): ahead = lax.ppermute(ahead, 'sp', pairs[0])  26.4 us
    ppermute x17, waiting for transfers between devices, ring_step(): back = lax.ppermute(back, 'sp', pairs[1])  16.2 us
    ppermute x17, starting transfers between devices, ring_step(): back = lax.ppermute(back, 'sp', pairs[1])  8.59 us
    pallas_call x4, Pallas kernels, attn_call(): pl.pallas_call(body, out_shape=out_shape, in_specs=specs(SMEM, smem) + sp...  6.06 us
    ppermute x9, starting transfers between devices, swap(): return lax.ppermute(rows, 'tp', pairs)  5.7 us
    pallas_call x1, Pallas kernels, hidden_call(): pl.pallas_call(lambda *refs: hidden_kernel(unit, *refs), out_shape=pltpu....  2.97 us
  transfers between devices with their start and end apart: 43, of which 22 were waited for; matrix products, arithmetic and copies ran while one was open for 1% of the time, Pallas kernels for 7%

profile of v5, /device:TPU:0, one launch (start us, length us, event | category | flops | bytes accessed | tf_op | source)
XLA Modules:
  0.0 139.9 jit_solution(241046137642259415)
XLA Ops:
  0.0 1.0 pack.1.refs_3_
  1.0 3.1 %collective-permute-start = (bf16[256,512]{1,0:T(8,128)(2,1)S(1)}, bf16[256,512]{1,0:T(8,128)(2,1)S(1)}, u32[]{:S(2)}, u32[]{:S(2)}) collective-permute-start(bf16[256,512]{1,0:T(8,128)(2,1)S(1)} %pack.1.refs_3_), channel_id=1, source_target_pairs={{0,8},{8,16},{16,24},{24,28},{28,20},{20,12},{12,4},{4,0},{1,9},{9... | collective-permute-start | bytes 786440 | tf_op jit(solution)/shard_map/ppermute | solution.py:665
  4.1 6.2 %collective-permute-done.refs_4_ = bf16[256,512]{1,0:T(8,128)(2,1)S(1)} collective-permute-done((bf16[256,512]{1,0:T(8,128)(2,1)S(1)}, bf16[256,512]{1,0:T(8,128)(2,1)S(1)}, u32[]{:S(2)}, u32[]{:S(2)}) %collective-permute-start) | collective-permute-done | bytes 262176 | tf_op jit(solution)/shard_map/ppermute | solution.py:665
  10.4 1.8 %collective-permute-start.2 = (bf16[256,512]{1,0:T(8,128)(2,1)S(1)}, bf16[256,512]{1,0:T(8,128)(2,1)S(1)}, u32[]{:S(2)}, u32[]{:S(2)}) collective-permute-start(bf16[256,512]{1,0:T(8,128)(2,1)S(1)} %collective-permute-done.refs_4_), channel_id=1, source_target_pairs={{0,8},{8,16},{16,24},{24,28},{28,20},{20,12},{12,4},{4,0},{1,9},{9... | collective-permute-start | bytes 786440 | tf_op jit(solution)/shard_map/ppermute | solution.py:665
  12.4 5.4 %collective-permute-done.2.refs_3_ = bf16[256,512]{1,0:T(8,128)(2,1)S(1)} collective-permute-done((bf16[256,512]{1,0:T(8,128)(2,1)S(1)}, bf16[256,512]{1,0:T(8,128)(2,1)S(1)}, u32[]{:S(2)}, u32[]{:S(2)}) %collective-permute-start.2) | collective-permute-done | bytes 262176 | tf_op jit(solution)/shard_map/ppermute | solution.py:665
  17.8 1.5 %collective-permute-start.3 = (bf16[256,512]{1,0:T(8,128)(2,1)S(1)}, bf16[256,512]{1,0:T(8,128)(2,1)S(1)}, u32[]{:S(2)}, u32[]{:S(2)}) collective-permute-start(bf16[256,512]{1,0:T(8,128)(2,1)S(1)} %collective-permute-done.2.refs_3_), channel_id=1, source_target_pairs={{0,8},{8,16},{16,24},{24,28},{28,20},{20,12},{12,4},{4,0},{1,9},{9... | collective-permute-start | bytes 786440 | tf_op jit(solution)/shard_map/ppermute | solution.py:665
  20.6 0.9 copy-done.7
  21.5 0.9 copy-done.8
  22.4 1.2 shard_map.172
  23.6 0.8 collective-permute-done.3.refs_3_
  24.5 1.5 %collective-permute-start.4 = (bf16[128,512]{1,0:T(8,128)(2,1)S(1)}, bf16[128,512]{1,0:T(8,128)(2,1)S(1)}, u32[]{:S(2)}, u32[]{:S(2)}) collective-permute-start(bf16[128,512]{1,0:T(8,128)(2,1)S(1)} %slice.50), channel_id=1, source_target_pairs={{0,8},{8,16},{16,24},{24,28},{28,20},{20,12},{12,4},{4,0},{1,9},{9... | collective-permute-start | bytes 393224 | tf_op jit(solution)/shard_map/ppermute | solution.py:665
  28.0 1.4 %collective-permute-done.4.refs_4_ = bf16[128,512]{1,0:T(8,128)(2,1)S(1)} collective-permute-done((bf16[128,512]{1,0:T(8,128)(2,1)S(1)}, bf16[128,512]{1,0:T(8,128)(2,1)S(1)}, u32[]{:S(2)}, u32[]{:S(2)}) %collective-permute-start.4) | collective-permute-done | bytes 131104 | tf_op jit(solution)/shard_map/ppermute | solution.py:665
  29.5 1.5 %collective-permute-done.7.refs_5_ = bf16[128,512]{1,0:T(8,128)(2,1)S(1)} collective-permute-done((bf16[128,512]{1,0:T(8,128)(2,1)S(1)}, bf16[128,512]{1,0:T(8,128)(2,1)S(1)}, u32[]{:S(2)}, u32[]{:S(2)}) %collective-permute-start.7) | collective-permute-done | bytes 131104 | tf_op jit(solution)/shard_map/ppermute | solution.py:666
  31.0 3.5 %shard_map.175 = (f32[128,4096]{1,0:T(8,128)S(1)}, bf16[128,4096]{1,0:T(8,128)(2,1)S(1)}) custom-call(s32[10]{0:T(128)S(1)} %pad_add_fusion.refs_0_, f32[2]{0:T(128)S(1)} %copy-done.6, bf16[256,256]{1,0:T(8,128)(2,1)S(1)} %get-tuple-element.30.refs_1_.refs_2_, bf16[256,256]{1,0:T(8,128)(2,1)S(1)} %get-tuple-element.31.refs_2_.refs_3_, ...), custom_call_target="tpu_custom_call" | custom-call | flops 402653184 | bytes 4194304 | tf_op jit(solution)/shard_map/pallas_call | solution.py:396
  34.6 2.6 %collective-permute-done.8 = bf16[128,4096]{1,0:T(8,128)(2,1)S(1)} collective-permute-done((bf16[128,4096]{1,0:T(8,128)(2,1)S(1)}, bf16[128,4096]{1,0:T(8,128)(2,1)S(1)}, u32[]{:S(2)}, u32[]{:S(2)}) %collective-permute-start.8) | collective-permute-done | bytes 1048608 | tf_op jit(solution)/shard_map/ppermute | solution.py:698
  37.6 1.6 %collective-permute-start.9 = (bf16[128,4096]{1,0:T(8,128)(2,1)S(1)}, bf16[128,4096]{1,0:T(8,128)(2,1)S(1)}, u32[]{:S(2)}, u32[]{:S(2)}) collective-permute-start(bf16[128,4096]{1,0:T(8,128)(2,1)S(1)} %add_convert_fusion.pair_ref), channel_id=1, source_target_pairs={{0,2},{1,3},{2,0},{3,1},{4,6},{5,7},{6,4},{7,5},{8,10},{9,11},{10,... | collective-permute-start | bytes 3145736 | tf_op jit(solution)/shard_map/ppermute | solution.py:698
  39.1 1.9 %slices.1 = (bf16[32,4096]{1,0:T(8,128)(2,1)S(1)}, bf16[32,4096]{1,0:T(8,128)(2,1)S(1)}, bf16[32,4096]{1,0:T(8,128)(2,1)S(1)}) custom-call(s32[1]{0:T(128)} %bitcast.1.refs_0_, bf16[4096,128]{1,0:T(8,128)(2,1)} %bitcast.9, bf16[4096,128]{1,0:T(8,128)(2,1)} %bitcast.10, bf16[128,4096]{1,0:T(8,128)(2,1)} %bitcast.11), custom_call_target="tpu_custom_call" | custom-call | tf_op jit(solution)/shard_map/slices/pallas_call | solution.py:454
  41.1 1.6 %collective-permute-start.13 = (bf16[32,4096]{1,0:T(8,128)(2,1)S(1)}, bf16[32,4096]{1,0:T(8,128)(2,1)S(1)}, u32[]{:S(2)}, u32[]{:S(2)}) collective-permute-start(bf16[32,4096]{1,0:T(8,128)(2,1)S(1)} %get-tuple-element.45.refs_0_), channel_id=1, source_target_pairs={{0,8},{8,16},{16,24},{24,28},{28,20},{20,12},{12,4},{4,0},{1,9},{9... | collective-permute-start | bytes 786440 | tf_op jit(solution)/shard_map/ppermute | solution.py:665
  44.1 2.0 %collective-permute-start.21 = (bf16[32,4096]{1,0:T(8,128)(2,1)S(1)}, bf16[32,4096]{1,0:T(8,128)(2,1)S(1)}, u32[]{:S(2)}, u32[]{:S(2)}) collective-permute-start(bf16[32,4096]{1,0:T(8,128)(2,1)S(1)} %get-tuple-element.49.refs_8_), channel_id=1, source_target_pairs={{0,8},{8,16},{16,24},{24,28},{28,20},{20,12},{12,4},{4,0},{1,9},{9... | collective-permute-start | bytes 786440 | tf_op jit(solution)/shard_map/ppermute | solution.py:665
  46.1 17.5 %collective-permute-done.11 = f32[64,128]{1,0:T(8,128)S(1)} collective-permute-done((f32[64,128]{1,0:T(8,128)S(1)}, f32[64,128]{1,0:T(8,128)S(1)}, u32[]{:S(2)}, u32[]{:S(2)}) %collective-permute-start.11) | collective-permute-done | bytes 32800 | tf_op jit(solution)/shard_map/ppermute | solution.py:698
  64.1 1.5 %collective-permute-start.29 = (bf16[32,4096]{1,0:T(8,128)(2,1)S(1)}, bf16[32,4096]{1,0:T(8,128)(2,1)S(1)}, u32[]{:S(2)}, u32[]{:S(2)}) collective-permute-start(bf16[32,4096]{1,0:T(8,128)(2,1)S(1)} %get-tuple-element.50.refs_2_), channel_id=1, source_target_pairs={{0,8},{8,16},{16,24},{24,28},{28,20},{20,12},{12,4},{4,0},{1,9},{9... | collective-permute-start | bytes 786440 | tf_op jit(solution)/shard_map/ppermute | solution.py:665
  65.6 2.0 %collective-permute-start.15 = (bf16[32,4096]{1,0:T(8,128)(2,1)S(1)}, bf16[32,4096]{1,0:T(8,128)(2,1)S(1)}, u32[]{:S(2)}, u32[]{:S(2)}) collective-permute-start(bf16[32,4096]{1,0:T(8,128)(2,1)S(1)} %collective-permute-done.13.refs_1_), channel_id=1, source_target_pairs={{0,8},{8,16},{16,24},{24,28},{28,20},{20,12},{12,4},{4,0},{1,9},{9... | collective-permute-start | bytes 786440 | tf_op jit(solution)/shard_map/ppermute | solution.py:665
  67.6 5.1 %collective-permute-done.22.refs_10_ = bf16[32,4096]{1,0:T(8,128)(2,1)S(1)} collective-permute-done((bf16[32,4096]{1,0:T(8,128)(2,1)S(1)}, bf16[32,4096]{1,0:T(8,128)(2,1)S(1)}, u32[]{:S(2)}, u32[]{:S(2)}) %collective-permute-start.22) | collective-permute-done | bytes 262176 | tf_op jit(solution)/shard_map/ppermute | solution.py:666
  73.3 1.5 %collective-permute-start.23 = (bf16[32,4096]{1,0:T(8,128)(2,1)S(1)}, bf16[32,4096]{1,0:T(8,128)(2,1)S(1)}, u32[]{:S(2)}, u32[]{:S(2)}) collective-permute-start(bf16[32,4096]{1,0:T(8,128)(2,1)S(1)} %collective-permute-done.21.refs_9_), channel_id=1, source_target_pairs={{0,8},{8,16},{16,24},{24,28},{28,20},{20,12},{12,4},{4,0},{1,9},{9... | collective-permute-start | bytes 786440 | tf_op jit(solution)/shard_map/ppermute | solution.py:665
  74.7 4.2 %collective-permute-done.15.refs_3_ = bf16[32,4096]{1,0:T(8,128)(2,1)S(1)} collective-permute-done((bf16[32,4096]{1,0:T(8,128)(2,1)S(1)}, bf16[32,4096]{1,0:T(8,128)(2,1)S(1)}, u32[]{:S(2)}, u32[]{:S(2)}) %collective-permute-start.15) | collective-permute-done | bytes 262176 | tf_op jit(solution)/shard_map/ppermute | solution.py:665
  78.9 1.5 %collective-permute-start.31 = (bf16[32,4096]{1,0:T(8,128)(2,1)S(1)}, bf16[32,4096]{1,0:T(8,128)(2,1)S(1)}, u32[]{:S(2)}, u32[]{:S(2)}) collective-permute-start(bf16[32,4096]{1,0:T(8,128)(2,1)S(1)} %collective-permute-done.29.refs_3_), channel_id=1, source_target_pairs={{0,8},{8,16},{16,24},{24,28},{28,20},{20,12},{12,4},{4,0},{1,9},{9... | collective-permute-start | bytes 786440 | tf_op jit(solution)/shard_map/ppermute | solution.py:665
  80.4 2.0 %collective-permute-start.17 = (bf16[32,4096]{1,0:T(8,128)(2,1)S(1)}, bf16[32,4096]{1,0:T(8,128)(2,1)S(1)}, u32[]{:S(2)}, u32[]{:S(2)}) collective-permute-start(bf16[32,4096]{1,0:T(8,128)(2,1)S(1)} %collective-permute-done.15.refs_3_), channel_id=1, source_target_pairs={{0,8},{8,16},{16,24},{24,28},{28,20},{20,12},{12,4},{4,0},{1,9},{9... | collective-permute-start | bytes 786440 | tf_op jit(solution)/shard_map/ppermute | solution.py:665
  83.1 1.2 collective-permute-start.32
  84.5 2.0 %collective-permute-start.18 = (bf16[32,4096]{1,0:T(8,128)(2,1)S(1)}, bf16[32,4096]{1,0:T(8,128)(2,1)S(1)}, u32[]{:S(2)}, u32[]{:S(2)}) collective-permute-start(bf16[32,4096]{1,0:T(8,128)(2,1)S(1)} %collective-permute-done.16.refs_4_), channel_id=1, source_target_pairs={{8,0},{16,8},{24,16},{28,24},{20,28},{12,20},{4,12},{0,4},{9,1},{1... | collective-permute-start | bytes 786440 | tf_op jit(solution)/shard_map/ppermute | solution.py:666
  86.5 3.6 %collective-permute-done.31.refs_5_ = bf16[32,4096]{1,0:T(8,128)(2,1)S(1)} collective-permute-done((bf16[32,4096]{1,0:T(8,128)(2,1)S(1)}, bf16[32,4096]{1,0:T(8,128)(2,1)S(1)}, u32[]{:S(2)}, u32[]{:S(2)}) %collective-permute-start.31) | collective-permute-done | bytes 262176 | tf_op jit(solution)/shard_map/ppermute | solution.py:665
  90.1 1.5 %collective-permute-start.25 = (bf16[32,4096]{1,0:T(8,128)(2,1)S(1)}, bf16[32,4096]{1,0:T(8,128)(2,1)S(1)}, u32[]{:S(2)}, u32[]{:S(2)}) collective-permute-start(bf16[32,4096]{1,0:T(8,128)(2,1)S(1)} %collective-permute-done.23.refs_11_), channel_id=1, source_target_pairs={{0,8},{8,16},{16,24},{24,28},{28,20},{20,12},{12,4},{4,0},{1,9},{9... | collective-permute-start | bytes 786440 | tf_op jit(solution)/shard_map/ppermute | solution.py:665
  91.6 4.2 %collective-permute-done.17.refs_5_ = bf16[32,4096]{1,0:T(8,128)(2,1)S(1)} collective-permute-done((bf16[32,4096]{1,0:T(8,128)(2,1)S(1)}, bf16[32,4096]{1,0:T(8,128)(2,1)S(1)}, u32[]{:S(2)}, u32[]{:S(2)}) %collective-permute-start.17) | collective-permute-done | bytes 262176 | tf_op jit(solution)/shard_map/ppermute | solution.py:665
  96.4 2.8 %collective-permute-done.18.refs_6_ = bf16[32,4096]{1,0:T(8,128)(2,1)S(1)} collective-permute-done((bf16[32,4096]{1,0:T(8,128)(2,1)S(1)}, bf16[32,4096]{1,0:T(8,128)(2,1)S(1)}, u32[]{:S(2)}, u32[]{:S(2)}) %collective-permute-start.18) | collective-permute-done | bytes 262176 | tf_op jit(solution)/shard_map/ppermute | solution.py:666
  99.7 2.4 %collective-permute-start.19 = (bf16[16,4096]{1,0:T(8,128)(2,1)S(1)}, bf16[16,4096]{1,0:T(8,128)(2,1)S(1)}, u32[]{:S(2)}, u32[]{:S(2)}) collective-permute-start(bf16[16,4096]{1,0:T(8,128)(2,1)S(1)} %slice.52), channel_id=1, source_target_pairs={{0,8},{8,16},{16,24},{24,28},{28,20},{20,12},{12,4},{4,0},{1,9},{9... | collective-permute-start | bytes 393224 | tf_op jit(solution)/shard_map/ppermute | solution.py:665
  102.1 2.1 %collective-permute-start.33 = (bf16[16,4096]{1,0:T(8,128)(2,1)S(1)}, bf16[16,4096]{1,0:T(8,128)(2,1)S(1)}, u32[]{:S(2)}, u32[]{:S(2)}) collective-permute-start(bf16[16,4096]{1,0:T(8,128)(2,1)S(1)} %get-tuple-element.58), channel_id=1, source_target_pairs={{0,8},{8,16},{16,24},{24,28},{28,20},{20,12},{12,4},{4,0},{1,9},{9... | collective-permute-start | bytes 393224 | tf_op jit(solution)/shard_map/ppermute | solution.py:665
  104.2 3.5 %collective-permute-done.26.refs_14_ = bf16[32,4096]{1,0:T(8,128)(2,1)S(1)} collective-permute-done((bf16[32,4096]{1,0:T(8,128)(2,1)S(1)}, bf16[32,4096]{1,0:T(8,128)(2,1)S(1)}, u32[]{:S(2)}, u32[]{:S(2)}) %collective-permute-start.26) | collective-permute-done | bytes 262176 | tf_op jit(solution)/shard_map/ppermute | solution.py:666
  108.1 1.9 %collective-permute-start.27 = (bf16[16,4096]{1,0:T(8,128)(2,1)S(1)}, bf16[16,4096]{1,0:T(8,128)(2,1)S(1)}, u32[]{:S(2)}, u32[]{:S(2)}) collective-permute-start(bf16[16,4096]{1,0:T(8,128)(2,1)S(1)} %slice.54), channel_id=1, source_target_pairs={{0,8},{8,16},{16,24},{24,28},{28,20},{20,12},{12,4},{4,0},{1,9},{9... | collective-permute-start | bytes 393224 | tf_op jit(solution)/shard_map/ppermute | solution.py:665
  110.8 0.7 stack.9
  111.5 2.1 %collective-permute-start.34 = (bf16[16,4096]{1,0:T(8,128)(2,1)S(1)}, bf16[16,4096]{1,0:T(8,128)(2,1)S(1)}, u32[]{:S(2)}, u32[]{:S(2)}) collective-permute-start(bf16[16,4096]{1,0:T(8,128)(2,1)S(1)} %get-tuple-element.57), channel_id=1, source_target_pairs={{0,8},{8,16},{16,24},{24,28},{28,20},{20,12},{12,4},{4,0},{1,9},{9... | collective-permute-start | bytes 393224 | tf_op jit(solution)/shard_map/ppermute | solution.py:665
  114.7 1.3 collective-permute-start.37
  116.0 1.1 collective-permute-done.28.refs_16_
  117.5 3.0 %hidden.1.refs_0_ = bf16[256,384]{1,0:T(8,128)(2,1)S(1)} custom-call(s32[10]{0:T(128)S(1)} %pad_add_fusion.refs_0_, bf16[128,4096]{1,0:T(8,128)(2,1)S(1)} %get-tuple-element.44.refs_1_, bf16[128,4096]{1,0:T(8,128)(2,1)S(1)} %collective-permute-done.10.refs_2_, f32[128,128]{1,0:T(8,128)S(1)} %pad_maximum_fusion.refs_3_, ...), custom_call_target="tpu_custom_call" | custom-call | flops 1610612736 | bytes 12582912 | tf_op jit(solution)/shard_map/hidden/pallas_call | solution.py:567
  120.5 1.6 %collective-permute-done.38.refs_12_ = bf16[16,4096]{1,0:T(8,128)(2,1)S(1)} collective-permute-done((bf16[16,4096]{1,0:T(8,128)(2,1)S(1)}, bf16[16,4096]{1,0:T(8,128)(2,1)S(1)}, u32[]{:S(2)}, u32[]{:S(2)}) %collective-permute-start.38) | collective-permute-done | bytes 131104 | tf_op jit(solution)/shard_map/ppermute | solution.py:666
  124.9 1.6 %collective-permute-start.42 = (bf16[64,2048]{1,0:T(8,128)(2,1)S(1)}, bf16[64,2048]{1,0:T(8,128)(2,1)S(1)}, u32[]{:S(2)}, u32[]{:S(2)}) collective-permute-start(bf16[64,2048]{1,0:T(8,128)(2,1)S(1)} %slice.64), channel_id=1, source_target_pairs={{0,2},{1,3},{2,0},{3,1},{4,6},{5,7},{6,4},{7,5},{8,10},{9,11},{10,... | collective-permute-start | bytes 786440 | tf_op jit(solution)/shard_map/ppermute | solution.py:698
  126.6 0.7 collective-permute-start.40
  127.4 6.8 %collective-permute-done.42.refs_3_ = bf16[64,2048]{1,0:T(8,128)(2,1)S(1)} collective-permute-done((bf16[64,2048]{1,0:T(8,128)(2,1)S(1)}, bf16[64,2048]{1,0:T(8,128)(2,1)S(1)}, u32[]{:S(2)}, u32[]{:S(2)}) %collective-permute-start.42) | collective-permute-done | bytes 262176 | tf_op jit(solution)/shard_map/ppermute | solution.py:698
  134.2 4.8 %collective-permute-done.40.refs_1_ = bf16[64,2048]{1,0:T(8,128)(2,1)S(1)} collective-permute-done((bf16[64,2048]{1,0:T(8,128)(2,1)S(1)}, bf16[64,2048]{1,0:T(8,128)(2,1)S(1)}, u32[]{:S(2)}, u32[]{:S(2)}) %collective-permute-start.40) | collective-permute-done | bytes 262176 | tf_op jit(solution)/shard_map/ppermute | solution.py:698
  139.0 1.0 final.1
  (91 shorter events, 14.1 us)
Async XLA Ops:
  1.0 9.4 %collective-permute-start = (bf16[256,512]{1,0:T(8,128)(2,1)S(1)}, bf16[256,512]{1,0:T(8,128)(2,1)S(1)}, u32[]{:S(2)}, u32[]{:S(2)}) collective-permute-start(bf16[256,512]{1,0:T(8,128)(2,1)S(1)} %pack.1.refs_3_), channel_id=1, source_target_pairs={{0,8},{8,16},{16,24},{24,28},{28,20},{20,12},{12,4},{4,0},{1,9},{9... | collective-permute-start | bytes 786440 | tf_op jit(solution)/shard_map/ppermute | solution.py:665
  4.1 8.0 %collective-permute-start.1 = (bf16[256,512]{1,0:T(8,128)(2,1)S(1)}, bf16[256,512]{1,0:T(8,128)(2,1)S(1)}, u32[]{:S(2)}, u32[]{:S(2)}) collective-permute-start(bf16[256,512]{1,0:T(8,128)(2,1)S(1)} %pack.1.refs_3_), channel_id=1, source_target_pairs={{8,0},{16,8},{24,16},{28,24},{20,28},{12,20},{4,12},{0,4},{9,1},{1... | collective-permute-start | bytes 786440 | tf_op jit(solution)/shard_map/ppermute | solution.py:666
  10.4 7.5 %collective-permute-start.2 = (bf16[256,512]{1,0:T(8,128)(2,1)S(1)}, bf16[256,512]{1,0:T(8,128)(2,1)S(1)}, u32[]{:S(2)}, u32[]{:S(2)}) collective-permute-start(bf16[256,512]{1,0:T(8,128)(2,1)S(1)} %collective-permute-done.refs_4_), channel_id=1, source_target_pairs={{0,8},{8,16},{16,24},{24,28},{28,20},{20,12},{12,4},{4,0},{1,9},{9... | collective-permute-start | bytes 786440 | tf_op jit(solution)/shard_map/ppermute | solution.py:665
  12.2 7.2 %collective-permute-start.5 = (bf16[256,512]{1,0:T(8,128)(2,1)S(1)}, bf16[256,512]{1,0:T(8,128)(2,1)S(1)}, u32[]{:S(2)}, u32[]{:S(2)}) collective-permute-start(bf16[256,512]{1,0:T(8,128)(2,1)S(1)} %collective-permute-done.1.refs_5_), channel_id=1, source_target_pairs={{8,0},{16,8},{24,16},{28,24},{20,28},{12,20},{4,12},{0,4},{9,1},{1... | collective-permute-start | bytes 786440 | tf_op jit(solution)/shard_map/ppermute | solution.py:666
  17.8 6.6 %collective-permute-start.3 = (bf16[256,512]{1,0:T(8,128)(2,1)S(1)}, bf16[256,512]{1,0:T(8,128)(2,1)S(1)}, u32[]{:S(2)}, u32[]{:S(2)}) collective-permute-start(bf16[256,512]{1,0:T(8,128)(2,1)S(1)} %collective-permute-done.2.refs_3_), channel_id=1, source_target_pairs={{0,8},{8,16},{16,24},{24,28},{28,20},{20,12},{12,4},{4,0},{1,9},{9... | collective-permute-start | bytes 786440 | tf_op jit(solution)/shard_map/ppermute | solution.py:665
  19.4 6.6 %collective-permute-start.6 = (bf16[256,512]{1,0:T(8,128)(2,1)S(1)}, bf16[256,512]{1,0:T(8,128)(2,1)S(1)}, u32[]{:S(2)}, u32[]{:S(2)}) collective-permute-start(bf16[256,512]{1,0:T(8,128)(2,1)S(1)} %collective-permute-done.5.refs_4_), channel_id=1, source_target_pairs={{8,0},{16,8},{24,16},{28,24},{20,28},{12,20},{4,12},{0,4},{9,1},{1... | collective-permute-start | bytes 786440 | tf_op jit(solution)/shard_map/ppermute | solution.py:666
  24.5 5.0 %collective-permute-start.4 = (bf16[128,512]{1,0:T(8,128)(2,1)S(1)}, bf16[128,512]{1,0:T(8,128)(2,1)S(1)}, u32[]{:S(2)}, u32[]{:S(2)}) collective-permute-start(bf16[128,512]{1,0:T(8,128)(2,1)S(1)} %slice.50), channel_id=1, source_target_pairs={{0,8},{8,16},{16,24},{24,28},{28,20},{20,12},{12,4},{4,0},{1,9},{9... | collective-permute-start | bytes 393224 | tf_op jit(solution)/shard_map/ppermute | solution.py:665
  26.0 5.0 %collective-permute-start.7 = (bf16[128,512]{1,0:T(8,128)(2,1)S(1)}, bf16[128,512]{1,0:T(8,128)(2,1)S(1)}, u32[]{:S(2)}, u32[]{:S(2)}) collective-permute-start(bf16[128,512]{1,0:T(8,128)(2,1)S(1)} %slice.51), channel_id=1, source_target_pairs={{8,0},{16,8},{24,16},{28,24},{20,28},{12,20},{4,12},{0,4},{9,1},{1... | collective-permute-start | bytes 393224 | tf_op jit(solution)/shard_map/ppermute | solution.py:666
  34.5 2.7 %collective-permute-start.8 = (bf16[128,4096]{1,0:T(8,128)(2,1)S(1)}, bf16[128,4096]{1,0:T(8,128)(2,1)S(1)}, u32[]{:S(2)}, u32[]{:S(2)}) collective-permute-start(bf16[128,4096]{1,0:T(8,128)(2,1)S(1)} %get-tuple-element.42), channel_id=1, source_target_pairs={{0,1},{1,0},{2,3},{3,2},{4,5},{5,4},{6,7},{7,6},{8,9},{9,8},{10,11... | collective-permute-start | bytes 3145736 | tf_op jit(solution)/shard_map/ppermute | solution.py:698
  37.5 5.6 %copy-start.9 = (s32[64,4]{0,1:T(4,128)S(1)}, s32[64,4]{0,1:T(4,128)}, u32[]{:S(2)}) copy-start(s32[64,4]{0,1:T(4,128)} %param.27) | copy-start | bytes 3076
  37.5 5.7 %copy-start.10 = (f32[64,4]{0,1:T(4,128)S(1)}, f32[64,4]{0,1:T(4,128)}, u32[]{:S(2)}) copy-start(f32[64,4]{0,1:T(4,128)} %param.28) | copy-start | bytes 3076
  37.5 44.8 %copy-start.5 = (f32[4096]{0:T(1024)S(1)}, f32[4096]{0:T(1024)}, u32[]{:S(2)}) copy-start(f32[4096]{0:T(1024)} %param.26) | copy-start | bytes 49156
  37.6 42.8 %collective-permute-start.9 = (bf16[128,4096]{1,0:T(8,128)(2,1)S(1)}, bf16[128,4096]{1,0:T(8,128)(2,1)S(1)}, u32[]{:S(2)}, u32[]{:S(2)}) collective-permute-start(bf16[128,4096]{1,0:T(8,128)(2,1)S(1)} %add_convert_fusion.pair_ref), channel_id=1, source_target_pairs={{0,2},{1,3},{2,0},{3,1},{4,6},{5,7},{6,4},{7,5},{8,10},{9,11},{10,... | collective-permute-start | bytes 3145736 | tf_op jit(solution)/shard_map/ppermute | solution.py:698
  41.1 23.0 %collective-permute-start.13 = (bf16[32,4096]{1,0:T(8,128)(2,1)S(1)}, bf16[32,4096]{1,0:T(8,128)(2,1)S(1)}, u32[]{:S(2)}, u32[]{:S(2)}) collective-permute-start(bf16[32,4096]{1,0:T(8,128)(2,1)S(1)} %get-tuple-element.45.refs_0_), channel_id=1, source_target_pairs={{0,8},{8,16},{16,24},{24,28},{28,20},{20,12},{12,4},{4,0},{1,9},{9... | collective-permute-start | bytes 786440 | tf_op jit(solution)/shard_map/ppermute | solution.py:665
  42.7 22.9 %collective-permute-start.14 = (bf16[32,4096]{1,0:T(8,128)(2,1)S(1)}, bf16[32,4096]{1,0:T(8,128)(2,1)S(1)}, u32[]{:S(2)}, u32[]{:S(2)}) collective-permute-start(bf16[32,4096]{1,0:T(8,128)(2,1)S(1)} %get-tuple-element.45.refs_0_), channel_id=1, source_target_pairs={{8,0},{16,8},{24,16},{28,24},{20,28},{12,20},{4,12},{0,4},{9,1},{1... | collective-permute-start | bytes 786440 | tf_op jit(solution)/shard_map/ppermute | solution.py:666
  43.5 20.0 %collective-permute-start.11 = (f32[64,128]{1,0:T(8,128)S(1)}, f32[64,128]{1,0:T(8,128)S(1)}, u32[]{:S(2)}, u32[]{:S(2)}) collective-permute-start(f32[64,128]{1,0:T(8,128)S(1)} %combine.1), channel_id=1, source_target_pairs={{0,2},{1,3},{2,0},{3,1},{4,6},{5,7},{6,4},{7,5},{8,10},{9,11},{10,... | collective-permute-start | bytes 98312 | tf_op jit(solution)/shard_map/ppermute | solution.py:698
  44.1 23.5 %collective-permute-start.21 = (bf16[32,4096]{1,0:T(8,128)(2,1)S(1)}, bf16[32,4096]{1,0:T(8,128)(2,1)S(1)}, u32[]{:S(2)}, u32[]{:S(2)}) collective-permute-start(bf16[32,4096]{1,0:T(8,128)(2,1)S(1)} %get-tuple-element.49.refs_8_), channel_id=1, source_target_pairs={{0,8},{8,16},{16,24},{24,28},{28,20},{20,12},{12,4},{4,0},{1,9},{9... | collective-permute-start | bytes 786440 | tf_op jit(solution)/shard_map/ppermute | solution.py:665
  63.5 9.2 %collective-permute-start.22 = (bf16[32,4096]{1,0:T(8,128)(2,1)S(1)}, bf16[32,4096]{1,0:T(8,128)(2,1)S(1)}, u32[]{:S(2)}, u32[]{:S(2)}) collective-permute-start(bf16[32,4096]{1,0:T(8,128)(2,1)S(1)} %get-tuple-element.49.refs_8_), channel_id=1, source_target_pairs={{8,0},{16,8},{24,16},{28,24},{20,28},{12,20},{4,12},{0,4},{9,1},{1... | collective-permute-start | bytes 786440 | tf_op jit(solution)/shard_map/ppermute | solution.py:666
  64.1 9.2 %collective-permute-start.29 = (bf16[32,4096]{1,0:T(8,128)(2,1)S(1)}, bf16[32,4096]{1,0:T(8,128)(2,1)S(1)}, u32[]{:S(2)}, u32[]{:S(2)}) collective-permute-start(bf16[32,4096]{1,0:T(8,128)(2,1)S(1)} %get-tuple-element.50.refs_2_), channel_id=1, source_target_pairs={{0,8},{8,16},{16,24},{24,28},{28,20},{20,12},{12,4},{4,0},{1,9},{9... | collective-permute-start | bytes 786440 | tf_op jit(solution)/shard_map/ppermute | solution.py:665
  65.6 13.3 %collective-permute-start.15 = (bf16[32,4096]{1,0:T(8,128)(2,1)S(1)}, bf16[32,4096]{1,0:T(8,128)(2,1)S(1)}, u32[]{:S(2)}, u32[]{:S(2)}) collective-permute-start(bf16[32,4096]{1,0:T(8,128)(2,1)S(1)} %collective-permute-done.13.refs_1_), channel_id=1, source_target_pairs={{0,8},{8,16},{16,24},{24,28},{28,20},{20,12},{12,4},{4,0},{1,9},{9... | collective-permute-start | bytes 786440 | tf_op jit(solution)/shard_map/ppermute | solution.py:665
  67.6 15.4 %collective-permute-start.30 = (bf16[32,4096]{1,0:T(8,128)(2,1)S(1)}, bf16[32,4096]{1,0:T(8,128)(2,1)S(1)}, u32[]{:S(2)}, u32[]{:S(2)}) collective-permute-start(bf16[32,4096]{1,0:T(8,128)(2,1)S(1)} %get-tuple-element.50.refs_2_), channel_id=1, source_target_pairs={{8,0},{16,8},{24,16},{28,24},{20,28},{12,20},{4,12},{0,4},{9,1},{1... | collective-permute-start | bytes 786440 | tf_op jit(solution)/shard_map/ppermute | solution.py:666
  72.7 10.4 %collective-permute-start.16 = (bf16[32,4096]{1,0:T(8,128)(2,1)S(1)}, bf16[32,4096]{1,0:T(8,128)(2,1)S(1)}, u32[]{:S(2)}, u32[]{:S(2)}) collective-permute-start(bf16[32,4096]{1,0:T(8,128)(2,1)S(1)} %collective-permute-done.14.refs_2_), channel_id=1, source_target_pairs={{8,0},{16,8},{24,16},{28,24},{20,28},{12,20},{4,12},{0,4},{9,1},{1... | collective-permute-start | bytes 786440 | tf_op jit(solution)/shard_map/ppermute | solution.py:666
  73.3 11.2 %collective-permute-start.23 = (bf16[32,4096]{1,0:T(8,128)(2,1)S(1)}, bf16[32,4096]{1,0:T(8,128)(2,1)S(1)}, u32[]{:S(2)}, u32[]{:S(2)}) collective-permute-start(bf16[32,4096]{1,0:T(8,128)(2,1)S(1)} %collective-permute-done.21.refs_9_), channel_id=1, source_target_pairs={{0,8},{8,16},{16,24},{24,28},{28,20},{20,12},{12,4},{4,0},{1,9},{9... | collective-permute-start | bytes 786440 | tf_op jit(solution)/shard_map/ppermute | solution.py:665
  78.9 11.2 %collective-permute-start.31 = (bf16[32,4096]{1,0:T(8,128)(2,1)S(1)}, bf16[32,4096]{1,0:T(8,128)(2,1)S(1)}, u32[]{:S(2)}, u32[]{:S(2)}) collective-permute-start(bf16[32,4096]{1,0:T(8,128)(2,1)S(1)} %collective-permute-done.29.refs_3_), channel_id=1, source_target_pairs={{0,8},{8,16},{16,24},{24,28},{28,20},{20,12},{12,4},{4,0},{1,9},{9... | collective-permute-start | bytes 786440 | tf_op jit(solution)/shard_map/ppermute | solution.py:665
  80.4 15.4 %collective-permute-start.17 = (bf16[32,4096]{1,0:T(8,128)(2,1)S(1)}, bf16[32,4096]{1,0:T(8,128)(2,1)S(1)}, u32[]{:S(2)}, u32[]{:S(2)}) collective-permute-start(bf16[32,4096]{1,0:T(8,128)(2,1)S(1)} %collective-permute-done.15.refs_3_), channel_id=1, source_target_pairs={{0,8},{8,16},{16,24},{24,28},{28,20},{20,12},{12,4},{4,0},{1,9},{9... | collective-permute-start | bytes 786440 | tf_op jit(solution)/shard_map/ppermute | solution.py:665
  82.4 28.4 %copy-start.2 = (bf16[4096,128]{1,0:T(8,128)(2,1)S(1)}, bf16[4096,128]{1,0:T(8,128)(2,1)}, u32[]{:S(2)}) copy-start(bf16[4096,128]{1,0:T(8,128)(2,1)} %refs_9_.3) | copy-start | bytes 3145732
  82.4 28.4 %copy-start.3 = (bf16[4096,128]{1,0:T(8,128)(2,1)S(1)}, bf16[4096,128]{1,0:T(8,128)(2,1)}, u32[]{:S(2)}) copy-start(bf16[4096,128]{1,0:T(8,128)(2,1)} %refs_10_.3) | copy-start | bytes 3145732
  83.0 12.8 %collective-permute-start.24 = (bf16[32,4096]{1,0:T(8,128)(2,1)S(1)}, bf16[32,4096]{1,0:T(8,128)(2,1)S(1)}, u32[]{:S(2)}, u32[]{:S(2)}) collective-permute-start(bf16[32,4096]{1,0:T(8,128)(2,1)S(1)} %collective-permute-done.22.refs_10_), channel_id=1, source_target_pairs={{8,0},{16,8},{24,16},{28,24},{20,28},{12,20},{4,12},{0,4},{9,1},{1... | collective-permute-start | bytes 786440 | tf_op jit(solution)/shard_map/ppermute | solution.py:666
  83.1 16.6 %collective-permute-start.32 = (bf16[32,4096]{1,0:T(8,128)(2,1)S(1)}, bf16[32,4096]{1,0:T(8,128)(2,1)S(1)}, u32[]{:S(2)}, u32[]{:S(2)}) collective-permute-start(bf16[32,4096]{1,0:T(8,128)(2,1)S(1)} %collective-permute-done.30.refs_4_), channel_id=1, source_target_pairs={{8,0},{16,8},{24,16},{28,24},{20,28},{12,20},{4,12},{0,4},{9,1},{1... | collective-permute-start | bytes 786440 | tf_op jit(solution)/shard_map/ppermute | solution.py:666
  84.5 14.7 %collective-permute-start.18 = (bf16[32,4096]{1,0:T(8,128)(2,1)S(1)}, bf16[32,4096]{1,0:T(8,128)(2,1)S(1)}, u32[]{:S(2)}, u32[]{:S(2)}) collective-permute-start(bf16[32,4096]{1,0:T(8,128)(2,1)S(1)} %collective-permute-done.16.refs_4_), channel_id=1, source_target_pairs={{8,0},{16,8},{24,16},{28,24},{20,28},{12,20},{4,12},{0,4},{9,1},{1... | collective-permute-start | bytes 786440 | tf_op jit(solution)/shard_map/ppermute | solution.py:666
  90.1 12.0 %collective-permute-start.25 = (bf16[32,4096]{1,0:T(8,128)(2,1)S(1)}, bf16[32,4096]{1,0:T(8,128)(2,1)S(1)}, u32[]{:S(2)}, u32[]{:S(2)}) collective-permute-start(bf16[32,4096]{1,0:T(8,128)(2,1)S(1)} %collective-permute-done.23.refs_11_), channel_id=1, source_target_pairs={{0,8},{8,16},{16,24},{24,28},{28,20},{20,12},{12,4},{4,0},{1,9},{9... | collective-permute-start | bytes 786440 | tf_op jit(solution)/shard_map/ppermute | solution.py:665
  95.7 21.7 %collective-permute-start.10 = (bf16[128,4096]{1,0:T(8,128)(2,1)S(1)}, bf16[128,4096]{1,0:T(8,128)(2,1)S(1)}, u32[]{:S(2)}, u32[]{:S(2)}) collective-permute-start(bf16[128,4096]{1,0:T(8,128)(2,1)S(1)} %get-tuple-element.44.refs_1_), channel_id=1, source_target_pairs={{0,1},{1,0},{2,3},{3,2},{4,5},{5,4},{6,7},{7,6},{8,9},{9,8},{10,11... | collective-permute-start | bytes 3145736 | tf_op jit(solution)/shard_map/ppermute | solution.py:698
  95.8 6.3 %collective-permute-start.12 = (f32[128,128]{1,0:T(8,128)S(1)}, f32[128,128]{1,0:T(8,128)S(1)}, u32[]{:S(2)}, u32[]{:S(2)}) collective-permute-start(f32[128,128]{1,0:T(8,128)S(1)} %pad_maximum_fusion.refs_3_), channel_id=1, source_target_pairs={{0,1},{1,0},{2,3},{3,2},{4,5},{5,4},{6,7},{7,6},{8,9},{9,8},{10,11... | collective-permute-start | bytes 196616 | tf_op jit(solution)/shard_map/ppermute | solution.py:698
  99.2 8.6 %collective-permute-start.26 = (bf16[32,4096]{1,0:T(8,128)(2,1)S(1)}, bf16[32,4096]{1,0:T(8,128)(2,1)S(1)}, u32[]{:S(2)}, u32[]{:S(2)}) collective-permute-start(bf16[32,4096]{1,0:T(8,128)(2,1)S(1)} %collective-permute-done.24.refs_12_), channel_id=1, source_target_pairs={{8,0},{16,8},{24,16},{28,24},{20,28},{12,20},{4,12},{0,4},{9,1},{1... | collective-permute-start | bytes 786440 | tf_op jit(solution)/shard_map/ppermute | solution.py:666
  99.7 8.4 %collective-permute-start.19 = (bf16[16,4096]{1,0:T(8,128)(2,1)S(1)}, bf16[16,4096]{1,0:T(8,128)(2,1)S(1)}, u32[]{:S(2)}, u32[]{:S(2)}) collective-permute-start(bf16[16,4096]{1,0:T(8,128)(2,1)S(1)} %slice.52), channel_id=1, source_target_pairs={{0,8},{8,16},{16,24},{24,28},{28,20},{20,12},{12,4},{4,0},{1,9},{9... | collective-permute-start | bytes 393224 | tf_op jit(solution)/shard_map/ppermute | solution.py:665
  102.1 8.0 %collective-permute-start.20 = (bf16[16,4096]{1,0:T(8,128)(2,1)S(1)}, bf16[16,4096]{1,0:T(8,128)(2,1)S(1)}, u32[]{:S(2)}, u32[]{:S(2)}) collective-permute-start(bf16[16,4096]{1,0:T(8,128)(2,1)S(1)} %slice.53), channel_id=1, source_target_pairs={{8,0},{16,8},{24,16},{28,24},{20,28},{12,20},{4,12},{0,4},{9,1},{1... | collective-permute-start | bytes 393224 | tf_op jit(solution)/shard_map/ppermute | solution.py:666
  102.1 9.3 %collective-permute-start.33 = (bf16[16,4096]{1,0:T(8,128)(2,1)S(1)}, bf16[16,4096]{1,0:T(8,128)(2,1)S(1)}, u32[]{:S(2)}, u32[]{:S(2)}) collective-permute-start(bf16[16,4096]{1,0:T(8,128)(2,1)S(1)} %get-tuple-element.58), channel_id=1, source_target_pairs={{0,8},{8,16},{16,24},{24,28},{28,20},{20,12},{12,4},{4,0},{1,9},{9... | collective-permute-start | bytes 393224 | tf_op jit(solution)/shard_map/ppermute | solution.py:665
  107.8 6.2 %collective-permute-start.36 = (bf16[16,4096]{1,0:T(8,128)(2,1)S(1)}, bf16[16,4096]{1,0:T(8,128)(2,1)S(1)}, u32[]{:S(2)}, u32[]{:S(2)}) collective-permute-start(bf16[16,4096]{1,0:T(8,128)(2,1)S(1)} %get-tuple-element.55), channel_id=1, source_target_pairs={{8,0},{16,8},{24,16},{28,24},{20,28},{12,20},{4,12},{0,4},{9,1},{1... | collective-permute-start | bytes 393224 | tf_op jit(solution)/shard_map/ppermute | solution.py:666
  108.1 6.6 %collective-permute-start.27 = (bf16[16,4096]{1,0:T(8,128)(2,1)S(1)}, bf16[16,4096]{1,0:T(8,128)(2,1)S(1)}, u32[]{:S(2)}, u32[]{:S(2)}) collective-permute-start(bf16[16,4096]{1,0:T(8,128)(2,1)S(1)} %slice.54), channel_id=1, source_target_pairs={{0,8},{8,16},{16,24},{24,28},{28,20},{20,12},{12,4},{4,0},{1,9},{9... | collective-permute-start | bytes 393224 | tf_op jit(solution)/shard_map/ppermute | solution.py:665
  110.1 7.0 %collective-permute-start.28 = (bf16[16,4096]{1,0:T(8,128)(2,1)S(1)}, bf16[16,4096]{1,0:T(8,128)(2,1)S(1)}, u32[]{:S(2)}, u32[]{:S(2)}) collective-permute-start(bf16[16,4096]{1,0:T(8,128)(2,1)S(1)} %slice.55), channel_id=1, source_target_pairs={{8,0},{16,8},{24,16},{28,24},{20,28},{12,20},{4,12},{0,4},{9,1},{1... | collective-permute-start | bytes 393224 | tf_op jit(solution)/shard_map/ppermute | solution.py:666
  111.5 9.0 %collective-permute-start.34 = (bf16[16,4096]{1,0:T(8,128)(2,1)S(1)}, bf16[16,4096]{1,0:T(8,128)(2,1)S(1)}, u32[]{:S(2)}, u32[]{:S(2)}) collective-permute-start(bf16[16,4096]{1,0:T(8,128)(2,1)S(1)} %get-tuple-element.57), channel_id=1, source_target_pairs={{0,8},{8,16},{16,24},{24,28},{28,20},{20,12},{12,4},{4,0},{1,9},{9... | collective-permute-start | bytes 393224 | tf_op jit(solution)/shard_map/ppermute | solution.py:665
  114.0 6.5 %collective-permute-start.35 = (bf16[16,4096]{1,0:T(8,128)(2,1)S(1)}, bf16[16,4096]{1,0:T(8,128)(2,1)S(1)}, u32[]{:S(2)}, u32[]{:S(2)}) collective-permute-start(bf16[16,4096]{1,0:T(8,128)(2,1)S(1)} %get-tuple-element.56), channel_id=1, source_target_pairs={{8,0},{16,8},{24,16},{28,24},{20,28},{12,20},{4,12},{0,4},{9,1},{1... | collective-permute-start | bytes 393224 | tf_op jit(solution)/shard_map/ppermute | solution.py:666
  114.7 5.8 %collective-permute-start.37 = (bf16[16,4096]{1,0:T(8,128)(2,1)S(1)}, bf16[16,4096]{1,0:T(8,128)(2,1)S(1)}, u32[]{:S(2)}, u32[]{:S(2)}) collective-permute-start(bf16[16,4096]{1,0:T(8,128)(2,1)S(1)} %collective-permute-done.33.refs_7_), channel_id=1, source_target_pairs={{0,8},{8,16},{16,24},{24,28},{28,20},{20,12},{12,4},{4,0},{1,9},{9... | collective-permute-start | bytes 393224 | tf_op jit(solution)/shard_map/ppermute | solution.py:665
  117.1 5.0 %collective-permute-start.38 = (bf16[16,4096]{1,0:T(8,128)(2,1)S(1)}, bf16[16,4096]{1,0:T(8,128)(2,1)S(1)}, u32[]{:S(2)}, u32[]{:S(2)}) collective-permute-start(bf16[16,4096]{1,0:T(8,128)(2,1)S(1)} %collective-permute-done.36.refs_10_), channel_id=1, source_target_pairs={{8,0},{16,8},{24,16},{28,24},{20,28},{12,20},{4,12},{0,4},{9,1},{1... | collective-permute-start | bytes 393224 | tf_op jit(solution)/shard_map/ppermute | solution.py:666
  122.8 2.0 %collective-permute-start.41 = (bf16[128,2048]{1,0:T(8,128)(2,1)S(1)}, bf16[128,2048]{1,0:T(8,128)(2,1)S(1)}, u32[]{:S(2)}, u32[]{:S(2)}) collective-permute-start(bf16[128,2048]{1,0:T(8,128)(2,1)S(1)} %get-tuple-element.54), channel_id=1, source_target_pairs={{0,1},{1,0},{2,3},{3,2},{4,5},{5,4},{6,7},{7,6},{8,9},{9,8},{10,11... | collective-permute-start | bytes 1572872 | tf_op jit(solution)/shard_map/ppermute | solution.py:698
  123.6 2.9 %collective-permute-start.39 = (bf16[128,2048]{1,0:T(8,128)(2,1)S(1)}, bf16[128,2048]{1,0:T(8,128)(2,1)S(1)}, u32[]{:S(2)}, u32[]{:S(2)}) collective-permute-start(bf16[128,2048]{1,0:T(8,128)(2,1)S(1)} %get-tuple-element.52), channel_id=1, source_target_pairs={{0,1},{1,0},{2,3},{3,2},{4,5},{5,4},{6,7},{7,6},{8,9},{9,8},{10,11... | collective-permute-start | bytes 1572872 | tf_op jit(solution)/shard_map/ppermute | solution.py:698
  124.9 9.2 %collective-permute-start.42 = (bf16[64,2048]{1,0:T(8,128)(2,1)S(1)}, bf16[64,2048]{1,0:T(8,128)(2,1)S(1)}, u32[]{:S(2)}, u32[]{:S(2)}) collective-permute-start(bf16[64,2048]{1,0:T(8,128)(2,1)S(1)} %slice.64), channel_id=1, source_target_pairs={{0,2},{1,3},{2,0},{3,1},{4,6},{5,7},{6,4},{7,5},{8,10},{9,11},{10,... | collective-permute-start | bytes 786440 | tf_op jit(solution)/shard_map/ppermute | solution.py:698
  126.6 12.3 %collective-permute-start.40 = (bf16[64,2048]{1,0:T(8,128)(2,1)S(1)}, bf16[64,2048]{1,0:T(8,128)(2,1)S(1)}, u32[]{:S(2)}, u32[]{:S(2)}) collective-permute-start(bf16[64,2048]{1,0:T(8,128)(2,1)S(1)} %slice.65), channel_id=1, source_target_pairs={{0,2},{1,3},{2,0},{3,1},{4,6},{5,7},{6,4},{7,5},{8,10},{9,11},{10,... | collective-permute-start | bytes 786440 | tf_op jit(solution)/shard_map/ppermute | solution.py:698
  (6 other events, 18.2 us)
